TPU v7x, 256 devices: a whole 4x4x8 slice. The times are simulated.
256 devices in a mesh: sp: 64 (over z, x, core), tp: 4 (over y).
Axes of the slice: x: 4, y: 4, z: 8, core: 2. Of those that a mesh axis runs over, the one named last changes fastest.
Arguments:
- conv_out: bfloat16 [12288, 2048], P('sp', 'tp'), may hold values from -6 to 6
- gate_in: bfloat16 [12288, 2048], P('sp', 'tp'), may hold values from -6 to 6
- block_states: float32 [64, 2048], P('sp', 'tp'), may hold values from -4 to 4
- decay_param: float32 [2048], P('tp'), may hold values from 4 to 20
- decay_shift: float32 [12288], P('sp'), may hold values from -2 to 0, as said below
- w_reset: bfloat16 [16, 128, 128], P('tp'), may hold values from -0.5 to 0.5
- w_input: bfloat16 [16, 128, 128], P('tp'), may hold values from -0.5 to 0.5
- w_out: bfloat16 [2048, 2048], P('tp'), may hold values from -0.125 to 0.125
- mixed: bfloat16 [12288, 2048], P('sp', 'tp'), may hold values from -6 to 6
- d_out: bfloat16 [12288, 2048], P('sp', 'tp'), may hold values from -16 to 16
- expert_ids: int32 [12288, 2], P('sp'), may hold values from 0 to 63, all different within a row; in each aligned block of 192 rows (0 to 191, 192 to 383, ...) at most 12 rows name the same one
- route_weights: float32 [12288, 2], P('sp'), may hold values from 0.2 to 1.4
- w_gate: bfloat16 [64, 2048, 1024], P('sp', None, 'tp'), may hold values from -0.125 to 0.125
- w_up: bfloat16 [64, 2048, 1024], P('sp', None, 'tp'), may hold values from -0.125 to 0.125
- w_down: bfloat16 [64, 1024, 2048], P('sp', 'tp'), may hold values from -0.1875 to 0.1875
Outputs:
- grad_w_gate: float32 [64, 2048, 1024], P('sp', None, 'tp')
- grad_w_up: float32 [64, 2048, 1024], P('sp', None, 'tp')
- grad_w_down: float32 [64, 1024, 2048], P('sp', 'tp')
- grad_out_proj_t: float32 [2048, 2048], P('sp', 'tp')
- recurrence_input_gradient: bfloat16 [12288, 2048], P('sp', 'tp')
- grad_gate: bfloat16 [12288, 2048], P('sp', 'tp')
Inputs may be any that keep to these rules, and one draw needn't show every extreme that they name: `expert_ids`: each row names 2 different experts; among the 192 tokens of one index of sp no expert is named more than 12 times, and in some index of sp one expert is named exactly 12 times. decay_shift is at most -0.05 / 12288 at every position.
All inputs are finite; a program needn't handle non-finite values.
Results may differ from a plain program's by a relative error of at most 0.013.
Values may be sent and summed in bfloat16 or wider, within the bound.
No kernel may reach another device: no remote copies, remote signals or barrier semaphores. Data moves between devices by JAX's collectives and lax.ppermute only.
A program may use at most 128 MiB of HBM per device.

v0:
```python
import jax
import jax.numpy as jnp
from jax import lax
from jax.sharding import Mesh
from jax.sharding import PartitionSpec as P

SP = ("sp_0", "sp_1", "sp_2")


def in_one_piece(arrays, axis, split_dim, concat_dim, along):
    widths = [a.shape[along] for a in arrays]
    both = jnp.concatenate(arrays, axis=along)
    filled = lax.all_to_all(both, axis, split_axis=split_dim, concat_axis=concat_dim, tiled=True)
    return tuple(jnp.split(filled, [sum(widths[:k]) for k in range(1, len(widths))], axis=along))


def side_by_side(arrays, axis, dim, along):
    both = jnp.concatenate(arrays, axis=along)
    filled, at, done = (lax.all_gather(both, axis, axis=dim, tiled=True), 0, [])
    for a in arrays:
        done.append(lax.slice_in_dim(filled, at, at + a.shape[along], axis=along))
        at += a.shape[along]
    return tuple(done)


def split_up(value, dim, devices):
    before, after = (value.shape[:dim], value.shape[dim + 1 :])
    return jnp.moveaxis(value.reshape(*before, devices, -1, *after), dim, 0)


def sent_and_summed(value, axis, dim):
    devices = lax.axis_size(axis)
    parts = lax.all_to_all(split_up(value, dim, devices), axis, 0, 0, tiled=True)
    return jnp.sum(parts.astype(jnp.float32), axis=0)


def copy_for_each(value, axis):
    devices = lax.axis_size(axis)
    return lax.all_to_all(
        jnp.broadcast_to(value[None], (devices, *value.shape)), axis, 0, 0, tiled=True
    )


def in_order(parts, dim):
    parts = jnp.moveaxis(parts, 0, dim)
    lengths = parts.shape
    return parts.reshape(*lengths[:dim], lengths[dim] * lengths[dim + 1], *lengths[dim + 2 :])


def collect(value, axis, dim):
    parts = copy_for_each(value, axis)
    return in_order(parts, dim)


def own_rows(terms, axes):
    so_far = terms.astype(jnp.bfloat16)
    for axis in axes:
        so_far = lax.psum_scatter(so_far, axis, scatter_dimension=0, tiled=True)
    return so_far.astype(jnp.float32)


def all_in_one(value, axis):
    leaves = jax.tree.leaves(value)
    turns = sorted(range(len(leaves)), key=lambda k: -leaves[k].size)
    width = (1, *leaves[turns[0]].shape)[-1]
    lines = [
        jnp.pad(leaves[k].reshape(-1), (0, -leaves[k].size % width)).reshape(-1, width)
        for k in turns
    ]
    both, at, found = (copy_for_each(jnp.concatenate(lines), axis), 0, {})
    for k, line in zip(turns, lines):
        section = both[:, at : at + len(line)].reshape(len(both), -1)
        found[k] = section[:, : leaves[k].size].reshape(-1, *leaves[k].shape)
        at += len(line)
    numbers = iter(range(len(leaves)))
    return jax.tree.map(lambda _: found[next(numbers)], value)


def combined_pairwise(pieces, combine):
    while len(jax.tree.leaves(pieces)[0]) > 1:
        pieces = jax.vmap(combine)(
            *(jax.tree.map(lambda part: part[side::2], pieces) for side in (0, 1))
        )
    return jax.tree.map(lambda part: part[0], pieces)


def entering(value, axis, combine, identity):
    devices, here = (lax.axis_size(axis), lax.axis_index(axis))
    passed = jnp.arange(devices) > here

    def kept(part, zero, own):
        part = jnp.where(
            passed.reshape(-1, *(1 for _ in own.shape)), part, jnp.asarray(zero, own.dtype)
        )
        return part[::-1]

    pieces = all_in_one(value, axis)
    return combined_pairwise(jax.tree.map(kept, pieces, identity, value), combine)


def decay_combine(first_pair, second_pair):
    return (first_pair[0] * second_pair[0], second_pair[0] * first_pair[1] + second_pair[1])


def carry_combine(earlier_pair, later_pair):
    return (later_pair[0] * earlier_pair[0], later_pair[1] + later_pair[0] * earlier_pair[1])


def gelu_slope(values):
    outcome, pullback = jax.vjp(jax.nn.gelu, values)
    return (outcome, pullback(jnp.ones_like(values))[0])


def head_maps(values, weights):
    count = values.shape[0]
    split = values.reshape(count, weights.shape[0], weights.shape[1])
    mapped = jnp.einsum("thi,hij->thj", split, weights, preferred_element_type=jnp.float32)
    return mapped.reshape(count, -1)


def head_back(grads, weights):
    count = grads.shape[0]
    split = grads.reshape(count, weights.shape[0], weights.shape[2])
    mapped = jnp.einsum("thj,hij->thi", split, weights, preferred_element_type=jnp.float32)
    return mapped.reshape(count, -1)


def over_rows(left_matrix, right_matrix):
    return lax.dot_general(
        left_matrix, right_matrix, (((0,), (0,)), ((), ())), preferred_element_type=jnp.float32
    )


def against_rows(left_matrix, right_matrix):
    return lax.dot_general(
        left_matrix, right_matrix, (((1,), (1,)), ((), ())), preferred_element_type=jnp.float32
    )


def slot_layout(expert_ids, experts, capacity):
    tok_rows, top_k = expert_ids.shape
    flat_ids = expert_ids.reshape(-1)
    onehot = (flat_ids[:, None] == jnp.arange(experts, dtype=jnp.int32)[None, :]).astype(jnp.int32)
    slot_rank = jnp.sum((jnp.cumsum(onehot, axis=0) - 1) * onehot, axis=1)
    slot_index = flat_ids * capacity + slot_rank
    slot_table = (
        jnp.full((experts * capacity,), tok_rows * top_k, jnp.int32)
        .at[slot_index]
        .set(jnp.arange(tok_rows * top_k, dtype=jnp.int32))
    )
    return (slot_index, slot_table)


def place_slots(cot_part, row_part, route_weights, slot_table, experts, capacity):
    tok_rows, top_k = route_weights.shape
    columns = cot_part.shape[1]
    scaled = (
        (route_weights[:, :, None] * cot_part.astype(jnp.float32)[:, None, :])
        .astype(jnp.bfloat16)
        .reshape(tok_rows * top_k, columns)
    )
    scaled = jnp.concatenate([scaled, jnp.zeros((1, columns), jnp.bfloat16)], axis=0)
    padded = jnp.concatenate([row_part, jnp.zeros((1, columns), jnp.bfloat16)], axis=0)
    token_ids = jnp.where(slot_table < tok_rows * top_k, slot_table // top_k, tok_rows)
    send_cot = scaled[slot_table].reshape(experts, capacity, columns)
    send_rows = padded[token_ids].reshape(experts, capacity, columns)
    return (send_cot, send_rows)


def expert_terms(expert_in, expert_cot, gate_matrix, up_matrix, down_matrix):
    up_pre = jnp.dot(expert_in, gate_matrix, preferred_element_type=jnp.float32)
    linear = jnp.dot(expert_in, up_matrix, preferred_element_type=jnp.float32)
    sigmoid_up = jax.nn.sigmoid(up_pre)
    silu_up = up_pre * sigmoid_up
    hidden_state = (silu_up * linear).astype(jnp.bfloat16)
    d_hidden = against_rows(expert_cot, down_matrix)
    d_linear = (d_hidden * silu_up).astype(jnp.bfloat16)
    d_up = (d_hidden * linear * sigmoid_up * (1.0 + up_pre * (1.0 - sigmoid_up))).astype(
        jnp.bfloat16
    )
    grad_gate_e = over_rows(expert_in, d_up)
    grad_up_e = over_rows(expert_in, d_linear)
    grad_down_e = over_rows(hidden_state, expert_cot)
    partial_value = against_rows(d_up, gate_matrix) + against_rows(d_linear, up_matrix)
    return (grad_gate_e, grad_up_e, grad_down_e, partial_value)


def body(
    conv_out,
    gate_in,
    block_states,
    decay_param,
    decay_shift,
    w_reset,
    w_input,
    w_out,
    mixed,
    d_out,
    expert_ids,
    route_weights,
    w_gate,
    w_up,
    w_down,
):
    tok_rows, top_k = expert_ids.shape
    experts = lax.axis_size(SP)
    capacity = 2 * tok_rows * top_k // experts
    conv_full = conv_out.astype(jnp.float32)
    reset = jax.nn.sigmoid(head_maps(conv_out, w_reset))
    input_gate = jax.nn.sigmoid(head_maps(conv_out, w_input))
    slow_rate = jax.nn.softplus(-decay_param)
    log_decay = -8.0 * reset * slow_rate[None, :] + decay_shift[:, None]
    decays = jnp.exp(log_decay)
    norm_in = jnp.sqrt(-jnp.expm1(2.0 * log_decay))
    drives = norm_in * input_gate * conv_full
    cum_decay, cum_drive = lax.associative_scan(decay_combine, (decays, drives), axis=0)
    states = cum_decay * block_states + cum_drive
    prev_states = jnp.concatenate([block_states, states[:-1]], axis=0)
    gate_act, gate_deriv = gelu_slope(gate_in.astype(jnp.float32))
    merged_in = (gate_act * states).astype(jnp.bfloat16)
    slot_index, slot_table = slot_layout(expert_ids, experts, capacity)
    send_cot, send_rows = place_slots(d_out, mixed, route_weights, slot_table, experts, capacity)
    part_cot, part_rows = in_one_piece((send_cot, send_rows), SP, 0, 0, 1)
    got_cot, got_rows = side_by_side((part_cot, part_rows), "tp", 2, 0)
    width_full = got_cot.shape[2]
    grad_gate_e, grad_up_e, grad_down_e, partial_value = expert_terms(
        got_rows.reshape(-1, width_full),
        got_cot.reshape(-1, width_full),
        w_gate[0],
        w_up[0],
        w_down[0],
    )
    row_grad = sent_and_summed(partial_value.astype(jnp.bfloat16), "tp", 1).astype(jnp.bfloat16)
    columns = row_grad.shape[1]
    returned = lax.all_to_all(
        row_grad.reshape(experts, capacity, columns), SP, split_axis=0, concat_axis=0, tiled=True
    )
    summed = jnp.sum(
        returned.reshape(-1, columns)[slot_index]
        .astype(jnp.float32)
        .reshape(tok_rows, top_k, columns),
        axis=1,
    )
    d_columns = (d_out.astype(jnp.float32) + summed).astype(jnp.bfloat16)
    d_mixed = collect(d_columns, "tp", 1)
    grad_out_proj_t = own_rows(over_rows(d_mixed, merged_in), SP)
    d_merged = against_rows(d_mixed, w_out)
    grad_gate = (d_merged * states * gate_deriv).astype(jnp.bfloat16)
    d_states = d_merged * gate_act
    next_decay = jnp.concatenate([decays[1:], jnp.ones((1, decays.shape[1]), jnp.float32)], axis=0)
    prods_flipped, local_flipped = lax.associative_scan(
        decay_combine, (next_decay[::-1], d_states[::-1]), axis=0
    )
    products = prods_flipped[::-1]
    local_grad = local_flipped[::-1]
    block_prod = products[0] * decays[0]
    block_lead = decays[0] * local_grad[0]
    incoming = entering(
        (block_prod, block_lead),
        SP,
        carry_combine,
        (jnp.ones_like(block_prod), jnp.zeros_like(block_lead)),
    )
    state_grad = local_grad + products * incoming[1][None, :]
    d_log_decay = (
        state_grad * decays * prev_states
        - state_grad * input_gate * conv_full * decays * decays / norm_in
    )
    d_pre_reset = (d_log_decay * (-8.0 * slow_rate[None, :]) * reset * (1.0 - reset)).astype(
        jnp.bfloat16
    )
    d_pre_input = (state_grad * norm_in * conv_full * input_gate * (1.0 - input_gate)).astype(
        jnp.bfloat16
    )
    recurrence_input_gradient = (
        state_grad * norm_in * input_gate
        + head_back(d_pre_reset, w_reset)
        + head_back(d_pre_input, w_input)
    ).astype(jnp.bfloat16)
    return (
        grad_gate_e[None],
        grad_up_e[None],
        grad_down_e[None],
        grad_out_proj_t,
        recurrence_input_gradient,
        grad_gate,
    )


def solution(mesh):
    torus = Mesh(mesh.devices.reshape(8, 4, 2, mesh.shape["tp"]), ("sp_0", "sp_1", "sp_2", "tp"))
    in_specs = (
        P(SP, "tp"),
        P(SP, "tp"),
        P(SP, "tp"),
        P("tp"),
        P(SP),
        P("tp", None, None),
        P("tp", None, None),
        P("tp", None),
        P(SP, "tp"),
        P(SP, "tp"),
        P(SP, None),
        P(SP, None),
        P(SP, None, "tp"),
        P(SP, None, "tp"),
        P(SP, "tp", None),
    )
    out_specs = (
        P(SP, None, "tp"),
        P(SP, None, "tp"),
        P(SP, "tp", None),
        P(SP, "tp"),
        P(SP, "tp"),
        P(SP, "tp"),
    )
    return jax.shard_map(body, mesh=torus, in_specs=in_specs, out_specs=out_specs, check_vma=False)
```

profile of v0, /device:TPU:24, one launch (start us, length us, event | category | flops | bytes accessed | tf_op | source)
XLA Modules:
  0.0 500.6 jit_solution(14403873241260485137)
XLA Ops:
  10.8 2.9 scatter_custom_fusion
  14.7 3.3 gather_fusion.1
  24.5 3.3 gather_fusion
  31.7 51.8 %all_to_all.25 = bf16[64,24,512]{2,1,0:T(8,128)(2,1)S(1)} all-to-all(bf16[64,24,512]{2,1,0:T(8,128)(2,1)S(1)} %pad_maximum_fusion.1), channel_id=1, replica_groups=mesh['sp_0'=8,'sp_1'=4,'sp_2'=2,'tp'=4] {'sp_0','sp_1','sp_2'}, dimensions={0} | all-to-all | bytes 3145728 | tf_op jit(solution)/shard_map/all_to_all | solution.py:13
  99.2 67.1 %all-gather.2.cloned.1.call-done = bf16[128,12,2048]{2,1,0:T(8,128)(2,1)} async-done(((bf16[128,12,512]{2,1,0:T(8,128)(2,1)}), bf16[128,12,2048]{2,1,0:T(8,128)(2,1)}) %all-gather.2.cloned.1.call-update) | async-done | bytes 6291472 | tf_op jit(solution)/shard_map/all_gather | solution.py:19
  166.3 6.1 %fusion.94 = (bf16[64,12,2048]{2,1,0:T(8,128)(2,1)}, bf16[64,12,2048]{2,1,0:T(8,128)(2,1)}) fusion(bf16[128,12,2048]{2,1,0:T(8,128)(2,1)} %all-gather.2.cloned.1.call-done), kind=kLoop, calls=%fused_computation.242 | loop fusion | bytes 12582912 | tf_op jit(solution)/shard_map/slice | solution.py:21
  172.5 6.2 %reshape.147 = bf16[768,2048]{1,0:T(8,128)(2,1)} reshape(bf16[64,12,2048]{2,1,0:T(8,128)(2,1)} %get-tuple-element.19) | data formatting | bytes 6291456 | tf_op jit(solution)/shard_map/reshape | solution.py:227
  178.6 4.2 fusion.10
  184.7 6.1 %reshape.148 = bf16[768,2048]{1,0:T(8,128)(2,1)} reshape(bf16[64,12,2048]{2,1,0:T(8,128)(2,1)} %get-tuple-element.18) | data formatting | bytes 6291456 | tf_op jit(solution)/shard_map/reshape | solution.py:228
  190.9 3.9 multiply_convert_fusion.1
  199.3 6.5 %all-to-all-start.1 = ((bf16[4,768,512]{2,1,0:T(8,128)(2,1)}), bf16[4,768,512]{2,1,0:T(8,128)(2,1)}, u32[]{:S(2)}, u32[]{:S(2)}) async-start(bf16[4,768,512]{2,1,0:T(8,128)(2,1)} %bitcast.160), calls=%async_computation.1 | async-start | bytes 6291456 | tf_op jit(solution)/shard_map/all_to_all | solution.py:33
  207.8 33.8 %all-to-all-done.1 = bf16[4,768,512]{2,1,0:T(8,128)(2,1)} async-done(((bf16[4,768,512]{2,1,0:T(8,128)(2,1)}), bf16[4,768,512]{2,1,0:T(8,128)(2,1)}, u32[]{:S(2)}, u32[]{:S(2)}) %all-to-all-start.1) | async-done | bytes 3145760 | tf_op jit(solution)/shard_map/all_to_all | solution.py:33
  245.6 11.1 %all-to-all-start.2 = ((bf16[64,12,512]{2,1,0:T(8,128)(2,1)}), bf16[64,12,512]{2,1,0:T(8,128)(2,1)}, u32[]{:S(2)}, u32[]{:S(2)}) async-start(bf16[64,12,512]{2,1,0:T(8,128)(2,1)} %reshape.150), calls=%async_computation.2 | async-start | bytes 2097152 | tf_op jit(solution)/shard_map/all_to_all | solution.py:235
  304.3 5.5 %all-to-all-start.3 = ((bf16[4,192,512]{2,1,0:T(8,128)(2,1)}), bf16[4,192,512]{2,1,0:T(8,128)(2,1)S(1)}, u32[]{:S(2)}, u32[]{:S(2)}) async-start(bf16[4,192,512]{2,1,0:T(8,128)(2,1)} %broadcast_in_dim.66), calls=%async_computation.3 | async-start | bytes 1572864 | tf_op jit(solution)/shard_map/all_to_all | solution.py:39
  315.5 2.9 slice.621
  324.7 4.3 convolution_bitcast_fusion.2
  331.1 3.4 fusion.22
  337.2 2.8 slice.627
  398.7 3.3 convolution_convert_fusion
  426.3 10.0 %all-to-all-start.4 = ((f32[64,2,512]{2,1,0:T(2,128)}), f32[64,2,512]{2,1,0:T(2,128)S(1)}, u32[]{:S(2)}, u32[]{:S(2)}) async-start(f32[64,2,512]{2,1,0:T(2,128)} %broadcast_in_dim.68), calls=%async_computation.7 | async-start | bytes 524288 | tf_op jit(solution)/shard_map/all_to_all | solution.py:39
  436.7 4.5 convolution_bitcast_fusion.1
  447.2 4.5 rev.5
  457.2 20.5 %reduce-scatter.6.cloned.1.call-done = bf16[64,512]{1,0:T(8,128)(2,1)} async-done(((bf16[256,512]{1,0:T(8,128)(2,1)}), bf16[64,512]{1,0:T(8,128)(2,1)}) %reduce-scatter.6.cloned.1.call-update) | async-done | bytes 65552 | tf_op jit(solution)/shard_map/reduce_scatter | solution.py:58
  479.5 13.2 %reduce-scatter.8.cloned.1.call-done = bf16[32,512]{1,0:T(8,128)(2,1)} async-done(((bf16[64,512]{1,0:T(8,128)(2,1)}), bf16[32,512]{1,0:T(8,128)(2,1)}) %reduce-scatter.8.cloned.1.call-update) | async-done | bytes 32784 | tf_op jit(solution)/shard_map/reduce_scatter | solution.py:58
  (461 shorter events, 204.0 us)
Async XLA Ops:
  7.2 323.9 %copy-start = (bf16[512,2048]{1,0:T(8,128)(2,1)S(1)}, bf16[512,2048]{1,0:T(8,128)(2,1)}, u32[]{:S(2)}) copy-start(bf16[512,2048]{1,0:T(8,128)(2,1)} %param.22) | copy-start | bytes 6291460
  7.2 159.1 %all-gather.2.cloned.1.call-start = ((), (), s32[]{:S(2)}) async-start(), calls=%async_computation.8 | async-start | bytes 10485760 | tf_op jit(solution)/shard_map/all_gather | solution.py:19
  87.7 84.8 %copy-start.6 = (f32[192,512]{1,0:T(8,128)}, f32[192,512]{1,0:T(8,128)S(1)}, u32[]{:S(2)}) copy-start(f32[192,512]{1,0:T(8,128)S(1)} %get-tuple-element.27) | copy-start | bytes 1179652
  96.9 75.5 %copy-start.23 = (f32[48,512]{1,0:T(8,128)}, f32[48,512]{1,0:T(8,128)S(1)}, u32[]{:S(2)}) copy-start(f32[48,512]{1,0:T(8,128)S(1)} %get-tuple-element.47) | copy-start | bytes 294916
  97.0 75.5 %copy-start.24 = (f32[48,512]{1,0:T(8,128)}, f32[48,512]{1,0:T(8,128)S(1)}, u32[]{:S(2)}) copy-start(f32[48,512]{1,0:T(8,128)S(1)} %get-tuple-element.46) | copy-start | bytes 294916
  199.3 42.3 %all-to-all-start.1 = ((bf16[4,768,512]{2,1,0:T(8,128)(2,1)}), bf16[4,768,512]{2,1,0:T(8,128)(2,1)}, u32[]{:S(2)}, u32[]{:S(2)}) async-start(bf16[4,768,512]{2,1,0:T(8,128)(2,1)} %bitcast.160), calls=%async_computation.1 | async-start | bytes 6291456 | tf_op jit(solution)/shard_map/all_to_all | solution.py:33
  245.6 25.8 %copy-start.7 = (f32[192,512]{1,0:T(8,128)S(1)}, f32[192,512]{1,0:T(8,128)}, u32[]{:S(2)}) copy-start(f32[192,512]{1,0:T(8,128)} %copy-done.6) | copy-start | bytes 1179652
  245.6 49.5 %all-to-all-start.2 = ((bf16[64,12,512]{2,1,0:T(8,128)(2,1)}), bf16[64,12,512]{2,1,0:T(8,128)(2,1)}, u32[]{:S(2)}, u32[]{:S(2)}) async-start(bf16[64,12,512]{2,1,0:T(8,128)(2,1)} %reshape.150), calls=%async_computation.2 | async-start | bytes 2097152 | tf_op jit(solution)/shard_map/all_to_all | solution.py:235
  261.7 14.5 %copy-start.35 = (f32[12,512]{1,0:T(8,128)S(1)}, f32[12,512]{1,0:T(8,128)}, u32[]{:S(2)}) copy-start(f32[12,512]{1,0:T(8,128)} %add.431) | copy-start | bytes 73732
  265.2 14.0 %copy-start.34 = (f32[23,512]{1,0:T(8,128)S(1)}, f32[23,512]{1,0:T(8,128)}, u32[]{:S(2)}) copy-start(f32[23,512]{1,0:T(8,128)} %slice.580) | copy-start | bytes 141316
  275.5 13.7 %copy-start.17 = (f32[95,512]{1,0:T(8,128)S(1)}, f32[95,512]{1,0:T(8,128)}, u32[]{:S(2)}) copy-start(f32[95,512]{1,0:T(8,128)} %slice.584) | copy-start | bytes 583684
  280.8 10.2 %copy-start.50 = (f32[1,512]{1,0:T(1,128)S(1)}, f32[1,512]{1,0:T(1,128)}, u32[]{:S(2)}) copy-start(f32[1,512]{1,0:T(1,128)} %slice.752) | copy-start | bytes 6148
  283.0 12.1 %copy-start.57 = (s32[384]{0:T(512)S(1)}, s32[384]{0:T(512)}, u32[]{:S(2)}) copy-start(s32[384]{0:T(512)} %copy-done.56) | copy-start | bytes 4612
  299.0 10.8 %copy-start.18 = (f32[95,512]{1,0:T(8,128)S(1)}, f32[95,512]{1,0:T(8,128)}, u32[]{:S(2)}) copy-start(f32[95,512]{1,0:T(8,128)} %get-tuple-element.36) | copy-start | bytes 583684
  299.0 10.8 %copy-start.49 = (f32[1,512]{1,0:T(1,128)S(1)}, f32[1,512]{1,0:T(1,128)}, u32[]{:S(2)}) copy-start(f32[1,512]{1,0:T(1,128)} %slice.731) | copy-start | bytes 6148
  304.3 24.7 %all-to-all-start.3 = ((bf16[4,192,512]{2,1,0:T(8,128)(2,1)}), bf16[4,192,512]{2,1,0:T(8,128)(2,1)S(1)}, u32[]{:S(2)}, u32[]{:S(2)}) async-start(bf16[4,192,512]{2,1,0:T(8,128)(2,1)} %broadcast_in_dim.66), calls=%async_computation.3 | async-start | bytes 1572864 | tf_op jit(solution)/shard_map/all_to_all | solution.py:39
  309.8 143.2 %reduce-scatter.4.cloned.1.call-start = ((), (), s32[]{:S(2)}) async-start(), calls=%async_computation.9 | async-start | bytes 2359296 | tf_op jit(solution)/shard_map/reduce_scatter | solution.py:58
  405.4 11.5 %copy-start.16 = (f32[95,512]{1,0:T(8,128)S(1)}, f32[95,512]{1,0:T(8,128)}, u32[]{:S(2)}) copy-start(f32[95,512]{1,0:T(8,128)} %slice.621) | copy-start | bytes 583684
  406.3 12.4 %copy-start.48 = (f32[1,512]{1,0:T(1,128)S(1)}, f32[1,512]{1,0:T(1,128)}, u32[]{:S(2)}) copy-start(f32[1,512]{1,0:T(1,128)} %slice.773) | copy-start | bytes 6148
  426.3 25.4 %all-to-all-start.4 = ((f32[64,2,512]{2,1,0:T(2,128)}), f32[64,2,512]{2,1,0:T(2,128)S(1)}, u32[]{:S(2)}, u32[]{:S(2)}) async-start(f32[64,2,512]{2,1,0:T(2,128)} %broadcast_in_dim.68), calls=%async_computation.7 | async-start | bytes 524288 | tf_op jit(solution)/shard_map/all_to_all | solution.py:39
  436.3 41.4 %reduce-scatter.6.cloned.1.call-start = ((), (), s32[]{:S(2)}) async-start(), calls=%async_computation.10 | async-start | bytes 327680 | tf_op jit(solution)/shard_map/reduce_scatter | solution.py:58
  443.6 9.5 %copy-start.2 = (f32[4,24,8,128]{3,2,1,0:T(8,128)S(1)}, f32[4,24,8,128]{3,2,1,0:T(8,128)}, u32[]{:S(2)}) copy-start(f32[4,24,8,128]{3,2,1,0:T(8,128)} %copy-done.1) | copy-start | bytes 1179652
  443.6 9.5 %copy-start.10 = (f32[192,512]{1,0:T(8,128)S(1)}, f32[192,512]{1,0:T(8,128)}, u32[]{:S(2)}) copy-start(f32[192,512]{1,0:T(8,128)} %get-tuple-element.7) | copy-start | bytes 1179652
  453.1 39.6 %reduce-scatter.8.cloned.1.call-start = ((), (), s32[]{:S(2)}) async-start(), calls=%async_computation.11 | async-start | bytes 98304 | tf_op jit(solution)/shard_map/reduce_scatter | solution.py:58
  (49 other events, 222.7 us)
Sparse Core Ops, SparseCore 0:
  85.8 80.4 all-gather.1
  402.2 48.5 reduce-scatter.3
  453.3 24.4 reduce-scatter.5
  480.1 12.5 reduce-scatter.7
where the time goes:
time: 508 us; the launch traced here: 501 us
  local copies, waits for them, and re-layouts  173 us (34%)
  waiting for transfers between devices  135 us (27%)
  other arithmetic  59.6 us (12%)
  blocking collectives  51.8 us (10%)
  starting transfers between devices  33.5 us (7%)
  matrix products  32.4 us (6%)
  between operations  15.3 us (3%)
    slice x53, local copies, waits for them, and re-layouts, body(): lax.associative_scan(decay_combine, (next_decay[::-1], d_states[::-1]), a...  68.3 us
    all_gather x1, waiting for transfers between devices, side_by_side(): filled, at, done = (lax.all_gather(both, axis, axis=dim, tiled=True), 0, [])  67.1 us
    all_to_all x1, blocking collectives, in_one_piece(): lax.all_to_all(both, axis, split_axis=split_dim, concat_axis=concat_dim,...  51.8 us
    all_to_all x1, waiting for transfers between devices, sent_and_summed(): lax.all_to_all(split_up(value, dim, devices), axis, 0, 0, tiled=True)  33.8 us
    reduce_scatter x3, waiting for transfers between devices, own_rows(): so_far = lax.psum_scatter(so_far, axis, scatter_dimension=0, tiled=True)  33.7 us
    slice x48, local copies, waits for them, and re-layouts, body(): lax.associative_scan(decay_combine, (decays, drives), axis=0)  21.7 us
    mul x26, other arithmetic, decay_combine(): first_pair[0] * second_pair[0]  20.5 us
    all_to_all x2, starting transfers between devices, copy_for_each(): lax.all_to_all(jnp.broadcast_to(value[None], (devices, *value.shape)), ax...  15.6 us
  transfers between devices with their start and end apart: 8, of which 4 were waited for; matrix products, arithmetic and copies ran while one was open for 23% of the time, Pallas kernels for 0%

commit v1 on v0

v1 whole, which is shorter than its diff:
```python
import jax
import jax.numpy as jnp
import numpy as np
from jax import lax
from jax.experimental import pallas as pl
from jax.experimental.pallas import tpu as pltpu
from jax.sharding import Mesh
from jax.sharding import PartitionSpec as P

SP = ("z", "x", "c")
XC = ("x", "c")
F32 = jnp.float32
BF16 = jnp.bfloat16
VMEM = pl.BlockSpec(memory_space=pltpu.VMEM)
SMEM = pl.BlockSpec(memory_space=pltpu.SMEM)

TOK = 192
WIDTH = 512
EXPERTS = 64
CAP = 12
BLOCK = 2 * CAP
ROWS = EXPERTS * CAP
HALF = ROWS // 2
GROUP = 8 * BLOCK
GROUPS = EXPERTS * BLOCK // GROUP
HID = 256


def dot(a, b):
    return lax.dot_general(a, b, (((1,), (0,)), ((), ())), preferred_element_type=F32)


def dot_bt(a, b):
    return lax.dot_general(a, b, (((1,), (1,)), ((), ())), preferred_element_type=F32)


def dot_at(a, b):
    return lax.dot_general(a, b, (((0,), (0,)), ((), ())), preferred_element_type=F32)


def shape(dims, dtype):
    return jax.ShapeDtypeStruct(dims, dtype)


def local(kernel, name, outs, flops, *args, scratch=(), smem=0):
    moved = sum(a.size * a.dtype.itemsize for a in (*args, *jax.tree.leaves(outs)))
    return pl.pallas_call(
        kernel,
        name=name,
        out_shape=outs,
        in_specs=[SMEM] * smem + [VMEM] * (len(args) - smem),
        out_specs=jax.tree.map(lambda _: VMEM, outs),
        scratch_shapes=list(scratch),
        cost_estimate=pl.CostEstimate(flops=int(flops), bytes_accessed=moved, transcendentals=0),
    )(*args)


def shift(value, axis, by):
    n = lax.axis_size(axis)
    return lax.ppermute(value, axis, [(i, (i + by) % n) for i in range(n)])


def exchange(value, axes):
    return lax.all_to_all(value, axes, 0, 0, tiled=True)


def one_hot(mask):
    return jnp.where(mask, 1.0, 0.0).astype(BF16)


def route_kernel(ids_ref, ids_t_ref, weights_t_ref, mixed_ref, d_out_ref, send_ref, slots_ref):
    i32 = jnp.int32
    before = one_hot(
        lax.broadcasted_iota(i32, (TOK, TOK), 0) < lax.broadcasted_iota(i32, (TOK, TOK), 1)
    )
    expert = lax.broadcasted_iota(i32, (EXPERTS, TOK), 0)
    rows = [ids_t_ref[k : k + 1, :] for k in range(2)]
    named = [r == expert for r in rows]
    count = dot(one_hot(named[0] | named[1]), before)
    slot = [
        rows[k] * BLOCK
        + jnp.sum(jnp.where(named[k], count, 0.0), axis=0, keepdims=True).astype(i32)
        for k in range(2)
    ]
    later = one_hot(
        lax.broadcasted_iota(i32, (TOK, TOK), 1) < lax.broadcasted_iota(i32, (TOK, TOK), 0)
    )
    expert_c = lax.broadcasted_iota(i32, (TOK, EXPERTS), 1)
    cols = [ids_ref[:, k : k + 1] for k in range(2)]
    named_c = [c == expert_c for c in cols]
    count_c = dot(later, one_hot(named_c[0] | named_c[1]))
    for k in range(2):
        rank = jnp.sum(jnp.where(named_c[k], count_c, 0.0), axis=1, keepdims=True)
        slots_ref[:, k : k + 1] = cols[k] * BLOCK + rank.astype(i32)
    weights = [weights_t_ref[k : k + 1, :] for k in range(2)]
    mixed = mixed_ref[...]
    d_out = d_out_ref[...]

    def pack(g):
        at = lax.broadcasted_iota(i32, (GROUP, TOK), 0) + g * GROUP
        to_mix = one_hot((slot[0] == at) | (slot[1] == at))
        first, second = (slot[0] + CAP == at, slot[1] + CAP == at)
        to_cot = one_hot(first | second)
        scale = jnp.sum(
            jnp.where(first, weights[0], 0.0) + jnp.where(second, weights[1], 0.0),
            axis=1,
            keepdims=True,
        )
        value = dot(to_mix, mixed) + dot(to_cot, d_out) * scale
        send_ref[pl.ds(pl.multiple_of(g * GROUP, GROUP), GROUP), :] = value.astype(BF16)

    def two(n, carry):
        pack(2 * n)
        pack(2 * n + 1)
        return carry

    lax.fori_loop(0, GROUPS // 2, two, 0)


def sort_matrix():
    matrix = np.zeros((GROUP, GROUP), np.float32)
    for j in range(8):
        for r in range(CAP):
            matrix[j * CAP + r, j * BLOCK + r] = 1
            matrix[GROUP // 2 + j * CAP + r, j * BLOCK + CAP + r] = 1
    return jnp.asarray(matrix, BF16)


def spread_matrix():
    matrix = np.zeros((GROUP, GROUP // 2), np.float32)
    for j in range(8):
        for r in range(BLOCK):
            matrix[j * BLOCK + r, j * CAP + r % CAP] = 1
    return jnp.asarray(matrix, BF16)


def sort_kernel(got_ref, order_ref, mix_a, mix_b, cot_a, cot_b):
    order = order_ref[...]
    half = GROUP // 2
    for g in range(GROUPS):
        out = dot(order, got_ref[g * GROUP : (g + 1) * GROUP, :]).astype(BF16)
        at = (g % (GROUPS // 2)) * half
        mix, cot = (mix_a, cot_a) if g < GROUPS // 2 else (mix_b, cot_b)
        mix[at : at + half, :] = out[:half]
        cot[at : at + half, :] = out[half:]


def block_of(me_ref, step):
    return pl.multiple_of(((me_ref[0] + step) % 4) * WIDTH, WIDTH)


STEPS = (0, 3, 1, 2)


def expert_up_kernel(me_ref, *refs):
    pieces, (gate_ref, up_ref), (hidden_ref, silu_ref, slope_ref) = refs[:8], refs[8:10], refs[10:]
    for h in range(2):
        up_pre = linear = None
        for p in range(4):
            piece = pieces[2 * p + h][...]
            at = block_of(me_ref, STEPS[p])
            one = dot(piece, gate_ref[pl.ds(at, WIDTH), :])
            two = dot(piece, up_ref[pl.ds(at, WIDTH), :])
            up_pre = one if up_pre is None else up_pre + one
            linear = two if linear is None else linear + two
        sigmoid = jax.nn.sigmoid(up_pre)
        silu = up_pre * sigmoid
        rows = slice(h * HALF, (h + 1) * HALF)
        hidden_ref[rows, :] = (silu * linear).astype(BF16)
        silu_ref[rows, :] = silu
        slope_ref[rows, :] = linear * sigmoid * (1.0 + up_pre * (1.0 - sigmoid))


def expert_down_kernel(me_ref, *refs):
    pieces = refs[:8]
    gate_ref, up_ref, down_ref, silu_ref, slope_ref = refs[8:13]
    d_up_ref, d_linear_ref, far_a, far_b, left_ref, right_ref, own_ref = refs[13:]
    ups, linears = [], []
    for h in range(2):
        rows = slice(h * HALF, (h + 1) * HALF)
        d_hidden = None
        for p in range(4):
            at = block_of(me_ref, STEPS[p])
            one = dot_bt(pieces[2 * p + h][...], down_ref[:, pl.ds(at, WIDTH)])
            d_hidden = one if d_hidden is None else d_hidden + one
        d_linear_ref[rows, :] = (d_hidden * silu_ref[rows, :]).astype(BF16)
        d_up_ref[rows, :] = (d_hidden * slope_ref[rows, :]).astype(BF16)

    def part(rows, step):
        at = block_of(me_ref, step)
        return (
            dot_bt(d_up_ref[rows, :], gate_ref[pl.ds(at, WIDTH), :])
            + dot_bt(d_linear_ref[rows, :], up_ref[pl.ds(at, WIDTH), :])
        ).astype(BF16)

    top, low = (slice(0, HALF), slice(HALF, ROWS))
    far_a[...] = part(top, 2)
    far_b[...] = part(low, 2)
    for rows in (top, low):
        left_ref[rows, :] = part(rows, 3)
        right_ref[rows, :] = part(rows, 1)
        own_ref[rows, :] = part(rows, 0)


def expert_grad_kernel(me_ref, *refs):
    mixes, cots = refs[:8], refs[8:16]
    d_up_ref, d_linear_ref, hidden_ref = refs[16:19]
    grad_gate_ref, grad_up_ref, grad_down_ref = refs[19:]
    top, low = (slice(0, HALF), slice(HALF, ROWS))
    for p in range(4):
        mix = (mixes[2 * p], mixes[2 * p + 1])
        cot = (cots[2 * p], cots[2 * p + 1])

        def step(n, carry):
            cols = pl.ds(pl.multiple_of(n * 128, 128), 128)
            at = pl.ds(pl.multiple_of(block_of(me_ref, STEPS[p]) + n * 128, 128), 128)
            mix_a, mix_b = (mix[0][:, cols], mix[1][:, cols])
            grad_gate_ref[0, at, :] = dot_at(mix_a, d_up_ref[top, :]) + dot_at(
                mix_b, d_up_ref[low, :]
            )
            grad_up_ref[0, at, :] = dot_at(mix_a, d_linear_ref[top, :]) + dot_at(
                mix_b, d_linear_ref[low, :]
            )
            grad_down_ref[0, :, at] = dot_at(hidden_ref[top, :], cot[0][:, cols]) + dot_at(
                hidden_ref[low, :], cot[1][:, cols]
            )
            return carry

        lax.fori_loop(0, 4, step, 0)


def spread_kernel(own_ref, la_ref, lb_ref, ra_ref, rb_ref, order_ref, out_ref):
    order = order_ref[...]
    half = GROUP // 2
    first = (lax.broadcasted_iota(jnp.int32, (GROUP, 1), 0) % BLOCK) < CAP
    for g in range(GROUPS):
        at = (g % (GROUPS // 2)) * half
        from_left, from_right = (la_ref, ra_ref) if g < GROUPS // 2 else (lb_ref, rb_ref)
        total = (
            own_ref[g * half : (g + 1) * half, :].astype(F32)
            + from_left[at : at + half, :].astype(F32)
            + from_right[at : at + half, :].astype(F32)
        ).astype(BF16)
        wide = dot(order, total)
        out_ref[g * GROUP : (g + 1) * GROUP, :] = jnp.where(
            first, wide[:, : WIDTH // 2], wide[:, WIDTH // 2 :]
        ).astype(BF16)


def combine_kernel(back_ref, slots_ref, d_out_ref, out_ref, send_ref):
    at = lax.broadcasted_iota(jnp.int32, (TOK, EXPERTS * BLOCK), 1)
    one, two = (slots_ref[:, 0:1], slots_ref[:, 1:2])
    back = back_ref[...]
    for h in range(2):
        pick = one_hot((one + h * CAP == at) | (two + h * CAP == at))
        cols = slice(h * WIDTH // 2, (h + 1) * WIDTH // 2)
        out_ref[:, cols] = (d_out_ref[:, cols].astype(F32) + dot(pick, back)).astype(BF16)
    source = lax.broadcasted_iota(jnp.int32, (WIDTH, WIDTH), 0)
    target = lax.broadcasted_iota(jnp.int32, (WIDTH, WIDTH), 1)
    wanted = ((target >> 5) & 1) * 256 + (target >> 6) * 32 + (target & 31)
    moved = dot(out_ref[...], one_hot(source == wanted))
    lane = lax.broadcasted_iota(jnp.int32, (TOK // 2, 128), 1)
    for m in range(4):
        top = moved[: TOK // 2, 128 * m : 128 * (m + 1)]
        low = moved[TOK // 2 :, 128 * m : 128 * (m + 1)]
        send_ref[2 * m] = jnp.where(lane < 64, top, pltpu.roll(low, 64, 1)).astype(BF16)
        send_ref[2 * m + 1] = jnp.where(lane < 64, pltpu.roll(top, 64, 1), low).astype(BF16)


def neg_expm1(y):
    small = 1.0 + y * (1.0 / 7.0)
    for n in (6.0, 5.0, 4.0, 3.0, 2.0):
        small = 1.0 + y * small * (1.0 / n)
    return jnp.where(y > -0.5, -y * small, 1.0 - jnp.exp(y))


CHUNK = 16


def forward_kernel(
    conv_ref,
    gate_ref,
    start_ref,
    slow_ref,
    shift_ref,
    w_reset_ref,
    w_input_ref,
    merged_ref,
    act_ref,
    slope_ref,
    decay_ref,
    kr_ref,
    ki_ref,
    kd_ref,
    pre_r,
    pre_i,
):
    for h in range(4):
        cols = slice(h * 128, (h + 1) * 128)
        pre_r[:, cols] = dot(conv_ref[:, cols], w_reset_ref[h])
        pre_i[:, cols] = dot(conv_ref[:, cols], w_input_ref[h])
    row = lax.broadcasted_iota(jnp.int32, (8, WIDTH), 0)
    slow = -8.0 * slow_ref[...]

    def step(c, state):
        rows = pl.ds(pl.multiple_of(c * CHUNK, CHUNK), CHUNK)
        conv = conv_ref[rows, :].astype(F32)
        reset = jax.nn.sigmoid(pre_r[rows, :])
        gate_in = jax.nn.sigmoid(pre_i[rows, :])
        log_decay = reset * slow + shift_ref[rows, :]
        decay = jnp.exp(log_decay)
        norm = jnp.sqrt(neg_expm1(2.0 * log_decay))
        direct = norm * gate_in
        drive = direct * conv
        states, prevs = [], []
        for s in range(0, CHUNK, 8):
            a, b = (decay[s : s + 8], drive[s : s + 8])
            for d in (1, 2, 4):
                keep = row >= d
                b = jnp.where(keep, b + a * pltpu.roll(b, d, 0), b)
                a = jnp.where(keep, a * pltpu.roll(a, d, 0), a)
            now = a * state + b
            prevs.append(jnp.where(row == 0, state, pltpu.roll(now, 1, 0)))
            states.append(now)
            state = now[7:8, :]
        states = jnp.concatenate(states, axis=0)
        prevs = jnp.concatenate(prevs, axis=0)
        x = gate_ref[rows, :].astype(F32)
        c0 = 0.7978845608028654
        t = jnp.tanh(c0 * (x + 0.044715 * x * x * x))
        act = 0.5 * x * (1.0 + t)
        deriv = 0.5 * (1.0 + t) + 0.5 * x * (1.0 - t * t) * (c0 * (1.0 + 0.134145 * x * x))
        merged_ref[rows, :] = (act * states).astype(BF16)
        act_ref[rows, :] = act
        slope_ref[rows, :] = states * deriv
        decay_ref[rows, :] = decay
        d_log = decay * prevs - gate_in * conv * decay * decay / norm
        kr_ref[rows, :] = d_log * slow * reset * (1.0 - reset)
        ki_ref[rows, :] = drive * (1.0 - gate_in)
        kd_ref[rows, :] = direct
        return state

    lax.fori_loop(0, TOK // CHUNK, step, start_ref[...])


def project_kernel(me_ref, p0, p1, p2, p3, merged_ref, out_ref):
    half = TOK // 2
    top = merged_ref[:, :half, :].reshape(8 * half, WIDTH)
    low = merged_ref[:, half:, :].reshape(8 * half, WIDTH)
    for piece, step in zip((p0, p1, p2, p3), STEPS):
        at = pl.multiple_of(((me_ref[0] + step) % 4) * 64, 64)
        value = piece[...].reshape(8 * half, 128)
        total = dot_at(value, top)[:64] + dot_at(value, low)[64:]
        out_ref[pl.ds(at, 64), :] = total.astype(BF16)


def reverse_kernel(
    me_ref,
    p0,
    p1,
    p2,
    p3,
    w_out_ref,
    act_ref,
    slope_ref,
    decay_ref,
    grad_gate_ref,
    local_ref,
    prod_ref,
    carry_ref,
    merged_ref,
):
    total = None
    for piece, step in zip((p0, p1, p2, p3), STEPS):
        one = dot_bt(piece[...], w_out_ref[:, pl.ds(block_of(me_ref, step), WIDTH)])
        total = one if total is None else total + one
    merged_ref[...] = total
    row = lax.broadcasted_iota(jnp.int32, (8, WIDTH), 0)
    steps = TOK // 16

    def step(n, state):
        grad, prod, after = state
        at = pl.multiple_of((steps - 1 - n) * 16, 16)
        rows16 = pl.ds(at, 16)
        d_merged = merged_ref[rows16, :]
        grad_gate_ref[rows16, :] = (d_merged * slope_ref[rows16, :]).astype(BF16)
        d_states = d_merged * act_ref[rows16, :]
        decays = decay_ref[rows16, :]
        for s in (8, 0):
            decay = decays[s : s + 8]
            a = jnp.where(row == 7, after, pltpu.roll(decay, 7, 0))
            b = d_states[s : s + 8]
            for d in (1, 2, 4):
                keep = row < 8 - d
                b = jnp.where(keep, b + a * pltpu.roll(b, 8 - d, 0), b)
                a = jnp.where(keep, a * pltpu.roll(a, 8 - d, 0), a)
            now = b + a * grad
            products = a * prod
            rows8 = pl.ds(pl.multiple_of(at + s, 8), 8)
            local_ref[rows8, :] = now
            prod_ref[rows8, :] = products
            grad, prod, after = (now[0:1, :], products[0:1, :], decay[0:1, :])
        return (grad, prod, after)

    one = jnp.ones((1, WIDTH), F32)
    grad, prod, first = lax.fori_loop(0, steps, step, (jnp.zeros((1, WIDTH), F32), one, one))
    prod, lead = (prod * first, grad * first)
    rows = [prod[:, k * 128 : (k + 1) * 128] for k in range(4)]
    rows += [lead[:, k * 128 : (k + 1) * 128] for k in range(4)]
    tile = jnp.concatenate(rows, axis=0)
    for k in range(EXPERTS):
        carry_ref[8 * k : 8 * k + 8, :] = tile


def final_kernel(
    here_ref,
    carry_ref,
    local_ref,
    prod_ref,
    kr_ref,
    ki_ref,
    kd_ref,
    w_reset_ref,
    w_input_ref,
    out_ref,
):
    here = here_ref[0]

    def fold(n, value):
        source = EXPERTS - 1 - n
        tile = carry_ref[pl.ds(pl.multiple_of(source * 8, 8), 8), :]
        return tile[4:8] + tile[0:4] * value

    entering = lax.fori_loop(0, EXPERTS - 1 - here, fold, jnp.zeros((4, 128), F32))
    for h in range(4):
        cols = slice(h * 128, (h + 1) * 128)
        grad = local_ref[:, cols] + prod_ref[:, cols] * entering[h : h + 1, :]
        d_reset = (grad * kr_ref[:, cols]).astype(BF16)
        d_input = (grad * ki_ref[:, cols]).astype(BF16)
        out_ref[:, cols] = (
            grad * kd_ref[:, cols]
            + dot_bt(d_reset, w_reset_ref[h])
            + dot_bt(d_input, w_input_ref[h])
        ).astype(BF16)


def gathered(a, b):
    left_a, right_b = (shift(a, "tp", 1), shift(b, "tp", -1))
    left_b, right_a = (shift(b, "tp", 1), shift(a, "tp", -1))
    far_a, far_b = (shift(left_a, "tp", 1), shift(right_b, "tp", -1))
    return (a, b, left_a, left_b, right_a, right_b, far_a, far_b)


def collected(value):
    return (value, shift(value, "tp", 1), shift(value, "tp", -1), shift(value, "tp", 2))


def after(value, *others):
    return lax.optimization_barrier((value, others))[0]


def body(
    conv_out,
    gate_in,
    block_states,
    decay_param,
    decay_shift,
    w_reset,
    w_input,
    w_out,
    mixed,
    d_out,
    expert_ids,
    route_weights,
    w_gate,
    w_up,
    w_down,
):
    me = lax.axis_index("tp").astype(jnp.int32).reshape(1)
    here = lax.axis_index(SP).astype(jnp.int32).reshape(1)
    unit = 2 * ROWS * 2048 * HID
    send, slots = local(
        route_kernel,
        "route",
        (shape((EXPERTS * BLOCK, WIDTH), BF16), shape((TOK, 2), jnp.int32)),
        1.3e9,
        expert_ids,
        expert_ids.T,
        route_weights.T,
        mixed,
        d_out,
    )
    got = exchange(send, SP)
    f_like = shape((TOK, WIDTH), F32)
    slow_rate = jax.nn.softplus(-decay_param)
    merged, act, slope, decay, kr, ki, kd = local(
        forward_kernel,
        "forward",
        (shape((TOK, WIDTH), BF16),) + (f_like,) * 6,
        6e9,
        after(conv_out, send),
        gate_in,
        block_states,
        slow_rate.reshape(1, -1),
        decay_shift.reshape(-1, 1),
        w_reset,
        w_input,
        scratch=(pltpu.VMEM((TOK, WIDTH), F32),) * 2,
    )
    got = after(got, merged)
    piece = shape((HALF, WIDTH), BF16)
    mix_a, mix_b, cot_a, cot_b = local(
        sort_kernel, "sort", (piece,) * 4, 1e9, got, sort_matrix()
    )
    mixes = gathered(mix_a, mix_b)
    cots = gathered(cot_a, cot_b)
    gate2, up2, down2 = (w_gate[0], w_up[0], w_down[0])
    hid = shape((ROWS, HID), BF16)
    hid_f = shape((ROWS, HID), F32)
    full = shape((ROWS, WIDTH), BF16)
    hidden, silu, up_slope = local(
        expert_up_kernel, "expert_up", (hid, hid_f, hid_f), 2 * unit, me, *mixes, gate2, up2, smem=1
    )
    merged_x = exchange(jnp.broadcast_to(after(merged, hidden)[None], (8, TOK, WIDTH)), XC)
    d_up, d_linear, far_a, far_b, left, right, own = local(
        expert_down_kernel,
        "expert_down",
        (hid, hid, piece, piece, full, full, full),
        3 * unit,
        me,
        *cots,
        gate2,
        up2,
        down2,
        silu,
        up_slope,
        smem=1,
    )
    over_a, over_b = (shift(far_a, "tp", 1), shift(far_b, "tp", -1))
    right_b, left_a = (shift(right[HALF:], "tp", 1), shift(left[:HALF], "tp", -1))
    add = lambda u, v: (u.astype(F32) + v.astype(F32)).astype(BF16)
    right_a = shift(add(right[:HALF], over_a), "tp", 1)
    left_b = shift(add(left[HALF:], over_b), "tp", -1)
    returned = local(
        spread_kernel,
        "spread",
        shape((EXPERTS * BLOCK, WIDTH // 2), BF16),
        1e9,
        after(own, merged_x),
        right_a,
        right_b,
        left_a,
        left_b,
        spread_matrix(),
    )
    back = exchange(returned, SP)
    grads = local(
        expert_grad_kernel,
        "expert_grad",
        (shape((1, 2048, HID), F32), shape((1, 2048, HID), F32), shape((1, HID, 2048), F32)),
        3 * unit,
        me,
        *mixes,
        *cots,
        after(d_up, returned),
        d_linear,
        hidden,
        smem=1,
    )
    back = after(back, grads)
    d_columns, crossing = local(
        combine_kernel,
        "combine",
        (shape((TOK, WIDTH), BF16), shape((8, TOK // 2, 128), BF16)),
        1e9,
        back,
        slots,
        d_out,
    )
    crossed = exchange(crossing, XC)
    pieces = collected(d_columns)
    columns = collected(crossed)
    grad_gate, local_grad, products, carries = local(
        reverse_kernel,
        "reverse",
        (shape((TOK, WIDTH), BF16), f_like, f_like, shape((EXPERTS * 8, 128), F32)),
        4e9,
        me,
        after(pieces[0], crossed),
        *pieces[1:],
        w_out,
        act,
        slope,
        decay,
        scratch=(pltpu.VMEM((TOK, WIDTH), F32),),
        smem=1,
    )
    carried = exchange(carries, SP)
    grad_part = local(
        project_kernel,
        "project",
        shape((256, WIDTH), BF16),
        1e9,
        me,
        *columns,
        merged_x,
        smem=1,
    )
    parts = exchange(grad_part, "z")
    grad_out_proj_t = jnp.sum(parts.reshape(8, -1, WIDTH).astype(F32), axis=0)
    out = local(
        final_kernel,
        "final",
        shape((TOK, WIDTH), BF16),
        2e9,
        here,
        carried,
        local_grad,
        products,
        kr,
        ki,
        kd,
        w_reset,
        w_input,
        smem=1,
    )
    return (*grads, grad_out_proj_t, out, grad_gate)


def solution(mesh):
    torus = Mesh(mesh.devices.reshape(8, 4, 2, mesh.shape["tp"]), ("z", "x", "c", "tp"))
    in_specs = (
        P(SP, "tp"),
        P(SP, "tp"),
        P(SP, "tp"),
        P("tp"),
        P(SP),
        P("tp", None, None),
        P("tp", None, None),
        P("tp", None),
        P(SP, "tp"),
        P(SP, "tp"),
        P(SP, None),
        P(SP, None),
        P(SP, None, "tp"),
        P(SP, None, "tp"),
        P(SP, "tp", None),
    )
    out_specs = (
        P(SP, None, "tp"),
        P(SP, None, "tp"),
        P(SP, "tp", None),
        P(SP, "tp"),
        P(SP, "tp"),
        P(SP, "tp"),
    )
    return jax.shard_map(body, mesh=torus, in_specs=in_specs, out_specs=out_specs, check_vma=False)
```

time: 508 us -> 253 us (0.50); the launches traced: 501 us -> 252 us
  local copies, waits for them, and re-layouts: 173 us -> 10.5 us
  other arithmetic: 59.6 us -> 2.46 us
  Pallas kernels: 0 us -> 54.8 us
  blocking collectives: 51.8 us -> 11.1 us
  starting transfers between devices: 33.5 us -> 68.5 us
  matrix products: 32.4 us -> 0 us
  waiting for transfers between devices: 135 us -> 104 us
  between operations: 15.3 us -> 0.86 us
    slice x129 -> x2, local copies, waits for them, and re-layouts: 97.5 us -> 2.04 us  [the longest x1 1.02 us: body(): left[:HALF]]
    all_gather x1 -> x0, waiting for transfers between devices: 67.1 us -> none  [side_by_side(): filled, at, done = (lax.all_gather(both, axis, axis=dim, tiled=True), 0, [])]
    pallas_call x0 -> x11, Pallas kernels: none -> 54.8 us  [local(): pl.pallas_call(kernel, name=name, out_shape=outs, in_specs=[SMEM] * smem...]
    ppermute x0 -> x24, waiting for transfers between devices: none -> 51.4 us  [shift(): return lax.ppermute(value, axis, [(i, (i + by) % n) for i in range(n)])]
    all_to_all x1, blocking collectives: 51.8 us -> 11.1 us  [exchange(): return lax.all_to_all(value, axes, 0, 0, tiled=True)]
    reduce_scatter x3 -> x0, waiting for transfers between devices: 33.7 us -> none  [own_rows(): so_far = lax.psum_scatter(so_far, axis, scatter_dimension=0, tiled=True)]
    ppermute x0 -> x24, starting transfers between devices: none -> 32.9 us  [shift(): return lax.ppermute(value, axis, [(i, (i + by) % n) for i in range(n)])]
    dot_general x14 -> x0, matrix products: 32.4 us -> none  [the longest x4 14.5 us: over_rows(): lax.dot_general(left_matrix, right_matrix, (((0,), (0,)), ((), ())), pref...]
  transfers between devices with their start and end apart: 8 -> 29, of which waited for: 4 -> 15; matrix products, arithmetic and copies ran while one was open for 23% -> 2% of each run, Pallas kernels for 0% -> 15%
where the time goes in v1:
time: 253 us; the launch traced here: 252 us
  waiting for transfers between devices  104 us (41%)
  starting transfers between devices  68.5 us (27%)
  Pallas kernels  54.8 us (22%)
  blocking collectives  11.1 us (4%)
  local copies, waits for them, and re-layouts  10.5 us (4%)
    pallas_call x11, Pallas kernels, local(): pl.pallas_call(kernel, name=name, out_shape=outs, in_specs=[SMEM] * smem...  54.8 us
    all_to_all x5, waiting for transfers between devices, exchange(): return lax.all_to_all(value, axes, 0, 0, tiled=True)  52.8 us
    ppermute x24, waiting for transfers between devices, shift(): return lax.ppermute(value, axis, [(i, (i + by) % n) for i in range(n)])  51.4 us
    all_to_all x5, starting transfers between devices, exchange(): return lax.all_to_all(value, axes, 0, 0, tiled=True)  35.6 us
    ppermute x24, starting transfers between devices, shift(): return lax.ppermute(value, axis, [(i, (i + by) % n) for i in range(n)])  32.9 us
    all_to_all x1, blocking collectives, exchange(): return lax.all_to_all(value, axes, 0, 0, tiled=True)  11.1 us
    unnamed x49, local copies, waits for them, and re-layouts  6.41 us
  transfers between devices with their start and end apart: 29, of which 15 were waited for; matrix products, arithmetic and copies ran while one was open for 2% of the time, Pallas kernels for 15%

profile of v1, /device:TPU:24, one launch (start us, length us, event | category | flops | bytes accessed | tf_op | source)
XLA Modules:
  0.0 252.3 jit_solution(1877137974000836910)
XLA Ops:
  2.1 4.3 %route.1 = (bf16[1536,512]{1,0:T(8,128)(2,1)}, s32[192,2]{1,0:T(8,128)}) custom-call(s32[192,2]{1,0:T(8,128)} %copy.24.ids_ref, s32[2,192]{1,0:T(2,128)} %bitcast.23, f32[2,192]{1,0:T(2,128)} %bitcast.31, bf16[192,512]{1,0:T(8,128)(2,1)} %mixed_ref.1, bf16[192,512]{1,0:T(8,128)(2,1)} %d_out_ref.3), custom_call_target="tpu_custom_call" | custom-call | flops 1300000000 | bytes 1972224 | tf_op jit(solution)/shard_map/route/pallas_call | solution.py:47
  6.3 12.1 %all-to-all-start = ((bf16[64,24,512]{2,1,0:T(8,128)(2,1)}), bf16[64,24,512]{2,1,0:T(8,128)(2,1)S(1)}, u32[]{:S(2)}, u32[]{:S(2)}) async-start(bf16[64,24,512]{2,1,0:T(8,128)(2,1)} %bitcast.17), calls=%async_computation | async-start | bytes 3145728 | tf_op jit(solution)/shard_map/all_to_all | solution.py:64
  19.8 5.2 %forward.1 = (bf16[192,512]{1,0:T(8,128)(2,1)}, f32[192,512]{1,0:T(8,128)}, f32[192,512]{1,0:T(8,128)}, f32[192,512]{1,0:T(8,128)}, f32[192,512]{1,0:T(8,128)}, /*index=5*/f32[192,512]{1,0:T(8,128)}, f32[192,512]{1,0:T(8,128)}) custom-call(bf16[192,512]{1,0:T(8,128)(2,1)} %conv_ref, bf16[192,512]{1,0:T(8,128)(2,1)} %gate_ref.1, f32[1,512]{1,0:T(1,128)} %start_ref.1, ...), custom_call_target="tpu_custom_call" | custom-call | flops 6000000000 | bytes 3216128 | tf_op jit(solution)/shard_map/forward/pallas_call | solution.py:47
  24.9 33.6 %all-to-all-done = bf16[64,24,512]{2,1,0:T(8,128)(2,1)S(1)} async-done(((bf16[64,24,512]{2,1,0:T(8,128)(2,1)}), bf16[64,24,512]{2,1,0:T(8,128)(2,1)S(1)}, u32[]{:S(2)}, u32[]{:S(2)}) %all-to-all-start) | async-done | bytes 1572896 | tf_op jit(solution)/shard_map/all_to_all | solution.py:64
  69.1 6.9 %collective-permute-done.2.refs_4_ = bf16[384,512]{1,0:T(8,128)(2,1)S(1)} collective-permute-done((bf16[384,512]{1,0:T(8,128)(2,1)}, bf16[384,512]{1,0:T(8,128)(2,1)S(1)}, u32[]{:S(2)}, u32[]{:S(2)}) %collective-permute-start.2) | collective-permute-done | bytes 393248 | tf_op jit(solution)/shard_map/ppermute | solution.py:60
  79.3 5.2 %collective-permute-done.3.refs_5_ = bf16[384,512]{1,0:T(8,128)(2,1)S(1)} collective-permute-done((bf16[384,512]{1,0:T(8,128)(2,1)}, bf16[384,512]{1,0:T(8,128)(2,1)S(1)}, u32[]{:S(2)}, u32[]{:S(2)}) %collective-permute-start.3) | collective-permute-done | bytes 393248 | tf_op jit(solution)/shard_map/ppermute | solution.py:60
  84.6 8.0 %collective-permute-done.6.refs_2_.refs_10_ = bf16[384,512]{1,0:T(8,128)(2,1)S(1)} collective-permute-done((bf16[384,512]{1,0:T(8,128)(2,1)}, bf16[384,512]{1,0:T(8,128)(2,1)S(1)}, u32[]{:S(2)}, u32[]{:S(2)}) %collective-permute-start.6) | collective-permute-done | bytes 393248 | tf_op jit(solution)/shard_map/ppermute | solution.py:60
  92.5 3.6 %collective-permute-start.7 = (bf16[384,512]{1,0:T(8,128)(2,1)}, bf16[384,512]{1,0:T(8,128)(2,1)}, u32[]{:S(2)}, u32[]{:S(2)}) collective-permute-start(bf16[384,512]{1,0:T(8,128)(2,1)} %get-tuple-element.52.refs_1_.refs_9_), channel_id=1, source_target_pairs={{0,1},{1,2},{2,3},{3,0},{4,5},{5,6},{6,7},{7,4},{8,9},{9,10},{10,1... | collective-permute-start | bytes 1179656 | tf_op jit(solution)/shard_map/ppermute | solution.py:60
  96.2 4.6 %collective-permute-done.4.refs_6_ = bf16[384,512]{1,0:T(8,128)(2,1)S(1)} collective-permute-done((bf16[384,512]{1,0:T(8,128)(2,1)S(1)}, bf16[384,512]{1,0:T(8,128)(2,1)S(1)}, u32[]{:S(2)}, u32[]{:S(2)}) %collective-permute-start.4) | collective-permute-done | bytes 393248 | tf_op jit(solution)/shard_map/ppermute | solution.py:60
  102.1 5.6 %expert_up.1 = (bf16[768,256]{1,0:T(8,128)(2,1)}, f32[768,256]{1,0:T(8,128)}, f32[768,256]{1,0:T(8,128)}) custom-call(s32[1]{0:T(128)} %bitcast.me_ref, bf16[384,512]{1,0:T(8,128)(2,1)} %get-tuple-element.49.refs_0_, bf16[384,512]{1,0:T(8,128)(2,1)} %get-tuple-element.50.refs_1_, bf16[384,512]{1,0:T(8,128)(2,1)} %copy-done.10, bf16[384,512]{1,0:T(8,128)(2,1)} %copy-done.12, ...), custom_call_target="tpu_custom_call" | custom-call | flops 1610612736 | bytes 7208964 | tf_op jit(solution)/shard_map/expert_up/pallas_call | solution.py:47
  109.0 4.3 %all-to-all-start.1 = ((bf16[8,192,512]{2,1,0:T(8,128)(2,1)}), bf16[8,192,512]{2,1,0:T(8,128)(2,1)S(1)}, u32[]{:S(2)}, u32[]{:S(2)}) async-start(bf16[8,192,512]{2,1,0:T(8,128)(2,1)} %broadcast_in_dim.2), calls=%async_computation.1 | async-start | bytes 3145728 | tf_op jit(solution)/shard_map/all_to_all | solution.py:64
  116.3 7.0 %expert_down.1 = (bf16[768,256]{1,0:T(8,128)(2,1)}, bf16[768,256]{1,0:T(8,128)(2,1)}, bf16[384,512]{1,0:T(8,128)(2,1)}, bf16[384,512]{1,0:T(8,128)(2,1)}, bf16[7...) custom-call(s32[1]{0:T(128)} %bitcast.me_ref, ...), custom_call_target="tpu_custom_call" | custom-call | flops 2415919104 | bytes 11796484 | tf_op jit(solution)/shard_map/expert_down/pallas_call | solution.py:47
  131.7 4.4 %collective-permute-done.12 = bf16[384,512]{1,0:T(8,128)(2,1)S(1)} collective-permute-done((bf16[384,512]{1,0:T(8,128)(2,1)}, bf16[384,512]{1,0:T(8,128)(2,1)S(1)}, u32[]{:S(2)}, u32[]{:S(2)}) %collective-permute-start.12) | collective-permute-done | bytes 393248 | tf_op jit(solution)/shard_map/ppermute | solution.py:60
  137.1 3.7 %collective-permute-start.13 = (bf16[384,512]{1,0:T(8,128)(2,1)S(1)}, bf16[384,512]{1,0:T(8,128)(2,1)}, u32[]{:S(2)}, u32[]{:S(2)}) collective-permute-start(bf16[384,512]{1,0:T(8,128)(2,1)S(1)} %add_convert_fusion.1), channel_id=1, source_target_pairs={{0,1},{1,2},{2,3},{3,0},{4,5},{5,6},{6,7},{7,4},{8,9},{9,10},{10,1... | collective-permute-start | bytes 1179656 | tf_op jit(solution)/shard_map/ppermute | solution.py:60
  141.0 7.0 %collective-permute-done.15.ra_ref = bf16[384,512]{1,0:T(8,128)(2,1)S(1)} collective-permute-done((bf16[384,512]{1,0:T(8,128)(2,1)S(1)}, bf16[384,512]{1,0:T(8,128)(2,1)S(1)}, u32[]{:S(2)}, u32[]{:S(2)}) %collective-permute-start.15) | collective-permute-done | bytes 393248 | tf_op jit(solution)/shard_map/ppermute | solution.py:60
  156.3 7.6 %all-to-all-start.2 = ((bf16[64,24,256]{2,1,0:T(8,128)(2,1)}), bf16[64,24,256]{2,1,0:T(8,128)(2,1)S(1)}, u32[]{:S(2)}, u32[]{:S(2)}) async-start(bf16[64,24,256]{2,1,0:T(8,128)(2,1)} %bitcast.19), calls=%async_computation.2 | async-start | bytes 1572864 | tf_op jit(solution)/shard_map/all_to_all | solution.py:64
  164.0 12.9 %expert_grad.1 = (f32[1,2048,256]{2,1,0:T(8,128)}, f32[1,2048,256]{2,1,0:T(8,128)}, f32[1,256,2048]{2,1,0:T(8,128)}) custom-call(s32[1]{0:T(128)} %bitcast.me_ref, bf16[384,512]{1,0:T(8,128)(2,1)} %get-tuple-element.49.refs_0_, bf16[384,512]{1,0:T(8,128)(2,1)} %get-tuple-element.50.refs_1_, bf16[384,512]{1,0:T(8,128)(2,1)} %copy-done.10, ...), custom_call_target="tpu_custom_call" | custom-call | flops 2415919104 | bytes 13762564 | tf_op jit(solution)/shard_map/expert_grad/pallas_call | solution.py:47
  176.9 10.1 %all-to-all-done.2 = bf16[64,24,256]{2,1,0:T(8,128)(2,1)S(1)} async-done(((bf16[64,24,256]{2,1,0:T(8,128)(2,1)}), bf16[64,24,256]{2,1,0:T(8,128)(2,1)S(1)}, u32[]{:S(2)}, u32[]{:S(2)}) %all-to-all-start.2) | async-done | bytes 786464 | tf_op jit(solution)/shard_map/all_to_all | solution.py:64
  194.0 11.1 %all_to_all.54.p0 = bf16[8,96,128]{2,1,0:T(8,128)(2,1)S(1)} all-to-all(bf16[8,96,128]{2,1,0:T(8,128)(2,1)} %get-tuple-element.71), channel_id=1, replica_groups=mesh['z'=8,'x'=4,'c'=2,'tp'=4] {'x','c'}, dimensions={0} | all-to-all | bytes 393216 | tf_op jit(solution)/shard_map/all_to_all | solution.py:64
  205.9 4.6 %reverse.1 = (bf16[192,512]{1,0:T(8,128)(2,1)}, f32[192,512]{1,0:T(8,128)}, f32[192,512]{1,0:T(8,128)}, f32[512,128]{1,0:T(8,128)}) custom-call(s32[1]{0:T(128)} %bitcast.me_ref, bf16[192,512]{1,0:T(8,128)(2,1)} %get-tuple-element.73.p0, bf16[192,512]{1,0:T(8,128)(2,1)} %copy-done.20, bf16[192,512]{1,0:T(8,128)(2,1)} %copy-done.19, ...), custom_call_target="tpu_custom_call" | custom-call | flops 4000000000 | bytes 5308420 | tf_op jit(solution)/shard_map/reverse/pallas_call | solution.py:47
  210.5 4.7 %all-to-all-start.5 = ((f32[64,8,128]{2,1,0:T(8,128)}), f32[64,8,128]{2,1,0:T(8,128)S(1)}, u32[]{:S(2)}, u32[]{:S(2)}) async-start(f32[64,8,128]{2,1,0:T(8,128)} %bitcast.22), calls=%async_computation.5 | async-start | bytes 524288 | tf_op jit(solution)/shard_map/all_to_all | solution.py:64
  220.8 3.7 %collective-permute-done.20.p3 = bf16[8,96,128]{2,1,0:T(8,128)(2,1)S(1)} collective-permute-done((bf16[8,96,128]{2,1,0:T(8,128)(2,1)S(1)}, bf16[8,96,128]{2,1,0:T(8,128)(2,1)S(1)}, u32[]{:S(2)}, u32[]{:S(2)}) %collective-permute-start.20) | collective-permute-done | bytes 196640 | tf_op jit(solution)/shard_map/ppermute | solution.py:60
  232.7 6.9 %all-to-all-start.4 = ((bf16[8,32,512]{2,1,0:T(8,128)(2,1)}), bf16[8,32,512]{2,1,0:T(8,128)(2,1)S(1)}, u32[]{:S(2)}, u32[]{:S(2)}) async-start(bf16[8,32,512]{2,1,0:T(8,128)(2,1)} %bitcast.21), calls=%async_computation.4 | async-start | bytes 524288 | tf_op jit(solution)/shard_map/all_to_all | solution.py:64
  242.6 9.1 %all-to-all-done.4 = bf16[8,32,512]{2,1,0:T(8,128)(2,1)S(1)} async-done(((bf16[8,32,512]{2,1,0:T(8,128)(2,1)}), bf16[8,32,512]{2,1,0:T(8,128)(2,1)S(1)}, u32[]{:S(2)}, u32[]{:S(2)}) %all-to-all-start.4) | async-done | bytes 262176 | tf_op jit(solution)/shard_map/all_to_all | solution.py:64
  (103 shorter events, 65.5 us)
Async XLA Ops:
  6.3 52.2 %all-to-all-start = ((bf16[64,24,512]{2,1,0:T(8,128)(2,1)}), bf16[64,24,512]{2,1,0:T(8,128)(2,1)S(1)}, u32[]{:S(2)}, u32[]{:S(2)}) async-start(bf16[64,24,512]{2,1,0:T(8,128)(2,1)} %bitcast.17), calls=%async_computation | async-start | bytes 3145728 | tf_op jit(solution)/shard_map/all_to_all | solution.py:64
  62.6 13.4 %collective-permute-start.2 = (bf16[384,512]{1,0:T(8,128)(2,1)}, bf16[384,512]{1,0:T(8,128)(2,1)S(1)}, u32[]{:S(2)}, u32[]{:S(2)}) collective-permute-start(bf16[384,512]{1,0:T(8,128)(2,1)} %get-tuple-element.49.refs_0_), channel_id=1, source_target_pairs={{0,3},{1,0},{2,1},{3,2},{4,7},{5,4},{6,5},{7,6},{8,11},{9,8},{10,9... | collective-permute-start | bytes 1179656 | tf_op jit(solution)/shard_map/ppermute | solution.py:60
  63.4 12.7 %collective-permute-start = (bf16[384,512]{1,0:T(8,128)(2,1)}, bf16[384,512]{1,0:T(8,128)(2,1)S(1)}, u32[]{:S(2)}, u32[]{:S(2)}) collective-permute-start(bf16[384,512]{1,0:T(8,128)(2,1)} %get-tuple-element.49.refs_0_), channel_id=1, source_target_pairs={{0,1},{1,2},{2,3},{3,0},{4,5},{5,6},{6,7},{7,4},{8,9},{9,10},{10,1... | collective-permute-start | bytes 1179656 | tf_op jit(solution)/shard_map/ppermute | solution.py:60
  65.9 18.6 %collective-permute-start.3 = (bf16[384,512]{1,0:T(8,128)(2,1)}, bf16[384,512]{1,0:T(8,128)(2,1)S(1)}, u32[]{:S(2)}, u32[]{:S(2)}) collective-permute-start(bf16[384,512]{1,0:T(8,128)(2,1)} %get-tuple-element.50.refs_1_), channel_id=1, source_target_pairs={{0,3},{1,0},{2,1},{3,2},{4,7},{5,4},{6,5},{7,6},{8,11},{9,8},{10,9... | collective-permute-start | bytes 1179656 | tf_op jit(solution)/shard_map/ppermute | solution.py:60
  65.9 18.6 %collective-permute-start.1 = (bf16[384,512]{1,0:T(8,128)(2,1)}, bf16[384,512]{1,0:T(8,128)(2,1)S(1)}, u32[]{:S(2)}, u32[]{:S(2)}) collective-permute-start(bf16[384,512]{1,0:T(8,128)(2,1)} %get-tuple-element.50.refs_1_), channel_id=1, source_target_pairs={{0,1},{1,2},{2,3},{3,0},{4,5},{5,6},{6,7},{7,4},{8,9},{9,10},{10,1... | collective-permute-start | bytes 1179656 | tf_op jit(solution)/shard_map/ppermute | solution.py:60
  69.1 23.4 %collective-permute-start.6 = (bf16[384,512]{1,0:T(8,128)(2,1)}, bf16[384,512]{1,0:T(8,128)(2,1)S(1)}, u32[]{:S(2)}, u32[]{:S(2)}) collective-permute-start(bf16[384,512]{1,0:T(8,128)(2,1)} %get-tuple-element.51.refs_0_.refs_8_), channel_id=1, source_target_pairs={{0,1},{1,2},{2,3},{3,0},{4,5},{5,6},{6,7},{7,4},{8,9},{9,10},{10,1... | collective-permute-start | bytes 1179656 | tf_op jit(solution)/shard_map/ppermute | solution.py:60
  76.0 20.1 %collective-permute-start.9 = (bf16[384,512]{1,0:T(8,128)(2,1)}, bf16[384,512]{1,0:T(8,128)(2,1)S(1)}, u32[]{:S(2)}, u32[]{:S(2)}) collective-permute-start(bf16[384,512]{1,0:T(8,128)(2,1)} %get-tuple-element.52.refs_1_.refs_9_), channel_id=1, source_target_pairs={{0,3},{1,0},{2,1},{3,2},{4,7},{5,4},{6,5},{7,6},{8,11},{9,8},{10,9... | collective-permute-start | bytes 1179656 | tf_op jit(solution)/shard_map/ppermute | solution.py:60
  76.0 24.8 %collective-permute-start.4 = (bf16[384,512]{1,0:T(8,128)(2,1)S(1)}, bf16[384,512]{1,0:T(8,128)(2,1)S(1)}, u32[]{:S(2)}, u32[]{:S(2)}) collective-permute-start(bf16[384,512]{1,0:T(8,128)(2,1)S(1)} %collective-permute-done.refs_2_), channel_id=1, source_target_pairs={{0,1},{1,2},{2,3},{3,0},{4,5},{5,6},{6,7},{7,4},{8,9},{9,10},{10,1... | collective-permute-start | bytes 1179656 | tf_op jit(solution)/shard_map/ppermute | solution.py:60
  84.5 16.9 %collective-permute-start.5 = (bf16[384,512]{1,0:T(8,128)(2,1)S(1)}, bf16[384,512]{1,0:T(8,128)(2,1)S(1)}, u32[]{:S(2)}, u32[]{:S(2)}) collective-permute-start(bf16[384,512]{1,0:T(8,128)(2,1)S(1)} %collective-permute-done.3.refs_5_), channel_id=1, source_target_pairs={{0,3},{1,0},{2,1},{3,2},{4,7},{5,4},{6,5},{7,6},{8,11},{9,8},{10,9... | collective-permute-start | bytes 1179656 | tf_op jit(solution)/shard_map/ppermute | solution.py:60
  84.5 28.8 %collective-permute-start.8 = (bf16[384,512]{1,0:T(8,128)(2,1)}, bf16[384,512]{1,0:T(8,128)(2,1)}, u32[]{:S(2)}, u32[]{:S(2)}) collective-permute-start(bf16[384,512]{1,0:T(8,128)(2,1)} %get-tuple-element.51.refs_0_.refs_8_), channel_id=1, source_target_pairs={{0,3},{1,0},{2,1},{3,2},{4,7},{5,4},{6,5},{7,6},{8,11},{9,8},{10,9... | collective-permute-start | bytes 1179656 | tf_op jit(solution)/shard_map/ppermute | solution.py:60
  92.5 20.7 %collective-permute-start.7 = (bf16[384,512]{1,0:T(8,128)(2,1)}, bf16[384,512]{1,0:T(8,128)(2,1)}, u32[]{:S(2)}, u32[]{:S(2)}) collective-permute-start(bf16[384,512]{1,0:T(8,128)(2,1)} %get-tuple-element.52.refs_1_.refs_9_), channel_id=1, source_target_pairs={{0,1},{1,2},{2,3},{3,0},{4,5},{5,6},{6,7},{7,4},{8,9},{9,10},{10,1... | collective-permute-start | bytes 1179656 | tf_op jit(solution)/shard_map/ppermute | solution.py:60
  96.1 19.4 %collective-permute-start.10 = (bf16[384,512]{1,0:T(8,128)(2,1)S(1)}, bf16[384,512]{1,0:T(8,128)(2,1)}, u32[]{:S(2)}, u32[]{:S(2)}) collective-permute-start(bf16[384,512]{1,0:T(8,128)(2,1)S(1)} %collective-permute-done.6.refs_2_.refs_10_), channel_id=1, source_target_pairs={{0,1},{1,2},{2,3},{3,0},{4,5},{5,6},{6,7},{7,4},{8,9},{9,10},{10,1... | collective-permute-start | bytes 1179656 | tf_op jit(solution)/shard_map/ppermute | solution.py:60
  100.8 15.5 %collective-permute-start.11 = (bf16[384,512]{1,0:T(8,128)(2,1)S(1)}, bf16[384,512]{1,0:T(8,128)(2,1)}, u32[]{:S(2)}, u32[]{:S(2)}) collective-permute-start(bf16[384,512]{1,0:T(8,128)(2,1)S(1)} %collective-permute-done.9.refs_5_.refs_13_), channel_id=1, source_target_pairs={{0,3},{1,0},{2,1},{3,2},{4,7},{5,4},{6,5},{7,6},{8,11},{9,8},{10,9... | collective-permute-start | bytes 1179656 | tf_op jit(solution)/shard_map/ppermute | solution.py:60
  109.0 32.0 %all-to-all-start.1 = ((bf16[8,192,512]{2,1,0:T(8,128)(2,1)}), bf16[8,192,512]{2,1,0:T(8,128)(2,1)S(1)}, u32[]{:S(2)}, u32[]{:S(2)}) async-start(bf16[8,192,512]{2,1,0:T(8,128)(2,1)} %broadcast_in_dim.2), calls=%async_computation.1 | async-start | bytes 3145728 | tf_op jit(solution)/shard_map/all_to_all | solution.py:64
  123.3 12.8 %collective-permute-start.12 = (bf16[384,512]{1,0:T(8,128)(2,1)}, bf16[384,512]{1,0:T(8,128)(2,1)S(1)}, u32[]{:S(2)}, u32[]{:S(2)}) collective-permute-start(bf16[384,512]{1,0:T(8,128)(2,1)} %get-tuple-element.61), channel_id=1, source_target_pairs={{0,1},{1,2},{2,3},{3,0},{4,5},{5,6},{6,7},{7,4},{8,9},{9,10},{10,1... | collective-permute-start | bytes 1179656 | tf_op jit(solution)/shard_map/ppermute | solution.py:60
  126.2 14.6 %collective-permute-start.16 = (bf16[384,512]{1,0:T(8,128)(2,1)}, bf16[384,512]{1,0:T(8,128)(2,1)S(1)}, u32[]{:S(2)}, u32[]{:S(2)}) collective-permute-start(bf16[384,512]{1,0:T(8,128)(2,1)} %get-tuple-element.63), channel_id=1, source_target_pairs={{0,3},{1,0},{2,1},{3,2},{4,7},{5,4},{6,5},{7,6},{8,11},{9,8},{10,9... | collective-permute-start | bytes 1179656 | tf_op jit(solution)/shard_map/ppermute | solution.py:60
  128.3 19.8 %collective-permute-start.15 = (bf16[384,512]{1,0:T(8,128)(2,1)S(1)}, bf16[384,512]{1,0:T(8,128)(2,1)S(1)}, u32[]{:S(2)}, u32[]{:S(2)}) collective-permute-start(bf16[384,512]{1,0:T(8,128)(2,1)S(1)} %slice.14), channel_id=1, source_target_pairs={{0,3},{1,0},{2,1},{3,2},{4,7},{5,4},{6,5},{7,6},{8,11},{9,8},{10,9... | collective-permute-start | bytes 1179656 | tf_op jit(solution)/shard_map/ppermute | solution.py:60
  128.4 19.7 %collective-permute-start.14 = (bf16[384,512]{1,0:T(8,128)(2,1)S(1)}, bf16[384,512]{1,0:T(8,128)(2,1)}, u32[]{:S(2)}, u32[]{:S(2)}) collective-permute-start(bf16[384,512]{1,0:T(8,128)(2,1)S(1)} %slice.13), channel_id=1, source_target_pairs={{0,1},{1,2},{2,3},{3,0},{4,5},{5,6},{6,7},{7,4},{8,9},{9,10},{10,1... | collective-permute-start | bytes 1179656 | tf_op jit(solution)/shard_map/ppermute | solution.py:60
  156.3 30.7 %all-to-all-start.2 = ((bf16[64,24,256]{2,1,0:T(8,128)(2,1)}), bf16[64,24,256]{2,1,0:T(8,128)(2,1)S(1)}, u32[]{:S(2)}, u32[]{:S(2)}) async-start(bf16[64,24,256]{2,1,0:T(8,128)(2,1)} %bitcast.19), calls=%async_computation.2 | async-start | bytes 1572864 | tf_op jit(solution)/shard_map/all_to_all | solution.py:64
  190.7 14.3 %collective-permute-start.23 = (bf16[192,512]{1,0:T(8,128)(2,1)}, bf16[192,512]{1,0:T(8,128)(2,1)S(1)}, u32[]{:S(2)}, u32[]{:S(2)}) collective-permute-start(bf16[192,512]{1,0:T(8,128)(2,1)} %get-tuple-element.73.p0), channel_id=1, source_target_pairs={{0,2},{1,3},{2,0},{3,1},{4,6},{5,7},{6,4},{7,5},{8,10},{9,11},{10,... | collective-permute-start | bytes 589832 | tf_op jit(solution)/shard_map/ppermute | solution.py:60
  190.7 14.3 %collective-permute-start.22 = (bf16[192,512]{1,0:T(8,128)(2,1)}, bf16[192,512]{1,0:T(8,128)(2,1)S(1)}, u32[]{:S(2)}, u32[]{:S(2)}) collective-permute-start(bf16[192,512]{1,0:T(8,128)(2,1)} %get-tuple-element.73.p0), channel_id=1, source_target_pairs={{0,3},{1,0},{2,1},{3,2},{4,7},{5,4},{6,5},{7,6},{8,11},{9,8},{10,9... | collective-permute-start | bytes 589832 | tf_op jit(solution)/shard_map/ppermute | solution.py:60
  191.9 13.2 %collective-permute-start.21 = (bf16[192,512]{1,0:T(8,128)(2,1)}, bf16[192,512]{1,0:T(8,128)(2,1)S(1)}, u32[]{:S(2)}, u32[]{:S(2)}) collective-permute-start(bf16[192,512]{1,0:T(8,128)(2,1)} %get-tuple-element.73.p0), channel_id=1, source_target_pairs={{0,1},{1,2},{2,3},{3,0},{4,5},{5,6},{6,7},{7,4},{8,9},{9,10},{10,1... | collective-permute-start | bytes 589832 | tf_op jit(solution)/shard_map/ppermute | solution.py:60
  210.5 22.2 %all-to-all-start.5 = ((f32[64,8,128]{2,1,0:T(8,128)}), f32[64,8,128]{2,1,0:T(8,128)S(1)}, u32[]{:S(2)}, u32[]{:S(2)}) async-start(f32[64,8,128]{2,1,0:T(8,128)} %bitcast.22), calls=%async_computation.5 | async-start | bytes 524288 | tf_op jit(solution)/shard_map/all_to_all | solution.py:64
  232.7 19.0 %all-to-all-start.4 = ((bf16[8,32,512]{2,1,0:T(8,128)(2,1)}), bf16[8,32,512]{2,1,0:T(8,128)(2,1)S(1)}, u32[]{:S(2)}, u32[]{:S(2)}) async-start(bf16[8,32,512]{2,1,0:T(8,128)(2,1)} %bitcast.21), calls=%async_computation.4 | async-start | bytes 524288 | tf_op jit(solution)/shard_map/all_to_all | solution.py:64
  (29 other events, 264.4 us)

commit v2 on v1

--- a/solution.py
+++ b/solution.py
@@ -19,8 +19,13 @@
 EXPERTS = 64
 CAP = 12
 BLOCK = 2 * CAP
-ROWS = EXPERTS * CAP
+SLOTS = EXPERTS * BLOCK
+ROWS = 512
 HALF = ROWS // 2
+MORE = EXPERTS * CAP - ROWS
+UNUSED = 256.0
+WIDE = 384
+PACKED = 4 * 2 * WIDTH + 3 * 256 + WIDTH
 GROUP = 8 * BLOCK
 GROUPS = EXPERTS * BLOCK // GROUP
 HID = 256
@@ -42,17 +47,46 @@
     return jax.ShapeDtypeStruct(dims, dtype)
 
 
+class Near:
+    def __init__(self, value):
+        self.value = value
+
+
+def size(a):
+    return a.size * a.dtype.itemsize
+
+
 def local(kernel, name, outs, flops, *args, scratch=(), smem=0):
-    moved = sum(a.size * a.dtype.itemsize for a in (*args, *jax.tree.leaves(outs)))
-    return pl.pallas_call(
+    def unwrapped(a):
+        return a.value if isinstance(a, Near) else a
+
+    def operand(n, a):
+        if isinstance(a, Near):
+            return pltpu.with_memory_space_constraint(a.value, pltpu.VMEM)
+        if n < smem or a.ndim < 2:
+            return a
+        return pltpu.with_memory_space_constraint(a, pltpu.HBM)
+
+    def result(o):
+        if isinstance(o, Near):
+            return pltpu.VMEM(o.value.shape, o.value.dtype)
+        return pltpu.HBM(o.shape, o.dtype)
+
+    single = not isinstance(outs, tuple)
+    every = (*args, *((outs,) if single else outs))
+    staged = sum(size(a) for a in every if not isinstance(a, Near))
+    moved = sum(size(unwrapped(a)) for a in every)
+    got = pl.pallas_call(
         kernel,
         name=name,
-        out_shape=outs,
+        out_shape=result(outs) if single else tuple(result(o) for o in outs),
         in_specs=[SMEM] * smem + [VMEM] * (len(args) - smem),
-        out_specs=jax.tree.map(lambda _: VMEM, outs),
+        out_specs=VMEM if single else (VMEM,) * len(outs),
         scratch_shapes=list(scratch),
+        compiler_params=pltpu.CompilerParams(vmem_limit_bytes=staged + (10 << 20)),
         cost_estimate=pl.CostEstimate(flops=int(flops), bytes_accessed=moved, transcendentals=0),
-    )(*args)
+    )(*[operand(n, a) for n, a in enumerate(args)])
+    return got
 
 
 def shift(value, axis, by):
@@ -96,9 +130,12 @@
     mixed = mixed_ref[...]
     d_out = d_out_ref[...]
 
-    def pack(g):
+    def pack(g, carry):
         at = lax.broadcasted_iota(i32, (GROUP, TOK), 0) + g * GROUP
-        to_mix = one_hot((slot[0] == at) | (slot[1] == at))
+        taken = (slot[0] == at) | (slot[1] == at)
+        to_mix = one_hot(taken)
+        empty = jnp.sum(jnp.where(taken, 1.0, 0.0), axis=1, keepdims=True) < 0.5
+        empty &= (lax.broadcasted_iota(i32, (GROUP, 1), 0) % BLOCK) < CAP
         first, second = (slot[0] + CAP == at, slot[1] + CAP == at)
         to_cot = one_hot(first | second)
         scale = jnp.sum(
@@ -106,43 +143,50 @@
             axis=1,
             keepdims=True,
         )
-        value = dot(to_mix, mixed) + dot(to_cot, d_out) * scale
+        value = dot(to_mix, mixed) + dot(to_cot, d_out) * scale + jnp.where(empty, UNUSED, 0.0)
         send_ref[pl.ds(pl.multiple_of(g * GROUP, GROUP), GROUP), :] = value.astype(BF16)
-
-    def two(n, carry):
-        pack(2 * n)
-        pack(2 * n + 1)
         return carry
 
-    lax.fori_loop(0, GROUPS // 2, two, 0)
-
-
-def sort_matrix():
-    matrix = np.zeros((GROUP, GROUP), np.float32)
-    for j in range(8):
-        for r in range(CAP):
-            matrix[j * CAP + r, j * BLOCK + r] = 1
-            matrix[GROUP // 2 + j * CAP + r, j * BLOCK + CAP + r] = 1
-    return jnp.asarray(matrix, BF16)
-
-
-def spread_matrix():
-    matrix = np.zeros((GROUP, GROUP // 2), np.float32)
-    for j in range(8):
-        for r in range(BLOCK):
-            matrix[j * BLOCK + r, j * CAP + r % CAP] = 1
-    return jnp.asarray(matrix, BF16)
-
-
-def sort_kernel(got_ref, order_ref, mix_a, mix_b, cot_a, cot_b):
-    order = order_ref[...]
-    half = GROUP // 2
-    for g in range(GROUPS):
-        out = dot(order, got_ref[g * GROUP : (g + 1) * GROUP, :]).astype(BF16)
-        at = (g % (GROUPS // 2)) * half
-        mix, cot = (mix_a, cot_a) if g < GROUPS // 2 else (mix_b, cot_b)
-        mix[at : at + half, :] = out[:half]
-        cot[at : at + half, :] = out[half:]
+    lax.fori_loop(0, GROUPS, pack, 0)
+
+
+def sort_kernel(got_ref, rows_a, rows_b, place_ref, total_ref):
+    i32 = jnp.int32
+    before = lax.broadcasted_iota(i32, (WIDE, WIDE), 0)
+    line = lax.broadcasted_iota(i32, (WIDE, WIDE), 1)
+    slot = line - jnp.where(line % BLOCK >= CAP, CAP, 0)
+    earlier, same = (one_hot(before < slot), one_hot(before == slot))
+    first = (lax.broadcasted_iota(i32, (WIDE, 128), 0) % BLOCK) < CAP
+    so_far = jnp.zeros((1, 128), F32)
+    for g in range(SLOTS // WIDE):
+        lines = slice(g * WIDE, (g + 1) * WIDE)
+        used = one_hot(first & (got_ref[lines, :128].astype(F32) < UNUSED / 2))
+        rank = dot_at(used, earlier)[0:1, :] + so_far[:, 0:1]
+        held = dot_at(used, same)[0:1, :] > 0.5
+        place_ref[:, lines] = jnp.where(held, rank, -1.0).astype(i32)
+        so_far = so_far + jnp.sum(used.astype(F32), axis=0, keepdims=True)
+    total_ref[...] = jnp.broadcast_to(so_far, (8, 128)).astype(i32)
+    for n, rows in enumerate((rows_a, rows_b)):
+        packed_rows(got_ref, place_ref, n * HALF, rows.at[:HALF], rows.at[HALF:])
+
+
+def packed_rows(got_ref, place_ref, start, mix_ref, cot_ref):
+    line = lax.broadcasted_iota(jnp.int32, (1, SLOTS), 1) % BLOCK
+    place = place_ref[...]
+    places = (jnp.where(line < CAP, place, -1), jnp.where(line < CAP, -1, place))
+
+    def step(n, carry):
+        row = lax.broadcasted_iota(jnp.int32, (128, SLOTS), 0) + (start + n * 128)
+        rows = pl.ds(pl.multiple_of(n * 128, 128), 128)
+        for wanted, out_ref in zip(places, (mix_ref, cot_ref)):
+            out_ref[rows, :] = dot(one_hot(wanted == row), got_ref[...]).astype(BF16)
+        return carry
+
+    lax.fori_loop(0, mix_ref.shape[0] // 128, step, 0)
+
+
+def sort_more_kernel(got_ref, place_ref, mix_ref, cot_ref):
+    packed_rows(got_ref, place_ref, ROWS, mix_ref, cot_ref)
 
 
 def block_of(me_ref, step):
@@ -152,42 +196,47 @@
 STEPS = (0, 3, 1, 2)
 
 
-def expert_up_kernel(me_ref, *refs):
-    pieces, (gate_ref, up_ref), (hidden_ref, silu_ref, slope_ref) = refs[:8], refs[8:10], refs[10:]
+def hidden_terms(me_ref, refs, turns, gate_ref, up_ref, down_ref, h):
+    sums = None
+    for p, turn in enumerate(turns):
+        piece = refs[2 * p + h]
+        at = block_of(me_ref, turn)
+        mix = piece[:HALF, :]
+        terms = (
+            dot(mix, gate_ref[pl.ds(at, WIDTH), :]),
+            dot(mix, up_ref[pl.ds(at, WIDTH), :]),
+            dot_bt(piece[HALF:, :], down_ref[:, pl.ds(at, WIDTH)]),
+        )
+        sums = terms if sums is None else tuple(a + b for a, b in zip(sums, terms))
+    return sums
+
+
+def expert_near_kernel(me_ref, *refs):
+    gate_ref, up_ref, down_ref = refs[6:9]
     for h in range(2):
-        up_pre = linear = None
-        for p in range(4):
-            piece = pieces[2 * p + h][...]
-            at = block_of(me_ref, STEPS[p])
-            one = dot(piece, gate_ref[pl.ds(at, WIDTH), :])
-            two = dot(piece, up_ref[pl.ds(at, WIDTH), :])
-            up_pre = one if up_pre is None else up_pre + one
-            linear = two if linear is None else linear + two
+        rows = slice(h * HALF, (h + 1) * HALF)
+        terms = hidden_terms(me_ref, refs[:6], STEPS[:3], gate_ref, up_ref, down_ref, h)
+        for term, out in zip(terms, refs[9:]):
+            out[rows, :] = term
+
+
+def expert_far_kernel(me_ref, *refs):
+    gate_ref, up_ref, down_ref = refs[2:5]
+    near_refs = refs[5:8]
+    hidden_ref, d_up_ref, d_linear_ref, far_a, far_b, left_ref, right_ref, own_ref = refs[8:]
+    for h in range(2):
+        rows = slice(h * HALF, (h + 1) * HALF)
+        terms = hidden_terms(me_ref, refs[:2], STEPS[3:], gate_ref, up_ref, down_ref, h)
+        up_pre, linear, d_hidden = (a[rows, :] + b for a, b in zip(near_refs, terms))
         sigmoid = jax.nn.sigmoid(up_pre)
         silu = up_pre * sigmoid
-        rows = slice(h * HALF, (h + 1) * HALF)
         hidden_ref[rows, :] = (silu * linear).astype(BF16)
-        silu_ref[rows, :] = silu
-        slope_ref[rows, :] = linear * sigmoid * (1.0 + up_pre * (1.0 - sigmoid))
-
-
-def expert_down_kernel(me_ref, *refs):
-    pieces = refs[:8]
-    gate_ref, up_ref, down_ref, silu_ref, slope_ref = refs[8:13]
-    d_up_ref, d_linear_ref, far_a, far_b, left_ref, right_ref, own_ref = refs[13:]
-    ups, linears = [], []
-    for h in range(2):
-        rows = slice(h * HALF, (h + 1) * HALF)
-        d_hidden = None
-        for p in range(4):
-            at = block_of(me_ref, STEPS[p])
-            one = dot_bt(pieces[2 * p + h][...], down_ref[:, pl.ds(at, WIDTH)])
-            d_hidden = one if d_hidden is None else d_hidden + one
-        d_linear_ref[rows, :] = (d_hidden * silu_ref[rows, :]).astype(BF16)
-        d_up_ref[rows, :] = (d_hidden * slope_ref[rows, :]).astype(BF16)
-
-    def part(rows, step):
-        at = block_of(me_ref, step)
+        d_linear_ref[rows, :] = (d_hidden * silu).astype(BF16)
+        slope = linear * sigmoid * (1.0 + up_pre * (1.0 - sigmoid))
+        d_up_ref[rows, :] = (d_hidden * slope).astype(BF16)
+
+    def part(rows, turn):
+        at = block_of(me_ref, turn)
         return (
             dot_bt(d_up_ref[rows, :], gate_ref[pl.ds(at, WIDTH), :])
             + dot_bt(d_linear_ref[rows, :], up_ref[pl.ds(at, WIDTH), :])
@@ -202,49 +251,82 @@
         own_ref[rows, :] = part(rows, 0)
 
 
-def expert_grad_kernel(me_ref, *refs):
-    mixes, cots = refs[:8], refs[8:16]
-    d_up_ref, d_linear_ref, hidden_ref = refs[16:19]
-    grad_gate_ref, grad_up_ref, grad_down_ref = refs[19:]
+def expert_grad_kernel(me_ref, total_ref, *refs):
+    pieces = refs[:8]
+    d_up_ref, d_linear_ref, hidden_ref, more_ref = refs[8:12]
+    grad_gate_ref, grad_up_ref, grad_down_ref = refs[12:]
     top, low = (slice(0, HALF), slice(HALF, ROWS))
     for p in range(4):
-        mix = (mixes[2 * p], mixes[2 * p + 1])
-        cot = (cots[2 * p], cots[2 * p + 1])
-
-        def step(n, carry):
+
+        def step(n, carry, halves=(pieces[2 * p], pieces[2 * p + 1]), p=p):
             cols = pl.ds(pl.multiple_of(n * 128, 128), 128)
             at = pl.ds(pl.multiple_of(block_of(me_ref, STEPS[p]) + n * 128, 128), 128)
-            mix_a, mix_b = (mix[0][:, cols], mix[1][:, cols])
+            mix_a, mix_b = (half[:HALF, cols] for half in halves)
+            cot_a, cot_b = (half[HALF:, cols] for half in halves)
             grad_gate_ref[0, at, :] = dot_at(mix_a, d_up_ref[top, :]) + dot_at(
                 mix_b, d_up_ref[low, :]
             )
             grad_up_ref[0, at, :] = dot_at(mix_a, d_linear_ref[top, :]) + dot_at(
                 mix_b, d_linear_ref[low, :]
             )
-            grad_down_ref[0, :, at] = dot_at(hidden_ref[top, :], cot[0][:, cols]) + dot_at(
-                hidden_ref[low, :], cot[1][:, cols]
+            grad_down_ref[0, :, at] = dot_at(hidden_ref[top, :], cot_a) + dot_at(
+                hidden_ref[low, :], cot_b
             )
             return carry
 
         lax.fori_loop(0, 4, step, 0)
 
-
-def spread_kernel(own_ref, la_ref, lb_ref, ra_ref, rb_ref, order_ref, out_ref):
-    order = order_ref[...]
-    half = GROUP // 2
-    first = (lax.broadcasted_iota(jnp.int32, (GROUP, 1), 0) % BLOCK) < CAP
-    for g in range(GROUPS):
-        at = (g % (GROUPS // 2)) * half
-        from_left, from_right = (la_ref, ra_ref) if g < GROUPS // 2 else (lb_ref, rb_ref)
-        total = (
-            own_ref[g * half : (g + 1) * half, :].astype(F32)
-            + from_left[at : at + half, :].astype(F32)
-            + from_right[at : at + half, :].astype(F32)
-        ).astype(BF16)
-        wide = dot(order, total)
-        out_ref[g * GROUP : (g + 1) * GROUP, :] = jnp.where(
-            first, wide[:, : WIDTH // 2], wide[:, WIDTH // 2 :]
-        ).astype(BF16)
+    @pl.when(total_ref[0] > ROWS)
+    def _():
+        base = 8 * WIDTH
+        d_up, d_linear, hidden = (more_ref[:, base + 256 * n : base + 256 * (n + 1)] for n in range(3))
+
+        def step(n, carry):
+            at = pl.ds(pl.multiple_of(n * 128, 128), 128)
+            mix = more_ref[:, at]
+            cot = more_ref[:, pl.ds(pl.multiple_of(n * 128 + 4 * WIDTH, 128), 128)]
+            grad_gate_ref[0, at, :] += dot_at(mix, d_up)
+            grad_up_ref[0, at, :] += dot_at(mix, d_linear)
+            grad_down_ref[0, :, at] += dot_at(hidden, cot)
+            return carry
+
+        lax.fori_loop(0, 4 * WIDTH // 128, step, 0)
+
+
+def spread_kernel(
+    total_ref, own_ref, la_ref, lb_ref, ra_ref, rb_ref, place_ref, more_ref, out_ref
+):
+    rows = [
+        (own.astype(F32) + from_left[...].astype(F32) + from_right[...].astype(F32)).astype(BF16)
+        for own, from_left, from_right in (
+            (own_ref[:HALF, :], la_ref, ra_ref),
+            (own_ref[HALF:, :], lb_ref, rb_ref),
+        )
+    ]
+    first = (lax.broadcasted_iota(jnp.int32, (WIDE, 1), 0) % BLOCK) < CAP
+
+    def spread(values, start, lines):
+        row = lax.broadcasted_iota(jnp.int32, (values.shape[0], WIDE), 0) + start
+        wide = dot_at(one_hot(place_ref[:, lines] == row), values)
+        return jnp.where(first, wide[:, : WIDTH // 2], wide[:, WIDTH // 2 :])
+
+    def step(g, carry):
+        lines = pl.ds(pl.multiple_of(g * WIDE, WIDE), WIDE)
+        value = spread(rows[0], 0, lines) + spread(rows[1], HALF, lines)
+        out_ref[lines, :] = value.astype(BF16)
+        return carry
+
+    lax.fori_loop(0, SLOTS // WIDE, step, 0)
+
+    @pl.when(total_ref[0] > ROWS)
+    def _():
+        def add(g, carry):
+            lines = pl.ds(pl.multiple_of(g * WIDE, WIDE), WIDE)
+            value = spread(more_ref[:, PACKED - WIDTH :], ROWS, lines)
+            out_ref[lines, :] = (out_ref[lines, :].astype(F32) + value).astype(BF16)
+            return carry
+
+        lax.fori_loop(0, SLOTS // WIDE, add, 0)
 
 
 def combine_kernel(back_ref, slots_ref, d_out_ref, out_ref, send_ref):
@@ -330,7 +412,9 @@
         t = jnp.tanh(c0 * (x + 0.044715 * x * x * x))
         act = 0.5 * x * (1.0 + t)
         deriv = 0.5 * (1.0 + t) + 0.5 * x * (1.0 - t * t) * (c0 * (1.0 + 0.134145 * x * x))
-        merged_ref[rows, :] = (act * states).astype(BF16)
+        merged = (act * states).astype(BF16)
+        for k in range(8):
+            merged_ref[k, rows, :] = merged
         act_ref[rows, :] = act
         slope_ref[rows, :] = states * deriv
         decay_ref[rows, :] = decay
@@ -449,6 +533,37 @@
     left_b, right_a = (shift(b, "tp", 1), shift(a, "tp", -1))
     far_a, far_b = (shift(left_a, "tp", 1), shift(right_b, "tp", -1))
     return (a, b, left_a, left_b, right_a, right_b, far_a, far_b)
+
+
+def reduced(far_a, far_b, left, right):
+    half = far_a.shape[0]
+
+    def add(u, v):
+        return (u.astype(F32) + v.astype(F32)).astype(BF16)
+
+    over_a, over_b = (shift(far_a, "tp", 1), shift(far_b, "tp", -1))
+    right_b, left_a = (shift(right[half:], "tp", 1), shift(left[:half], "tp", -1))
+    right_a = shift(add(right[:half], over_a), "tp", 1)
+    left_b = shift(add(left[half:], over_b), "tp", -1)
+    return right_a, right_b, left_a, left_b, over_a
+
+
+def overflow(gate2, up2, down2, got, place):
+    full = shape((MORE, WIDTH), BF16)
+    mix, cot = local(sort_more_kernel, "sort_more", (full, full), 1e9, got, place)
+    both = exchange(jnp.broadcast_to(jnp.stack([mix, cot])[None], (4, 2, MORE, WIDTH)), "tp")
+    mix, cot = (jnp.moveaxis(both[:, n], 0, 1).reshape(MORE, -1) for n in range(2))
+    up_pre, linear = (dot(mix, gate2), dot(mix, up2))
+    sigmoid = jax.nn.sigmoid(up_pre)
+    silu = up_pre * sigmoid
+    hidden = (silu * linear).astype(BF16)
+    d_hidden = dot_bt(cot, down2)
+    d_linear = (d_hidden * silu).astype(BF16)
+    d_up = (d_hidden * (linear * sigmoid * (1.0 + up_pre * (1.0 - sigmoid)))).astype(BF16)
+    part = (dot_bt(d_up, gate2) + dot_bt(d_linear, up2)).astype(BF16)
+    parts = exchange(jnp.moveaxis(part.reshape(MORE, 4, WIDTH), 1, 0), "tp")
+    total = jnp.sum(parts.astype(F32), axis=0).astype(BF16)
+    return jnp.concatenate([mix, cot, d_up, d_linear, hidden, total], axis=1)
 
 
 def collected(value):
@@ -496,7 +611,7 @@
     merged, act, slope, decay, kr, ki, kd = local(
         forward_kernel,
         "forward",
-        (shape((TOK, WIDTH), BF16),) + (f_like,) * 6,
+        (shape((8, TOK, WIDTH), BF16),) + (f_like,) * 6,
         6e9,
         after(conv_out, send),
         gate_in,
@@ -509,49 +624,67 @@
     )
     got = after(got, merged)
     piece = shape((HALF, WIDTH), BF16)
-    mix_a, mix_b, cot_a, cot_b = local(
-        sort_kernel, "sort", (piece,) * 4, 1e9, got, sort_matrix()
-    )
-    mixes = gathered(mix_a, mix_b)
-    cots = gathered(cot_a, cot_b)
+    full = shape((ROWS, WIDTH), BF16)
+    rows_a, rows_b, place, total = local(
+        sort_kernel,
+        "sort",
+        (Near(full), Near(full), shape((1, SLOTS), jnp.int32), shape((8, 128), jnp.int32)),
+        2e9,
+        Near(got),
+    )
+    total = total[0, :1]
+    pieces = gathered(rows_a, rows_b)
     gate2, up2, down2 = (w_gate[0], w_up[0], w_down[0])
     hid = shape((ROWS, HID), BF16)
     hid_f = shape((ROWS, HID), F32)
-    full = shape((ROWS, WIDTH), BF16)
-    hidden, silu, up_slope = local(
-        expert_up_kernel, "expert_up", (hid, hid_f, hid_f), 2 * unit, me, *mixes, gate2, up2, smem=1
-    )
-    merged_x = exchange(jnp.broadcast_to(after(merged, hidden)[None], (8, TOK, WIDTH)), XC)
-    d_up, d_linear, far_a, far_b, left, right, own = local(
-        expert_down_kernel,
-        "expert_down",
-        (hid, hid, piece, piece, full, full, full),
-        3 * unit,
+    near = local(
+        expert_near_kernel,
+        "expert_near",
+        (hid_f,) * 3,
+        2 * unit,
         me,
-        *cots,
+        *map(Near, pieces[:6]),
         gate2,
         up2,
         down2,
-        silu,
-        up_slope,
         smem=1,
     )
-    over_a, over_b = (shift(far_a, "tp", 1), shift(far_b, "tp", -1))
-    right_b, left_a = (shift(right[HALF:], "tp", 1), shift(left[:HALF], "tp", -1))
-    add = lambda u, v: (u.astype(F32) + v.astype(F32)).astype(BF16)
-    right_a = shift(add(right[:HALF], over_a), "tp", 1)
-    left_b = shift(add(left[HALF:], over_b), "tp", -1)
+    merged_x = exchange(after(merged, pieces[3]), XC)
+    hidden, d_up, d_linear, far_a, far_b, left, right, own = local(
+        expert_far_kernel,
+        "expert_far",
+        (hid, hid, hid, *map(Near, (piece, piece, full, full)), full),
+        3 * unit,
+        me,
+        *map(Near, pieces[6:]),
+        gate2,
+        up2,
+        down2,
+        *near,
+        smem=1,
+    )
+    right_a, right_b, left_a, left_b, over_a = reduced(far_a, far_b, left, right)
+    more = lax.cond(
+        total[0] > ROWS,
+        lambda *both: overflow(gate2, up2, down2, *both),
+        lambda *_: jnp.zeros((MORE, PACKED), BF16),
+        after(got, pieces[2]),
+        place,
+    )
     returned = local(
         spread_kernel,
         "spread",
         shape((EXPERTS * BLOCK, WIDTH // 2), BF16),
-        1e9,
+        2e9,
+        total,
         after(own, merged_x),
-        right_a,
-        right_b,
-        left_a,
-        left_b,
-        spread_matrix(),
+        Near(right_a),
+        Near(right_b),
+        Near(left_a),
+        Near(left_b),
+        place,
+        more,
+        smem=1,
     )
     back = exchange(returned, SP)
     grads = local(
@@ -560,20 +693,21 @@
         (shape((1, 2048, HID), F32), shape((1, 2048, HID), F32), shape((1, HID, 2048), F32)),
         3 * unit,
         me,
-        *mixes,
-        *cots,
+        total,
+        *pieces,
         after(d_up, returned),
         d_linear,
         hidden,
-        smem=1,
+        more,
+        smem=2,
     )
     back = after(back, grads)
     d_columns, crossing = local(
         combine_kernel,
         "combine",
-        (shape((TOK, WIDTH), BF16), shape((8, TOK // 2, 128), BF16)),
+        (Near(shape((TOK, WIDTH), BF16)), Near(shape((8, TOK // 2, 128), BF16))),
         1e9,
-        back,
+        Near(back),
         slots,
         d_out,
     )
@@ -583,11 +717,10 @@
     grad_gate, local_grad, products, carries = local(
         reverse_kernel,
         "reverse",
-        (shape((TOK, WIDTH), BF16), f_like, f_like, shape((EXPERTS * 8, 128), F32)),
+        (shape((TOK, WIDTH), BF16), Near(f_like), Near(f_like), shape((EXPERTS * 8, 128), F32)),
         4e9,
         me,
-        after(pieces[0], crossed),
-        *pieces[1:],
+        *map(Near, (after(pieces[0], crossed), *pieces[1:])),
         w_out,
         act,
         slope,
@@ -602,8 +735,8 @@
         shape((256, WIDTH), BF16),
         1e9,
         me,
-        *columns,
-        merged_x,
+        *map(Near, columns),
+        Near(merged_x),
         smem=1,
     )
     parts = exchange(grad_part, "z")
@@ -614,9 +747,9 @@
         shape((TOK, WIDTH), BF16),
         2e9,
         here,
-        carried,
-        local_grad,
-        products,
+        Near(carried),
+        Near(local_grad),
+        Near(products),
         kr,
         ki,
         kd,

time: 253 us -> 291 us (1.15); the launches traced: 252 us -> 285 us
  starting transfers between devices: 68.5 us -> 120 us
  waiting for transfers between devices: 104 us -> 92.8 us
  local copies, waits for them, and re-layouts: 10.5 us -> 5.26 us
    all_to_all x5, starting transfers between devices: 35.6 us -> 96.4 us  [exchange(): return lax.all_to_all(value, axes, 0, 0, tiled=True)]
    ppermute x24 -> x18, waiting for transfers between devices: 51.4 us -> 39.2 us  [shift(): return lax.ppermute(value, axis, [(i, (i + by) % n) for i in range(n)])]
    ppermute x24 -> x18, starting transfers between devices: 32.9 us -> 24 us  [shift(): return lax.ppermute(value, axis, [(i, (i + by) % n) for i in range(n)])]
    unnamed x49 -> x19, local copies, waits for them, and re-layouts: 6.41 us -> 1.48 us
  transfers between devices with their start and end apart: 29 -> 23, of which waited for: 15 -> 11; matrix products, arithmetic and copies ran while one was open for 2% -> 2% of each run, Pallas kernels for 15% -> 12%
where the time goes in v2:
time: 291 us; the launch traced here: 285 us
  starting transfers between devices  120 us (41%)
  waiting for transfers between devices  92.8 us (32%)
  Pallas kernels  52.7 us (18%)
  blocking collectives  10.9 us (4%)
  local copies, waits for them, and re-layouts  5.26 us (2%)
    all_to_all x5, starting transfers between devices, exchange(): return lax.all_to_all(value, axes, 0, 0, tiled=True)  96.4 us
    all_to_all x5, waiting for transfers between devices, exchange(): return lax.all_to_all(value, axes, 0, 0, tiled=True)  53.6 us
    pallas_call x11, Pallas kernels, local(): pl.pallas_call(kernel, name=name, out_shape=result(outs) if single else t...  52.7 us
    ppermute x18, waiting for transfers between devices, shift(): return lax.ppermute(value, axis, [(i, (i + by) % n) for i in range(n)])  39.2 us
    ppermute x18, starting transfers between devices, shift(): return lax.ppermute(value, axis, [(i, (i + by) % n) for i in range(n)])  24 us
    all_to_all x1, blocking collectives, exchange(): return lax.all_to_all(value, axes, 0, 0, tiled=True)  10.9 us
  transfers between devices with their start and end apart: 23, of which 11 were waited for; matrix products, arithmetic and copies ran while one was open for 2% of the time, Pallas kernels for 12%

profile of v2, /device:TPU:24, one launch (start us, length us, event | category | flops | bytes accessed | tf_op | source)
XLA Modules:
  0.0 284.9 jit_solution(662523119363089552)
XLA Ops:
  2.1 5.0 %route.1 = (bf16[1536,512]{1,0:T(8,128)(2,1)}, s32[192,2]{1,0:T(8,128)}) custom-call(s32[192,2]{1,0:T(8,128)} %copy.47.ids_ref, s32[2,192]{1,0:T(2,128)} %bitcast.73, f32[2,192]{1,0:T(2,128)} %bitcast.76, bf16[192,512]{1,0:T(8,128)(2,1)} %mixed_ref.1, bf16[192,512]{1,0:T(8,128)(2,1)} %d_out_ref.3), custom_call_target="tpu_custom_call" | custom-call | flops 1300000000 | bytes 1972224 | tf_op jit(solution)/shard_map/route/pallas_call | solution.py:79
  7.1 12.1 %all-to-all-start.2 = ((bf16[64,24,512]{2,1,0:T(8,128)(2,1)}), bf16[64,24,512]{2,1,0:T(8,128)(2,1)S(1)}, u32[]{:S(2)}, u32[]{:S(2)}) async-start(bf16[64,24,512]{2,1,0:T(8,128)(2,1)} %bitcast.64), calls=%async_computation.2 | async-start | bytes 3145728 | tf_op jit(solution)/shard_map/all_to_all | solution.py:98
  20.5 5.6 %forward.1 = (bf16[8,192,512]{2,1,0:T(8,128)(2,1)}, f32[192,512]{1,0:T(8,128)}, f32[192,512]{1,0:T(8,128)}, f32[192,512]{1,0:T(8,128)}, f32[192,512]{1,0:T(8,128...) custom-call(bf16[192,512]{1,0:T(8,128)(2,1)} %conv_ref, bf16[192,512]{1,0:T(8,128)(2,1)} %gate_ref.1, f32[1,512]{1,0:T(1,128)} %start_ref.1, ...), custom_call_target="tpu_custom_call" | custom-call | flops 6000000000 | bytes 4592384 | tf_op jit(solution)/shard_map/forward/pallas_call | solution.py:79
  26.2 33.1 %all-to-all-done.2 = bf16[64,24,512]{2,1,0:T(8,128)(2,1)S(1)} async-done(((bf16[64,24,512]{2,1,0:T(8,128)(2,1)}), bf16[64,24,512]{2,1,0:T(8,128)(2,1)S(1)}, u32[]{:S(2)}, u32[]{:S(2)}) %all-to-all-start.2) | async-done | bytes 1572896 | tf_op jit(solution)/shard_map/all_to_all | solution.py:98
  66.6 10.7 %collective-permute-done.refs_2_ = bf16[512,512]{1,0:T(8,128)(2,1)S(1)} collective-permute-done((bf16[512,512]{1,0:T(8,128)(2,1)S(1)}, bf16[512,512]{1,0:T(8,128)(2,1)S(1)}, u32[]{:S(2)}, u32[]{:S(2)}) %collective-permute-start) | collective-permute-done | bytes 524320 | tf_op jit(solution)/shard_map/ppermute | solution.py:94
  81.3 7.3 %collective-permute-done.1.refs_3_ = bf16[512,512]{1,0:T(8,128)(2,1)S(1)} collective-permute-done((bf16[512,512]{1,0:T(8,128)(2,1)S(1)}, bf16[512,512]{1,0:T(8,128)(2,1)S(1)}, u32[]{:S(2)}, u32[]{:S(2)}) %collective-permute-start.1) | collective-permute-done | bytes 524320 | tf_op jit(solution)/shard_map/ppermute | solution.py:94
  90.3 65.9 %all-to-all-start.3 = ((bf16[8,192,512]{2,1,0:T(8,128)(2,1)}), bf16[8,192,512]{2,1,0:T(8,128)(2,1)}, u32[]{:S(2)}, u32[]{:S(2)}) async-start(bf16[8,192,512]{2,1,0:T(8,128)(2,1)} %get-tuple-element.79), calls=%async_computation.3 | async-start | bytes 3145728 | tf_op jit(solution)/shard_map/all_to_all | solution.py:98
  156.2 4.3 %expert_near.1 = (f32[512,256]{1,0:T(8,128)}, f32[512,256]{1,0:T(8,128)}, f32[512,256]{1,0:T(8,128)}) custom-call(s32[1]{0:T(128)} %bitcast.13.me_ref, bf16[512,512]{1,0:T(8,128)(2,1)S(1)} %get-tuple-element.72.refs_0_, bf16[512,512]{1,0:T(8,128)(2,1)S(1)} %get-tuple-element.73.refs_1_, bf16[512,512]{1,0:T(8,128)(2,1)S(1)} %collective-permute-done.refs_2_, ...), custom_call_target="tpu_custom_call" | custom-call | flops 1073741824 | bytes 7864324 | tf_op jit(solution)/shard_map/expert_near/pallas_call | solution.py:79
  160.5 5.3 %expert_far.1 = (bf16[512,256]{1,0:T(8,128)(2,1)}, bf16[512,256]{1,0:T(8,128)(2,1)}, bf16[512,256]{1,0:T(8,128)(2,1)}, bf16[256,512]{1,0:T(8,128)(2,1)S(1)}, bf1...) custom-call(s32[1]{0:T(128)} %bitcast.13.me_ref, ...), custom_call_target="tpu_custom_call" | custom-call | flops 1610612736 | bytes 8650756 | tf_op jit(solution)/shard_map/expert_far/pallas_call | solution.py:79
  168.0 3.3 %collective-permute-start.8 = (bf16[256,512]{1,0:T(8,128)(2,1)S(1)}, bf16[256,512]{1,0:T(8,128)(2,1)S(1)}, u32[]{:S(2)}, u32[]{:S(2)}) collective-permute-start(bf16[256,512]{1,0:T(8,128)(2,1)S(1)} %slice.23), channel_id=1, source_target_pairs={{0,1},{1,2},{2,3},{3,0},{4,5},{5,6},{6,7},{7,4},{8,9},{9,10},{10,1... | collective-permute-start | bytes 786440 | tf_op jit(solution)/shard_map/ppermute | solution.py:94
  171.3 3.7 %collective-permute-done.6 = bf16[256,512]{1,0:T(8,128)(2,1)S(1)} collective-permute-done((bf16[256,512]{1,0:T(8,128)(2,1)S(1)}, bf16[256,512]{1,0:T(8,128)(2,1)S(1)}, u32[]{:S(2)}, u32[]{:S(2)}) %collective-permute-start.6) | collective-permute-done | bytes 262176 | tf_op jit(solution)/shard_map/ppermute | solution.py:94
  175.1 3.3 %collective-permute-start.7 = (bf16[256,512]{1,0:T(8,128)(2,1)S(1)}, bf16[256,512]{1,0:T(8,128)(2,1)S(1)}, u32[]{:S(2)}, u32[]{:S(2)}) collective-permute-start(bf16[256,512]{1,0:T(8,128)(2,1)S(1)} %add_convert_fusion.1), channel_id=1, source_target_pairs={{0,1},{1,2},{2,3},{3,0},{4,5},{5,6},{6,7},{7,4},{8,9},{9,10},{10,1... | collective-permute-start | bytes 786440 | tf_op jit(solution)/shard_map/ppermute | solution.py:94
  178.6 5.3 %collective-permute-done.9.ra_ref = bf16[256,512]{1,0:T(8,128)(2,1)S(1)} collective-permute-done((bf16[256,512]{1,0:T(8,128)(2,1)S(1)}, bf16[256,512]{1,0:T(8,128)(2,1)S(1)}, u32[]{:S(2)}, u32[]{:S(2)}) %collective-permute-start.9) | collective-permute-done | bytes 262176 | tf_op jit(solution)/shard_map/ppermute | solution.py:94
  188.8 5.5 %spread.1 = bf16[1536,256]{1,0:T(8,128)(2,1)} custom-call(s32[1]{0:T(128)} %bitcast.20.total_ref, bf16[512,512]{1,0:T(8,128)(2,1)} %get-tuple-element.80.own_ref, bf16[256,512]{1,0:T(8,128)(2,1)S(1)} %collective-permute-done.7.la_ref, bf16[256,512]{1,0:T(8,128)(2,1)S(1)} %collective-permute-done.8.lb_ref, ...), custom_call_target="tpu_custom_call" | custom-call | flops 2000000000 | bytes 5117956 | tf_op jit(solution)/shard_map/spread/pallas_call | solution.py:79
  194.3 6.8 %all-to-all-start.4 = ((bf16[64,24,256]{2,1,0:T(8,128)(2,1)}), bf16[64,24,256]{2,1,0:T(8,128)(2,1)S(1)}, u32[]{:S(2)}, u32[]{:S(2)}) async-start(bf16[64,24,256]{2,1,0:T(8,128)(2,1)} %bitcast.68), calls=%async_computation.4 | async-start | bytes 1572864 | tf_op jit(solution)/shard_map/all_to_all | solution.py:98
  201.1 12.1 %expert_grad.1 = (f32[1,2048,256]{2,1,0:T(8,128)}, f32[1,2048,256]{2,1,0:T(8,128)}, f32[1,256,2048]{2,1,0:T(8,128)}) custom-call(s32[1]{0:T(128)} %bitcast.13.me_ref, s32[1]{0:T(128)} %bitcast.20.total_ref, bf16[512,512]{1,0:T(8,128)(2,1)} %copy-done, bf16[512,512]{1,0:T(8,128)(2,1)} %copy-done.1, bf16[512,512]{1,0:T(8,128)(2,1)} %copy-done.2, ...), custom_call_target="tpu_custom_call" | custom-call | flops 1610612736 | bytes 14024712 | tf_op jit(solution)/shard_map/expert_grad/pallas_call | solution.py:79
  213.2 11.1 %all-to-all-done.4 = bf16[64,24,256]{2,1,0:T(8,128)(2,1)S(1)} async-done(((bf16[64,24,256]{2,1,0:T(8,128)(2,1)}), bf16[64,24,256]{2,1,0:T(8,128)(2,1)S(1)}, u32[]{:S(2)}, u32[]{:S(2)}) %all-to-all-start.4) | async-done | bytes 786464 | tf_op jit(solution)/shard_map/all_to_all | solution.py:98
  230.0 10.9 %all_to_all.63.p0 = bf16[8,96,128]{2,1,0:T(8,128)(2,1)S(1)} all-to-all(bf16[8,96,128]{2,1,0:T(8,128)(2,1)S(1)} %get-tuple-element.95), channel_id=1, replica_groups=mesh['z'=8,'x'=4,'c'=2,'tp'=4] {'x','c'}, dimensions={0} | all-to-all | bytes 393216 | tf_op jit(solution)/shard_map/all_to_all | solution.py:98
  240.8 4.0 %reverse.1 = (bf16[192,512]{1,0:T(8,128)(2,1)}, f32[192,512]{1,0:T(8,128)S(1)}, f32[192,512]{1,0:T(8,128)S(1)}, f32[512,128]{1,0:T(8,128)}) custom-call(s32[1]{0:T(128)} %bitcast.13.me_ref, bf16[192,512]{1,0:T(8,128)(2,1)S(1)} %get-tuple-element.97.p0, bf16[192,512]{1,0:T(8,128)(2,1)S(1)} %collective-permute-done.15.p1, ...), custom_call_target="tpu_custom_call" | custom-call | flops 4000000000 | bytes 5308420 | tf_op jit(solution)/shard_map/reverse/pallas_call | solution.py:79
  244.8 4.6 %all-to-all-start.7 = ((f32[64,8,128]{2,1,0:T(8,128)}), f32[64,8,128]{2,1,0:T(8,128)S(1)}, u32[]{:S(2)}, u32[]{:S(2)}) async-start(f32[64,8,128]{2,1,0:T(8,128)} %bitcast.70), calls=%async_computation.7 | async-start | bytes 524288 | tf_op jit(solution)/shard_map/all_to_all | solution.py:98
  251.5 3.2 %collective-permute-start.12 = (bf16[8,96,128]{2,1,0:T(8,128)(2,1)S(1)}, bf16[8,96,128]{2,1,0:T(8,128)(2,1)S(1)}, u32[]{:S(2)}, u32[]{:S(2)}) collective-permute-start(bf16[8,96,128]{2,1,0:T(8,128)(2,1)S(1)} %all_to_all.63.p0), channel_id=1, source_target_pairs={{0,1},{1,2},{2,3},{3,0},{4,5},{5,6},{6,7},{7,4},{8,9},{9,10},{10,1... | collective-permute-start | bytes 589832 | tf_op jit(solution)/shard_map/ppermute | solution.py:94
  254.7 4.1 %collective-permute-done.14.p3 = bf16[8,96,128]{2,1,0:T(8,128)(2,1)S(1)} collective-permute-done((bf16[8,96,128]{2,1,0:T(8,128)(2,1)S(1)}, bf16[8,96,128]{2,1,0:T(8,128)(2,1)S(1)}, u32[]{:S(2)}, u32[]{:S(2)}) %collective-permute-start.14) | collective-permute-done | bytes 196640 | tf_op jit(solution)/shard_map/ppermute | solution.py:94
  265.2 7.0 %all-to-all-start.6 = ((bf16[8,32,512]{2,1,0:T(8,128)(2,1)}), bf16[8,32,512]{2,1,0:T(8,128)(2,1)S(1)}, u32[]{:S(2)}, u32[]{:S(2)}) async-start(bf16[8,32,512]{2,1,0:T(8,128)(2,1)} %bitcast.69), calls=%async_computation.6 | async-start | bytes 524288 | tf_op jit(solution)/shard_map/all_to_all | solution.py:98
  274.9 9.4 %all-to-all-done.6 = bf16[8,32,512]{2,1,0:T(8,128)(2,1)S(1)} async-done(((bf16[8,32,512]{2,1,0:T(8,128)(2,1)}), bf16[8,32,512]{2,1,0:T(8,128)(2,1)S(1)}, u32[]{:S(2)}, u32[]{:S(2)}) %all-to-all-start.6) | async-done | bytes 262176 | tf_op jit(solution)/shard_map/all_to_all | solution.py:98
  (63 shorter events, 41.5 us)
Async XLA Ops:
  7.1 52.2 %all-to-all-start.2 = ((bf16[64,24,512]{2,1,0:T(8,128)(2,1)}), bf16[64,24,512]{2,1,0:T(8,128)(2,1)S(1)}, u32[]{:S(2)}, u32[]{:S(2)}) async-start(bf16[64,24,512]{2,1,0:T(8,128)(2,1)} %bitcast.64), calls=%async_computation.2 | async-start | bytes 3145728 | tf_op jit(solution)/shard_map/all_to_all | solution.py:98
  62.5 93.7 %copy-start.1 = (bf16[512,512]{1,0:T(8,128)(2,1)}, bf16[512,512]{1,0:T(8,128)(2,1)S(1)}, u32[]{:S(2)}) copy-start(bf16[512,512]{1,0:T(8,128)(2,1)S(1)} %get-tuple-element.73.refs_1_) | copy-start | bytes 1572868
  62.5 14.9 %collective-permute-start = (bf16[512,512]{1,0:T(8,128)(2,1)S(1)}, bf16[512,512]{1,0:T(8,128)(2,1)S(1)}, u32[]{:S(2)}, u32[]{:S(2)}) collective-permute-start(bf16[512,512]{1,0:T(8,128)(2,1)S(1)} %get-tuple-element.72.refs_0_), channel_id=1, source_target_pairs={{0,1},{1,2},{2,3},{3,0},{4,5},{5,6},{6,7},{7,4},{8,9},{9,10},{10,1... | collective-permute-start | bytes 1572872 | tf_op jit(solution)/shard_map/ppermute | solution.py:94
  62.8 16.0 %collective-permute-start.3 = (bf16[512,512]{1,0:T(8,128)(2,1)S(1)}, bf16[512,512]{1,0:T(8,128)(2,1)S(1)}, u32[]{:S(2)}, u32[]{:S(2)}) collective-permute-start(bf16[512,512]{1,0:T(8,128)(2,1)S(1)} %get-tuple-element.73.refs_1_), channel_id=1, source_target_pairs={{0,3},{1,0},{2,1},{3,2},{4,7},{5,4},{6,5},{7,6},{8,11},{9,8},{10,9... | collective-permute-start | bytes 1572872 | tf_op jit(solution)/shard_map/ppermute | solution.py:94
  64.6 24.0 %collective-permute-start.1 = (bf16[512,512]{1,0:T(8,128)(2,1)S(1)}, bf16[512,512]{1,0:T(8,128)(2,1)S(1)}, u32[]{:S(2)}, u32[]{:S(2)}) collective-permute-start(bf16[512,512]{1,0:T(8,128)(2,1)S(1)} %get-tuple-element.73.refs_1_), channel_id=1, source_target_pairs={{0,1},{1,2},{2,3},{3,0},{4,5},{5,6},{6,7},{7,4},{8,9},{9,10},{10,1... | collective-permute-start | bytes 1572872 | tf_op jit(solution)/shard_map/ppermute | solution.py:94
  66.0 90.2 %collective-permute-start.2 = (bf16[512,512]{1,0:T(8,128)(2,1)S(1)}, bf16[512,512]{1,0:T(8,128)(2,1)S(1)}, u32[]{:S(2)}, u32[]{:S(2)}) collective-permute-start(bf16[512,512]{1,0:T(8,128)(2,1)S(1)} %get-tuple-element.72.refs_0_), channel_id=1, source_target_pairs={{0,3},{1,0},{2,1},{3,2},{4,7},{5,4},{6,5},{7,6},{8,11},{9,8},{10,9... | collective-permute-start | bytes 1572872 | tf_op jit(solution)/shard_map/ppermute | solution.py:94
  77.4 83.2 %collective-permute-start.4 = (bf16[512,512]{1,0:T(8,128)(2,1)S(1)}, bf16[512,512]{1,0:T(8,128)(2,1)}, u32[]{:S(2)}, u32[]{:S(2)}) collective-permute-start(bf16[512,512]{1,0:T(8,128)(2,1)S(1)} %collective-permute-done.refs_2_), channel_id=1, source_target_pairs={{0,1},{1,2},{2,3},{3,0},{4,5},{5,6},{6,7},{7,4},{8,9},{9,10},{10,1... | collective-permute-start | bytes 1572872 | tf_op jit(solution)/shard_map/ppermute | solution.py:94
  78.8 81.8 %collective-permute-start.5 = (bf16[512,512]{1,0:T(8,128)(2,1)S(1)}, bf16[512,512]{1,0:T(8,128)(2,1)}, u32[]{:S(2)}, u32[]{:S(2)}) collective-permute-start(bf16[512,512]{1,0:T(8,128)(2,1)S(1)} %collective-permute-done.3.refs_5_), channel_id=1, source_target_pairs={{0,3},{1,0},{2,1},{3,2},{4,7},{5,4},{6,5},{7,6},{8,11},{9,8},{10,9... | collective-permute-start | bytes 1572872 | tf_op jit(solution)/shard_map/ppermute | solution.py:94
  90.3 88.3 %all-to-all-start.3 = ((bf16[8,192,512]{2,1,0:T(8,128)(2,1)}), bf16[8,192,512]{2,1,0:T(8,128)(2,1)}, u32[]{:S(2)}, u32[]{:S(2)}) async-start(bf16[8,192,512]{2,1,0:T(8,128)(2,1)} %get-tuple-element.79), calls=%async_computation.3 | async-start | bytes 3145728 | tf_op jit(solution)/shard_map/all_to_all | solution.py:98
  165.8 9.2 %collective-permute-start.6 = (bf16[256,512]{1,0:T(8,128)(2,1)S(1)}, bf16[256,512]{1,0:T(8,128)(2,1)S(1)}, u32[]{:S(2)}, u32[]{:S(2)}) collective-permute-start(bf16[256,512]{1,0:T(8,128)(2,1)S(1)} %get-tuple-element.82), channel_id=1, source_target_pairs={{0,1},{1,2},{2,3},{3,0},{4,5},{5,6},{6,7},{7,4},{8,9},{9,10},{10,1... | collective-permute-start | bytes 786440 | tf_op jit(solution)/shard_map/ppermute | solution.py:94
  167.9 10.5 %collective-permute-start.10 = (bf16[256,512]{1,0:T(8,128)(2,1)S(1)}, bf16[256,512]{1,0:T(8,128)(2,1)S(1)}, u32[]{:S(2)}, u32[]{:S(2)}) collective-permute-start(bf16[256,512]{1,0:T(8,128)(2,1)S(1)} %get-tuple-element.84), channel_id=1, source_target_pairs={{0,3},{1,0},{2,1},{3,2},{4,7},{5,4},{6,5},{7,6},{8,11},{9,8},{10,9... | collective-permute-start | bytes 786440 | tf_op jit(solution)/shard_map/ppermute | solution.py:94
  167.9 16.0 %collective-permute-start.9 = (bf16[256,512]{1,0:T(8,128)(2,1)S(1)}, bf16[256,512]{1,0:T(8,128)(2,1)S(1)}, u32[]{:S(2)}, u32[]{:S(2)}) collective-permute-start(bf16[256,512]{1,0:T(8,128)(2,1)S(1)} %slice.24), channel_id=1, source_target_pairs={{0,3},{1,0},{2,1},{3,2},{4,7},{5,4},{6,5},{7,6},{8,11},{9,8},{10,9... | collective-permute-start | bytes 786440 | tf_op jit(solution)/shard_map/ppermute | solution.py:94
  168.0 15.9 %collective-permute-start.8 = (bf16[256,512]{1,0:T(8,128)(2,1)S(1)}, bf16[256,512]{1,0:T(8,128)(2,1)S(1)}, u32[]{:S(2)}, u32[]{:S(2)}) collective-permute-start(bf16[256,512]{1,0:T(8,128)(2,1)S(1)} %slice.23), channel_id=1, source_target_pairs={{0,1},{1,2},{2,3},{3,0},{4,5},{5,6},{6,7},{7,4},{8,9},{9,10},{10,1... | collective-permute-start | bytes 786440 | tf_op jit(solution)/shard_map/ppermute | solution.py:94
  175.1 10.7 %collective-permute-start.7 = (bf16[256,512]{1,0:T(8,128)(2,1)S(1)}, bf16[256,512]{1,0:T(8,128)(2,1)S(1)}, u32[]{:S(2)}, u32[]{:S(2)}) collective-permute-start(bf16[256,512]{1,0:T(8,128)(2,1)S(1)} %add_convert_fusion.1), channel_id=1, source_target_pairs={{0,1},{1,2},{2,3},{3,0},{4,5},{5,6},{6,7},{7,4},{8,9},{9,10},{10,1... | collective-permute-start | bytes 786440 | tf_op jit(solution)/shard_map/ppermute | solution.py:94
  178.5 10.3 %collective-permute-start.11 = (bf16[256,512]{1,0:T(8,128)(2,1)S(1)}, bf16[256,512]{1,0:T(8,128)(2,1)S(1)}, u32[]{:S(2)}, u32[]{:S(2)}) collective-permute-start(bf16[256,512]{1,0:T(8,128)(2,1)S(1)} %add_convert_fusion), channel_id=1, source_target_pairs={{0,3},{1,0},{2,1},{3,2},{4,7},{5,4},{6,5},{7,6},{8,11},{9,8},{10,9... | collective-permute-start | bytes 786440 | tf_op jit(solution)/shard_map/ppermute | solution.py:94
  194.3 30.1 %all-to-all-start.4 = ((bf16[64,24,256]{2,1,0:T(8,128)(2,1)}), bf16[64,24,256]{2,1,0:T(8,128)(2,1)S(1)}, u32[]{:S(2)}, u32[]{:S(2)}) async-start(bf16[64,24,256]{2,1,0:T(8,128)(2,1)} %bitcast.68), calls=%async_computation.4 | async-start | bytes 1572864 | tf_op jit(solution)/shard_map/all_to_all | solution.py:98
  226.3 14.5 %collective-permute-start.17 = (bf16[192,512]{1,0:T(8,128)(2,1)S(1)}, bf16[192,512]{1,0:T(8,128)(2,1)S(1)}, u32[]{:S(2)}, u32[]{:S(2)}) collective-permute-start(bf16[192,512]{1,0:T(8,128)(2,1)S(1)} %get-tuple-element.97.p0), channel_id=1, source_target_pairs={{0,2},{1,3},{2,0},{3,1},{4,6},{5,7},{6,4},{7,5},{8,10},{9,11},{10,... | collective-permute-start | bytes 589832 | tf_op jit(solution)/shard_map/ppermute | solution.py:94
  226.4 14.4 %collective-permute-start.16 = (bf16[192,512]{1,0:T(8,128)(2,1)S(1)}, bf16[192,512]{1,0:T(8,128)(2,1)S(1)}, u32[]{:S(2)}, u32[]{:S(2)}) collective-permute-start(bf16[192,512]{1,0:T(8,128)(2,1)S(1)} %get-tuple-element.97.p0), channel_id=1, source_target_pairs={{0,3},{1,0},{2,1},{3,2},{4,7},{5,4},{6,5},{7,6},{8,11},{9,8},{10,9... | collective-permute-start | bytes 589832 | tf_op jit(solution)/shard_map/ppermute | solution.py:94
  227.5 13.3 %collective-permute-start.15 = (bf16[192,512]{1,0:T(8,128)(2,1)S(1)}, bf16[192,512]{1,0:T(8,128)(2,1)S(1)}, u32[]{:S(2)}, u32[]{:S(2)}) collective-permute-start(bf16[192,512]{1,0:T(8,128)(2,1)S(1)} %get-tuple-element.97.p0), channel_id=1, source_target_pairs={{0,1},{1,2},{2,3},{3,0},{4,5},{5,6},{6,7},{7,4},{8,9},{9,10},{10,1... | collective-permute-start | bytes 589832 | tf_op jit(solution)/shard_map/ppermute | solution.py:94
  244.8 20.3 %all-to-all-start.7 = ((f32[64,8,128]{2,1,0:T(8,128)}), f32[64,8,128]{2,1,0:T(8,128)S(1)}, u32[]{:S(2)}, u32[]{:S(2)}) async-start(f32[64,8,128]{2,1,0:T(8,128)} %bitcast.70), calls=%async_computation.7 | async-start | bytes 524288 | tf_op jit(solution)/shard_map/all_to_all | solution.py:98
  249.4 9.4 %collective-permute-start.14 = (bf16[8,96,128]{2,1,0:T(8,128)(2,1)S(1)}, bf16[8,96,128]{2,1,0:T(8,128)(2,1)S(1)}, u32[]{:S(2)}, u32[]{:S(2)}) collective-permute-start(bf16[8,96,128]{2,1,0:T(8,128)(2,1)S(1)} %all_to_all.63.p0), channel_id=1, source_target_pairs={{0,2},{1,3},{2,0},{3,1},{4,6},{5,7},{6,4},{7,5},{8,10},{9,11},{10,... | collective-permute-start | bytes 589832 | tf_op jit(solution)/shard_map/ppermute | solution.py:94
  251.5 10.5 %collective-permute-start.13 = (bf16[8,96,128]{2,1,0:T(8,128)(2,1)S(1)}, bf16[8,96,128]{2,1,0:T(8,128)(2,1)S(1)}, u32[]{:S(2)}, u32[]{:S(2)}) collective-permute-start(bf16[8,96,128]{2,1,0:T(8,128)(2,1)S(1)} %all_to_all.63.p0), channel_id=1, source_target_pairs={{0,3},{1,0},{2,1},{3,2},{4,7},{5,4},{6,5},{7,6},{8,11},{9,8},{10,9... | collective-permute-start | bytes 589832 | tf_op jit(solution)/shard_map/ppermute | solution.py:94
  251.5 10.5 %collective-permute-start.12 = (bf16[8,96,128]{2,1,0:T(8,128)(2,1)S(1)}, bf16[8,96,128]{2,1,0:T(8,128)(2,1)S(1)}, u32[]{:S(2)}, u32[]{:S(2)}) collective-permute-start(bf16[8,96,128]{2,1,0:T(8,128)(2,1)S(1)} %all_to_all.63.p0), channel_id=1, source_target_pairs={{0,1},{1,2},{2,3},{3,0},{4,5},{5,6},{6,7},{7,4},{8,9},{9,10},{10,1... | collective-permute-start | bytes 589832 | tf_op jit(solution)/shard_map/ppermute | solution.py:94
  265.2 19.1 %all-to-all-start.6 = ((bf16[8,32,512]{2,1,0:T(8,128)(2,1)}), bf16[8,32,512]{2,1,0:T(8,128)(2,1)S(1)}, u32[]{:S(2)}, u32[]{:S(2)}) async-start(bf16[8,32,512]{2,1,0:T(8,128)(2,1)} %bitcast.69), calls=%async_computation.6 | async-start | bytes 524288 | tf_op jit(solution)/shard_map/all_to_all | solution.py:98
  (8 other events, 350.2 us)

commit v3 on v1

--- a/solution.py
+++ b/solution.py
@@ -42,17 +42,46 @@
     return jax.ShapeDtypeStruct(dims, dtype)
 
 
+class Near:
+    def __init__(self, value):
+        self.value = value
+
+
+def size(a):
+    return a.size * a.dtype.itemsize
+
+
 def local(kernel, name, outs, flops, *args, scratch=(), smem=0):
-    moved = sum(a.size * a.dtype.itemsize for a in (*args, *jax.tree.leaves(outs)))
-    return pl.pallas_call(
+    def unwrapped(a):
+        return a.value if isinstance(a, Near) else a
+
+    def operand(n, a):
+        if isinstance(a, Near):
+            return pltpu.with_memory_space_constraint(a.value, pltpu.VMEM)
+        if n < smem or a.ndim < 2:
+            return a
+        return pltpu.with_memory_space_constraint(a, pltpu.HBM)
+
+    def result(o):
+        if isinstance(o, Near):
+            return pltpu.VMEM(o.value.shape, o.value.dtype)
+        return pltpu.HBM(o.shape, o.dtype)
+
+    single = not isinstance(outs, tuple)
+    every = (*args, *((outs,) if single else outs))
+    staged = sum(size(a) for a in every if not isinstance(a, Near))
+    moved = sum(size(unwrapped(a)) for a in every)
+    got = pl.pallas_call(
         kernel,
         name=name,
-        out_shape=outs,
+        out_shape=result(outs) if single else tuple(result(o) for o in outs),
         in_specs=[SMEM] * smem + [VMEM] * (len(args) - smem),
-        out_specs=jax.tree.map(lambda _: VMEM, outs),
+        out_specs=VMEM if single else (VMEM,) * len(outs),
         scratch_shapes=list(scratch),
+        compiler_params=pltpu.CompilerParams(vmem_limit_bytes=staged + (10 << 20)),
         cost_estimate=pl.CostEstimate(flops=int(flops), bytes_accessed=moved, transcendentals=0),
-    )(*args)
+    )(*[operand(n, a) for n, a in enumerate(args)])
+    return got
 
 
 def shift(value, axis, by):
@@ -68,7 +97,21 @@
     return jnp.where(mask, 1.0, 0.0).astype(BF16)
 
 
-def route_kernel(ids_ref, ids_t_ref, weights_t_ref, mixed_ref, d_out_ref, send_ref, slots_ref):
+def slots_kernel(ids_ref, slots_ref):
+    i32 = jnp.int32
+    later = one_hot(
+        lax.broadcasted_iota(i32, (TOK, TOK), 1) < lax.broadcasted_iota(i32, (TOK, TOK), 0)
+    )
+    expert_c = lax.broadcasted_iota(i32, (TOK, EXPERTS), 1)
+    cols = [ids_ref[:, k : k + 1] for k in range(2)]
+    named_c = [c == expert_c for c in cols]
+    count_c = dot(later, one_hot(named_c[0] | named_c[1]))
+    for k in range(2):
+        rank = jnp.sum(jnp.where(named_c[k], count_c, 0.0), axis=1, keepdims=True)
+        slots_ref[:, k : k + 1] = cols[k] * BLOCK + rank.astype(i32)
+
+
+def route_kernel(ids_t_ref, weights_t_ref, mixed_ref, d_out_ref, send_ref):
     i32 = jnp.int32
     before = one_hot(
         lax.broadcasted_iota(i32, (TOK, TOK), 0) < lax.broadcasted_iota(i32, (TOK, TOK), 1)
@@ -82,16 +125,6 @@
         + jnp.sum(jnp.where(named[k], count, 0.0), axis=0, keepdims=True).astype(i32)
         for k in range(2)
     ]
-    later = one_hot(
-        lax.broadcasted_iota(i32, (TOK, TOK), 1) < lax.broadcasted_iota(i32, (TOK, TOK), 0)
-    )
-    expert_c = lax.broadcasted_iota(i32, (TOK, EXPERTS), 1)
-    cols = [ids_ref[:, k : k + 1] for k in range(2)]
-    named_c = [c == expert_c for c in cols]
-    count_c = dot(later, one_hot(named_c[0] | named_c[1]))
-    for k in range(2):
-        rank = jnp.sum(jnp.where(named_c[k], count_c, 0.0), axis=1, keepdims=True)
-        slots_ref[:, k : k + 1] = cols[k] * BLOCK + rank.astype(i32)
     weights = [weights_t_ref[k : k + 1, :] for k in range(2)]
     mixed = mixed_ref[...]
     d_out = d_out_ref[...]
@@ -134,15 +167,15 @@
     return jnp.asarray(matrix, BF16)
 
 
-def sort_kernel(got_ref, order_ref, mix_a, mix_b, cot_a, cot_b):
+def sort_kernel(got_ref, order_ref, rows_a, rows_b):
     order = order_ref[...]
     half = GROUP // 2
     for g in range(GROUPS):
         out = dot(order, got_ref[g * GROUP : (g + 1) * GROUP, :]).astype(BF16)
         at = (g % (GROUPS // 2)) * half
-        mix, cot = (mix_a, cot_a) if g < GROUPS // 2 else (mix_b, cot_b)
-        mix[at : at + half, :] = out[:half]
-        cot[at : at + half, :] = out[half:]
+        rows = rows_a if g < GROUPS // 2 else rows_b
+        rows[at : at + half, :] = out[:half]
+        rows[HALF + at : HALF + at + half, :] = out[half:]
 
 
 def block_of(me_ref, step):
@@ -152,42 +185,47 @@
 STEPS = (0, 3, 1, 2)
 
 
-def expert_up_kernel(me_ref, *refs):
-    pieces, (gate_ref, up_ref), (hidden_ref, silu_ref, slope_ref) = refs[:8], refs[8:10], refs[10:]
+def hidden_terms(me_ref, refs, turns, gate_ref, up_ref, down_ref, h):
+    sums = None
+    for p, turn in enumerate(turns):
+        piece = refs[2 * p + h]
+        at = block_of(me_ref, turn)
+        mix = piece[:HALF, :]
+        terms = (
+            dot(mix, gate_ref[pl.ds(at, WIDTH), :]),
+            dot(mix, up_ref[pl.ds(at, WIDTH), :]),
+            dot_bt(piece[HALF:, :], down_ref[:, pl.ds(at, WIDTH)]),
+        )
+        sums = terms if sums is None else tuple(a + b for a, b in zip(sums, terms))
+    return sums
+
+
+def expert_near_kernel(me_ref, *refs):
+    gate_ref, up_ref, down_ref = refs[6:9]
     for h in range(2):
-        up_pre = linear = None
-        for p in range(4):
-            piece = pieces[2 * p + h][...]
-            at = block_of(me_ref, STEPS[p])
-            one = dot(piece, gate_ref[pl.ds(at, WIDTH), :])
-            two = dot(piece, up_ref[pl.ds(at, WIDTH), :])
-            up_pre = one if up_pre is None else up_pre + one
-            linear = two if linear is None else linear + two
+        rows = slice(h * HALF, (h + 1) * HALF)
+        terms = hidden_terms(me_ref, refs[:6], STEPS[:3], gate_ref, up_ref, down_ref, h)
+        for term, out in zip(terms, refs[9:]):
+            out[rows, :] = term
+
+
+def expert_far_kernel(me_ref, *refs):
+    gate_ref, up_ref, down_ref = refs[2:5]
+    near_refs = refs[5:8]
+    hidden_ref, d_up_ref, d_linear_ref, far_a, far_b, left_ref, right_ref, own_ref = refs[8:]
+    for h in range(2):
+        rows = slice(h * HALF, (h + 1) * HALF)
+        terms = hidden_terms(me_ref, refs[:2], STEPS[3:], gate_ref, up_ref, down_ref, h)
+        up_pre, linear, d_hidden = (a[rows, :] + b for a, b in zip(near_refs, terms))
         sigmoid = jax.nn.sigmoid(up_pre)
         silu = up_pre * sigmoid
-        rows = slice(h * HALF, (h + 1) * HALF)
         hidden_ref[rows, :] = (silu * linear).astype(BF16)
-        silu_ref[rows, :] = silu
-        slope_ref[rows, :] = linear * sigmoid * (1.0 + up_pre * (1.0 - sigmoid))
-
-
-def expert_down_kernel(me_ref, *refs):
-    pieces = refs[:8]
-    gate_ref, up_ref, down_ref, silu_ref, slope_ref = refs[8:13]
-    d_up_ref, d_linear_ref, far_a, far_b, left_ref, right_ref, own_ref = refs[13:]
-    ups, linears = [], []
-    for h in range(2):
-        rows = slice(h * HALF, (h + 1) * HALF)
-        d_hidden = None
-        for p in range(4):
-            at = block_of(me_ref, STEPS[p])
-            one = dot_bt(pieces[2 * p + h][...], down_ref[:, pl.ds(at, WIDTH)])
-            d_hidden = one if d_hidden is None else d_hidden + one
-        d_linear_ref[rows, :] = (d_hidden * silu_ref[rows, :]).astype(BF16)
-        d_up_ref[rows, :] = (d_hidden * slope_ref[rows, :]).astype(BF16)
-
-    def part(rows, step):
-        at = block_of(me_ref, step)
+        d_linear_ref[rows, :] = (d_hidden * silu).astype(BF16)
+        slope = linear * sigmoid * (1.0 + up_pre * (1.0 - sigmoid))
+        d_up_ref[rows, :] = (d_hidden * slope).astype(BF16)
+
+    def part(rows, turn):
+        at = block_of(me_ref, turn)
         return (
             dot_bt(d_up_ref[rows, :], gate_ref[pl.ds(at, WIDTH), :])
             + dot_bt(d_linear_ref[rows, :], up_ref[pl.ds(at, WIDTH), :])
@@ -203,26 +241,25 @@
 
 
 def expert_grad_kernel(me_ref, *refs):
-    mixes, cots = refs[:8], refs[8:16]
-    d_up_ref, d_linear_ref, hidden_ref = refs[16:19]
-    grad_gate_ref, grad_up_ref, grad_down_ref = refs[19:]
+    pieces = refs[:8]
+    d_up_ref, d_linear_ref, hidden_ref = refs[8:11]
+    grad_gate_ref, grad_up_ref, grad_down_ref = refs[11:]
     top, low = (slice(0, HALF), slice(HALF, ROWS))
     for p in range(4):
-        mix = (mixes[2 * p], mixes[2 * p + 1])
-        cot = (cots[2 * p], cots[2 * p + 1])
-
-        def step(n, carry):
+
+        def step(n, carry, halves=(pieces[2 * p], pieces[2 * p + 1]), p=p):
             cols = pl.ds(pl.multiple_of(n * 128, 128), 128)
             at = pl.ds(pl.multiple_of(block_of(me_ref, STEPS[p]) + n * 128, 128), 128)
-            mix_a, mix_b = (mix[0][:, cols], mix[1][:, cols])
+            mix_a, mix_b = (half[:HALF, cols] for half in halves)
+            cot_a, cot_b = (half[HALF:, cols] for half in halves)
             grad_gate_ref[0, at, :] = dot_at(mix_a, d_up_ref[top, :]) + dot_at(
                 mix_b, d_up_ref[low, :]
             )
             grad_up_ref[0, at, :] = dot_at(mix_a, d_linear_ref[top, :]) + dot_at(
                 mix_b, d_linear_ref[low, :]
             )
-            grad_down_ref[0, :, at] = dot_at(hidden_ref[top, :], cot[0][:, cols]) + dot_at(
-                hidden_ref[low, :], cot[1][:, cols]
+            grad_down_ref[0, :, at] = dot_at(hidden_ref[top, :], cot_a) + dot_at(
+                hidden_ref[low, :], cot_b
             )
             return carry
 
@@ -330,7 +367,9 @@
         t = jnp.tanh(c0 * (x + 0.044715 * x * x * x))
         act = 0.5 * x * (1.0 + t)
         deriv = 0.5 * (1.0 + t) + 0.5 * x * (1.0 - t * t) * (c0 * (1.0 + 0.134145 * x * x))
-        merged_ref[rows, :] = (act * states).astype(BF16)
+        merged = (act * states).astype(BF16)
+        for k in range(8):
+            merged_ref[k, rows, :] = merged
         act_ref[rows, :] = act
         slope_ref[rows, :] = states * deriv
         decay_ref[rows, :] = decay
@@ -479,16 +518,18 @@
     me = lax.axis_index("tp").astype(jnp.int32).reshape(1)
     here = lax.axis_index(SP).astype(jnp.int32).reshape(1)
     unit = 2 * ROWS * 2048 * HID
-    send, slots = local(
+    send = local(
         route_kernel,
         "route",
-        (shape((EXPERTS * BLOCK, WIDTH), BF16), shape((TOK, 2), jnp.int32)),
+        shape((EXPERTS * BLOCK, WIDTH), BF16),
         1.3e9,
-        expert_ids,
         expert_ids.T,
         route_weights.T,
         mixed,
         d_out,
+    )
+    slots = local(
+        slots_kernel, "slots", shape((TOK, 2), jnp.int32), 1e7, after(expert_ids, send)
     )
     got = exchange(send, SP)
     f_like = shape((TOK, WIDTH), F32)
@@ -496,7 +537,7 @@
     merged, act, slope, decay, kr, ki, kd = local(
         forward_kernel,
         "forward",
-        (shape((TOK, WIDTH), BF16),) + (f_like,) * 6,
+        (shape((8, TOK, WIDTH), BF16),) + (f_like,) * 6,
         6e9,
         after(conv_out, send),
         gate_in,
@@ -507,33 +548,40 @@
         w_input,
         scratch=(pltpu.VMEM((TOK, WIDTH), F32),) * 2,
     )
-    got = after(got, merged)
+    got = after(got, merged, slots)
     piece = shape((HALF, WIDTH), BF16)
-    mix_a, mix_b, cot_a, cot_b = local(
-        sort_kernel, "sort", (piece,) * 4, 1e9, got, sort_matrix()
-    )
-    mixes = gathered(mix_a, mix_b)
-    cots = gathered(cot_a, cot_b)
+    full = shape((ROWS, WIDTH), BF16)
+    rows_a, rows_b = local(
+        sort_kernel, "sort", (Near(full), Near(full)), 1e9, Near(got), sort_matrix()
+    )
+    pieces = gathered(rows_a, rows_b)
     gate2, up2, down2 = (w_gate[0], w_up[0], w_down[0])
     hid = shape((ROWS, HID), BF16)
     hid_f = shape((ROWS, HID), F32)
-    full = shape((ROWS, WIDTH), BF16)
-    hidden, silu, up_slope = local(
-        expert_up_kernel, "expert_up", (hid, hid_f, hid_f), 2 * unit, me, *mixes, gate2, up2, smem=1
-    )
-    merged_x = exchange(jnp.broadcast_to(after(merged, hidden)[None], (8, TOK, WIDTH)), XC)
-    d_up, d_linear, far_a, far_b, left, right, own = local(
-        expert_down_kernel,
-        "expert_down",
-        (hid, hid, piece, piece, full, full, full),
-        3 * unit,
+    near = local(
+        expert_near_kernel,
+        "expert_near",
+        (hid_f,) * 3,
+        2 * unit,
         me,
-        *cots,
+        *map(Near, pieces[:6]),
         gate2,
         up2,
         down2,
-        silu,
-        up_slope,
+        smem=1,
+    )
+    merged_x = exchange(after(merged, pieces[3]), XC)
+    hidden, d_up, d_linear, far_a, far_b, left, right, own = local(
+        expert_far_kernel,
+        "expert_far",
+        (hid, hid, hid, *map(Near, (piece, piece, full, full)), full),
+        3 * unit,
+        me,
+        *map(Near, pieces[6:]),
+        gate2,
+        up2,
+        down2,
+        *near,
         smem=1,
     )
     over_a, over_b = (shift(far_a, "tp", 1), shift(far_b, "tp", -1))
@@ -547,10 +595,10 @@
         shape((EXPERTS * BLOCK, WIDTH // 2), BF16),
         1e9,
         after(own, merged_x),
-        right_a,
-        right_b,
-        left_a,
-        left_b,
+        Near(right_a),
+        Near(right_b),
+        Near(left_a),
+        Near(left_b),
         spread_matrix(),
     )
     back = exchange(returned, SP)
@@ -560,8 +608,7 @@
         (shape((1, 2048, HID), F32), shape((1, 2048, HID), F32), shape((1, HID, 2048), F32)),
         3 * unit,
         me,
-        *mixes,
-        *cots,
+        *pieces,
         after(d_up, returned),
         d_linear,
         hidden,
@@ -571,9 +618,9 @@
     d_columns, crossing = local(
         combine_kernel,
         "combine",
-        (shape((TOK, WIDTH), BF16), shape((8, TOK // 2, 128), BF16)),
+        (Near(shape((TOK, WIDTH), BF16)), Near(shape((8, TOK // 2, 128), BF16))),
         1e9,
-        back,
+        Near(back),
         slots,
         d_out,
     )
@@ -583,11 +630,10 @@
     grad_gate, local_grad, products, carries = local(
         reverse_kernel,
         "reverse",
-        (shape((TOK, WIDTH), BF16), f_like, f_like, shape((EXPERTS * 8, 128), F32)),
+        (shape((TOK, WIDTH), BF16), Near(f_like), Near(f_like), shape((EXPERTS * 8, 128), F32)),
         4e9,
         me,
-        after(pieces[0], crossed),
-        *pieces[1:],
+        *map(Near, (after(pieces[0], crossed), *pieces[1:])),
         w_out,
         act,
         slope,
@@ -602,8 +648,8 @@
         shape((256, WIDTH), BF16),
         1e9,
         me,
-        *columns,
-        merged_x,
+        *map(Near, columns),
+        Near(merged_x),
         smem=1,
     )
     parts = exchange(grad_part, "z")
@@ -614,9 +660,9 @@
         shape((TOK, WIDTH), BF16),
         2e9,
         here,
-        carried,
-        local_grad,
-        products,
+        Near(carried),
+        Near(local_grad),
+        Near(products),
         kr,
         ki,
         kd,

time: 253 us -> 240 us (0.949)
  starting transfers between devices: 68.5 us -> 57.8 us
  waiting for transfers between devices: 104 us -> 111 us
  local copies, waits for them, and re-layouts: 10.5 us -> 4.37 us
  Pallas kernels: 54.8 us -> 50.9 us
    ppermute x24 -> x18, starting transfers between devices: 32.9 us -> 22.4 us  [shift(): return lax.ppermute(value, axis, [(i, (i + by) % n) for i in range(n)])]
    ppermute x24 -> x18, waiting for transfers between devices: 51.4 us -> 60.7 us  [shift(): return lax.ppermute(value, axis, [(i, (i + by) % n) for i in range(n)])]
    unnamed x49 -> x14, local copies, waits for them, and re-layouts: 6.41 us -> 2.03 us
    pallas_call x11 -> x12, Pallas kernels: 54.8 us -> 50.9 us  [local(): pl.pallas_call(kernel, name=name, out_shape=result(outs) if single else t...]
    all_to_all x5, waiting for transfers between devices: 52.8 us -> 50.1 us  [exchange(): return lax.all_to_all(value, axes, 0, 0, tiled=True)]
  transfers between devices with their start and end apart: 29 -> 23, of which waited for: 15 -> 13; matrix products, arithmetic and copies ran while one was open for 2% -> 2% of each run, Pallas kernels for 15% -> 16%
where the time goes in v3:
time: 240 us; the launch traced here: 239 us
  waiting for transfers between devices  111 us (46%)
  starting transfers between devices  57.8 us (24%)
  Pallas kernels  50.9 us (21%)
  blocking collectives  10.9 us (5%)
  local copies, waits for them, and re-layouts  4.37 us (2%)
  other arithmetic  2.97 us (1%)
    ppermute x18, waiting for transfers between devices, shift(): return lax.ppermute(value, axis, [(i, (i + by) % n) for i in range(n)])  60.7 us
    pallas_call x12, Pallas kernels, local(): pl.pallas_call(kernel, name=name, out_shape=result(outs) if single else t...  50.9 us
    all_to_all x5, waiting for transfers between devices, exchange(): return lax.all_to_all(value, axes, 0, 0, tiled=True)  50.1 us
    all_to_all x5, starting transfers between devices, exchange(): return lax.all_to_all(value, axes, 0, 0, tiled=True)  35.4 us
    ppermute x18, starting transfers between devices, shift(): return lax.ppermute(value, axis, [(i, (i + by) % n) for i in range(n)])  22.4 us
    all_to_all x1, blocking collectives, exchange(): return lax.all_to_all(value, axes, 0, 0, tiled=True)  10.9 us
  transfers between devices with their start and end apart: 23, of which 13 were waited for; matrix products, arithmetic and copies ran while one was open for 2% of the time, Pallas kernels for 16%

profile of v3, /device:TPU:24, one launch (start us, length us, event | category | flops | bytes accessed | tf_op | source)
XLA Modules:
  0.0 238.5 jit_solution(8769513864049639487)
XLA Ops:
  0.6 4.0 %route.1 = bf16[1536,512]{1,0:T(8,128)(2,1)} custom-call(s32[2,192]{1,0:T(2,128)} %bitcast.29, f32[2,192]{1,0:T(2,128)} %bitcast.32, bf16[192,512]{1,0:T(8,128)(2,1)} %mixed_ref.1, bf16[192,512]{1,0:T(8,128)(2,1)} %d_out_ref.3), custom_call_target="tpu_custom_call" | custom-call | flops 1300000000 | bytes 1969152 | tf_op jit(solution)/shard_map/route/pallas_call | solution.py:74
  4.6 12.1 %all-to-all-start = ((bf16[64,24,512]{2,1,0:T(8,128)(2,1)}), bf16[64,24,512]{2,1,0:T(8,128)(2,1)S(1)}, u32[]{:S(2)}, u32[]{:S(2)}) async-start(bf16[64,24,512]{2,1,0:T(8,128)(2,1)} %bitcast.19), calls=%async_computation | async-start | bytes 3145728 | tf_op jit(solution)/shard_map/all_to_all | solution.py:93
  20.8 5.6 %forward.1 = (bf16[8,192,512]{2,1,0:T(8,128)(2,1)}, f32[192,512]{1,0:T(8,128)}, f32[192,512]{1,0:T(8,128)}, f32[192,512]{1,0:T(8,128)}, f32[192,512]{1,0:T(8,128...) custom-call(bf16[192,512]{1,0:T(8,128)(2,1)} %conv_ref, bf16[192,512]{1,0:T(8,128)(2,1)} %gate_ref.1, f32[1,512]{1,0:T(1,128)} %start_ref.1, ...), custom_call_target="tpu_custom_call" | custom-call | flops 6000000000 | bytes 4592384 | tf_op jit(solution)/shard_map/forward/pallas_call | solution.py:74
  26.4 30.4 %all-to-all-done = bf16[64,24,512]{2,1,0:T(8,128)(2,1)S(1)} async-done(((bf16[64,24,512]{2,1,0:T(8,128)(2,1)}), bf16[64,24,512]{2,1,0:T(8,128)(2,1)S(1)}, u32[]{:S(2)}, u32[]{:S(2)}) %all-to-all-start) | async-done | bytes 1572896 | tf_op jit(solution)/shard_map/all_to_all | solution.py:93
  62.4 16.5 %collective-permute-done.refs_2_ = bf16[768,512]{1,0:T(8,128)(2,1)} collective-permute-done((bf16[768,512]{1,0:T(8,128)(2,1)S(1)}, bf16[768,512]{1,0:T(8,128)(2,1)}, u32[]{:S(2)}, u32[]{:S(2)}) %collective-permute-start) | collective-permute-done | bytes 786464 | tf_op jit(solution)/shard_map/ppermute | solution.py:89
  80.9 14.7 %collective-permute-done.1.refs_3_ = bf16[768,512]{1,0:T(8,128)(2,1)S(1)} collective-permute-done((bf16[768,512]{1,0:T(8,128)(2,1)S(1)}, bf16[768,512]{1,0:T(8,128)(2,1)S(1)}, u32[]{:S(2)}, u32[]{:S(2)}) %collective-permute-start.1) | collective-permute-done | bytes 786464 | tf_op jit(solution)/shard_map/ppermute | solution.py:89
  96.5 4.3 %all-to-all-start.1 = ((bf16[8,192,512]{2,1,0:T(8,128)(2,1)}), bf16[8,192,512]{2,1,0:T(8,128)(2,1)S(1)}, u32[]{:S(2)}, u32[]{:S(2)}) async-start(bf16[8,192,512]{2,1,0:T(8,128)(2,1)} %get-tuple-element.54), calls=%async_computation.1 | async-start | bytes 3145728 | tf_op jit(solution)/shard_map/all_to_all | solution.py:93
  101.9 5.6 %expert_near.1 = (f32[768,256]{1,0:T(8,128)}, f32[768,256]{1,0:T(8,128)}, f32[768,256]{1,0:T(8,128)}) custom-call(s32[1]{0:T(128)} %bitcast.me_ref, bf16[768,512]{1,0:T(8,128)(2,1)S(1)} %get-tuple-element.47.refs_0_, bf16[768,512]{1,0:T(8,128)(2,1)S(1)} %get-tuple-element.48.refs_1_, bf16[768,512]{1,0:T(8,128)(2,1)} %collective-permute-done.refs_2_, ...), custom_call_target="tpu_custom_call" | custom-call | flops 1610612736 | bytes 10223620 | tf_op jit(solution)/shard_map/expert_near/pallas_call | solution.py:74
  107.5 3.1 %collective-permute-done.4.refs_0_.refs_6_ = bf16[768,512]{1,0:T(8,128)(2,1)} collective-permute-done((bf16[768,512]{1,0:T(8,128)(2,1)}, bf16[768,512]{1,0:T(8,128)(2,1)}, u32[]{:S(2)}, u32[]{:S(2)}) %collective-permute-start.4) | collective-permute-done | bytes 786464 | tf_op jit(solution)/shard_map/ppermute | solution.py:89
  111.9 6.5 %expert_far.1 = (bf16[768,256]{1,0:T(8,128)(2,1)}, bf16[768,256]{1,0:T(8,128)(2,1)}, bf16[768,256]{1,0:T(8,128)(2,1)}, bf16[384,512]{1,0:T(8,128)(2,1)S(1)}, bf1...) custom-call(s32[1]{0:T(128)} %bitcast.me_ref, ...), custom_call_target="tpu_custom_call" | custom-call | flops 2415919104 | bytes 11403268 | tf_op jit(solution)/shard_map/expert_far/pallas_call | solution.py:74
  124.5 5.9 %collective-permute-done.6 = bf16[384,512]{1,0:T(8,128)(2,1)S(1)} collective-permute-done((bf16[384,512]{1,0:T(8,128)(2,1)S(1)}, bf16[384,512]{1,0:T(8,128)(2,1)S(1)}, u32[]{:S(2)}, u32[]{:S(2)}) %collective-permute-start.6) | collective-permute-done | bytes 393248 | tf_op jit(solution)/shard_map/ppermute | solution.py:89
  134.2 6.1 %collective-permute-done.9.ra_ref = bf16[384,512]{1,0:T(8,128)(2,1)S(1)} collective-permute-done((bf16[384,512]{1,0:T(8,128)(2,1)}, bf16[384,512]{1,0:T(8,128)(2,1)S(1)}, u32[]{:S(2)}, u32[]{:S(2)}) %collective-permute-start.9) | collective-permute-done | bytes 393248 | tf_op jit(solution)/shard_map/ppermute | solution.py:89
  140.3 4.0 %collective-permute-done.7.la_ref = bf16[384,512]{1,0:T(8,128)(2,1)S(1)} collective-permute-done((bf16[384,512]{1,0:T(8,128)(2,1)}, bf16[384,512]{1,0:T(8,128)(2,1)S(1)}, u32[]{:S(2)}, u32[]{:S(2)}) %collective-permute-start.7) | collective-permute-done | bytes 393248 | tf_op jit(solution)/shard_map/ppermute | solution.py:89
  148.3 7.5 %all-to-all-start.2 = ((bf16[64,24,256]{2,1,0:T(8,128)(2,1)}), bf16[64,24,256]{2,1,0:T(8,128)(2,1)S(1)}, u32[]{:S(2)}, u32[]{:S(2)}) async-start(bf16[64,24,256]{2,1,0:T(8,128)(2,1)} %bitcast.26), calls=%async_computation.2 | async-start | bytes 1572864 | tf_op jit(solution)/shard_map/all_to_all | solution.py:93
  155.7 12.9 %expert_grad.1 = (f32[1,2048,256]{2,1,0:T(8,128)}, f32[1,2048,256]{2,1,0:T(8,128)}, f32[1,256,2048]{2,1,0:T(8,128)}) custom-call(s32[1]{0:T(128)} %bitcast.me_ref, bf16[768,512]{1,0:T(8,128)(2,1)} %copy-done, bf16[768,512]{1,0:T(8,128)(2,1)} %copy-done.1, bf16[768,512]{1,0:T(8,128)(2,1)} %collective-permute-done.refs_2_, bf16[768,512]{1,0:T(8,128)(2,1)} %copy-done.2, ...), custom_call_target="tpu_custom_call" | custom-call | flops 2415919104 | bytes 13762564 | tf_op jit(solution)/shard_map/expert_grad/pallas_call | solution.py:74
  168.6 10.3 %all-to-all-done.2 = bf16[64,24,256]{2,1,0:T(8,128)(2,1)S(1)} async-done(((bf16[64,24,256]{2,1,0:T(8,128)(2,1)}), bf16[64,24,256]{2,1,0:T(8,128)(2,1)S(1)}, u32[]{:S(2)}, u32[]{:S(2)}) %all-to-all-start.2) | async-done | bytes 786464 | tf_op jit(solution)/shard_map/all_to_all | solution.py:93
  182.1 2.9 %collective-permute-start.15 = (bf16[192,512]{1,0:T(8,128)(2,1)S(1)}, bf16[192,512]{1,0:T(8,128)(2,1)S(1)}, u32[]{:S(2)}, u32[]{:S(2)}) collective-permute-start(bf16[192,512]{1,0:T(8,128)(2,1)S(1)} %get-tuple-element.69.p0), channel_id=1, source_target_pairs={{0,1},{1,2},{2,3},{3,0},{4,5},{5,6},{6,7},{7,4},{8,9},{9,10},{10,1... | collective-permute-start | bytes 589832 | tf_op jit(solution)/shard_map/ppermute | solution.py:89
  185.0 10.9 %all_to_all.54.p0 = bf16[8,96,128]{2,1,0:T(8,128)(2,1)S(1)} all-to-all(bf16[8,96,128]{2,1,0:T(8,128)(2,1)S(1)} %get-tuple-element.67), channel_id=1, replica_groups=mesh['z'=8,'x'=4,'c'=2,'tp'=4] {'x','c'}, dimensions={0} | all-to-all | bytes 393216 | tf_op jit(solution)/shard_map/all_to_all | solution.py:93
  195.9 4.0 %reverse.1 = (bf16[192,512]{1,0:T(8,128)(2,1)}, f32[192,512]{1,0:T(8,128)S(1)}, f32[192,512]{1,0:T(8,128)S(1)}, f32[512,128]{1,0:T(8,128)}) custom-call(s32[1]{0:T(128)} %bitcast.me_ref, bf16[192,512]{1,0:T(8,128)(2,1)S(1)} %get-tuple-element.69.p0, bf16[192,512]{1,0:T(8,128)(2,1)S(1)} %collective-permute-done.15.p1, ...), custom_call_target="tpu_custom_call" | custom-call | flops 4000000000 | bytes 5308420 | tf_op jit(solution)/shard_map/reverse/pallas_call | solution.py:74
  199.8 4.6 %all-to-all-start.5 = ((f32[64,8,128]{2,1,0:T(8,128)}), f32[64,8,128]{2,1,0:T(8,128)S(1)}, u32[]{:S(2)}, u32[]{:S(2)}) async-start(f32[64,8,128]{2,1,0:T(8,128)} %bitcast.28), calls=%async_computation.5 | async-start | bytes 524288 | tf_op jit(solution)/shard_map/all_to_all | solution.py:93
  209.3 4.5 %collective-permute-done.14.p3 = bf16[8,96,128]{2,1,0:T(8,128)(2,1)S(1)} collective-permute-done((bf16[8,96,128]{2,1,0:T(8,128)(2,1)S(1)}, bf16[8,96,128]{2,1,0:T(8,128)(2,1)S(1)}, u32[]{:S(2)}, u32[]{:S(2)}) %collective-permute-start.14) | collective-permute-done | bytes 196640 | tf_op jit(solution)/shard_map/ppermute | solution.py:89
  213.8 3.1 %collective-permute-done.13.p2 = bf16[8,96,128]{2,1,0:T(8,128)(2,1)S(1)} collective-permute-done((bf16[8,96,128]{2,1,0:T(8,128)(2,1)S(1)}, bf16[8,96,128]{2,1,0:T(8,128)(2,1)S(1)}, u32[]{:S(2)}, u32[]{:S(2)}) %collective-permute-start.13) | collective-permute-done | bytes 196640 | tf_op jit(solution)/shard_map/ppermute | solution.py:89
  218.7 7.0 %all-to-all-start.4 = ((bf16[8,32,512]{2,1,0:T(8,128)(2,1)}), bf16[8,32,512]{2,1,0:T(8,128)(2,1)S(1)}, u32[]{:S(2)}, u32[]{:S(2)}) async-start(bf16[8,32,512]{2,1,0:T(8,128)(2,1)} %bitcast.27), calls=%async_computation.4 | async-start | bytes 524288 | tf_op jit(solution)/shard_map/all_to_all | solution.py:93
  228.4 9.4 %all-to-all-done.4 = bf16[8,32,512]{2,1,0:T(8,128)(2,1)S(1)} async-done(((bf16[8,32,512]{2,1,0:T(8,128)(2,1)}), bf16[8,32,512]{2,1,0:T(8,128)(2,1)S(1)}, u32[]{:S(2)}, u32[]{:S(2)}) %all-to-all-start.4) | async-done | bytes 262176 | tf_op jit(solution)/shard_map/all_to_all | solution.py:93
  (57 shorter events, 41.8 us)
Async XLA Ops:
  4.6 52.2 %all-to-all-start = ((bf16[64,24,512]{2,1,0:T(8,128)(2,1)}), bf16[64,24,512]{2,1,0:T(8,128)(2,1)S(1)}, u32[]{:S(2)}, u32[]{:S(2)}) async-start(bf16[64,24,512]{2,1,0:T(8,128)(2,1)} %bitcast.19), calls=%async_computation | async-start | bytes 3145728 | tf_op jit(solution)/shard_map/all_to_all | solution.py:93
  58.2 49.2 %copy-start = (bf16[768,512]{1,0:T(8,128)(2,1)}, bf16[768,512]{1,0:T(8,128)(2,1)S(1)}, u32[]{:S(2)}) copy-start(bf16[768,512]{1,0:T(8,128)(2,1)S(1)} %get-tuple-element.47.refs_0_) | copy-start | bytes 2359300
  58.3 20.6 %collective-permute-start = (bf16[768,512]{1,0:T(8,128)(2,1)S(1)}, bf16[768,512]{1,0:T(8,128)(2,1)}, u32[]{:S(2)}, u32[]{:S(2)}) collective-permute-start(bf16[768,512]{1,0:T(8,128)(2,1)S(1)} %get-tuple-element.47.refs_0_), channel_id=1, source_target_pairs={{0,1},{1,2},{2,3},{3,0},{4,5},{5,6},{6,7},{7,4},{8,9},{9,10},{10,1... | collective-permute-start | bytes 2359304 | tf_op jit(solution)/shard_map/ppermute | solution.py:89
  58.6 21.7 %collective-permute-start.3 = (bf16[768,512]{1,0:T(8,128)(2,1)S(1)}, bf16[768,512]{1,0:T(8,128)(2,1)}, u32[]{:S(2)}, u32[]{:S(2)}) collective-permute-start(bf16[768,512]{1,0:T(8,128)(2,1)S(1)} %get-tuple-element.48.refs_1_), channel_id=1, source_target_pairs={{0,3},{1,0},{2,1},{3,2},{4,7},{5,4},{6,5},{7,6},{8,11},{9,8},{10,9... | collective-permute-start | bytes 2359304 | tf_op jit(solution)/shard_map/ppermute | solution.py:89
  60.4 35.2 %collective-permute-start.1 = (bf16[768,512]{1,0:T(8,128)(2,1)S(1)}, bf16[768,512]{1,0:T(8,128)(2,1)S(1)}, u32[]{:S(2)}, u32[]{:S(2)}) collective-permute-start(bf16[768,512]{1,0:T(8,128)(2,1)S(1)} %get-tuple-element.48.refs_1_), channel_id=1, source_target_pairs={{0,1},{1,2},{2,3},{3,0},{4,5},{5,6},{6,7},{7,4},{8,9},{9,10},{10,1... | collective-permute-start | bytes 2359304 | tf_op jit(solution)/shard_map/ppermute | solution.py:89
  61.8 39.0 %collective-permute-start.2 = (bf16[768,512]{1,0:T(8,128)(2,1)S(1)}, bf16[768,512]{1,0:T(8,128)(2,1)}, u32[]{:S(2)}, u32[]{:S(2)}) collective-permute-start(bf16[768,512]{1,0:T(8,128)(2,1)S(1)} %get-tuple-element.47.refs_0_), channel_id=1, source_target_pairs={{0,3},{1,0},{2,1},{3,2},{4,7},{5,4},{6,5},{7,6},{8,11},{9,8},{10,9... | collective-permute-start | bytes 2359304 | tf_op jit(solution)/shard_map/ppermute | solution.py:89
  78.9 31.7 %collective-permute-start.4 = (bf16[768,512]{1,0:T(8,128)(2,1)}, bf16[768,512]{1,0:T(8,128)(2,1)}, u32[]{:S(2)}, u32[]{:S(2)}) collective-permute-start(bf16[768,512]{1,0:T(8,128)(2,1)} %collective-permute-done.refs_2_), channel_id=1, source_target_pairs={{0,1},{1,2},{2,3},{3,0},{4,5},{5,6},{6,7},{7,4},{8,9},{9,10},{10,1... | collective-permute-start | bytes 2359304 | tf_op jit(solution)/shard_map/ppermute | solution.py:89
  80.3 31.6 %collective-permute-start.5 = (bf16[768,512]{1,0:T(8,128)(2,1)}, bf16[768,512]{1,0:T(8,128)(2,1)}, u32[]{:S(2)}, u32[]{:S(2)}) collective-permute-start(bf16[768,512]{1,0:T(8,128)(2,1)} %collective-permute-done.3.refs_5_), channel_id=1, source_target_pairs={{0,3},{1,0},{2,1},{3,2},{4,7},{5,4},{6,5},{7,6},{8,11},{9,8},{10,9... | collective-permute-start | bytes 2359304 | tf_op jit(solution)/shard_map/ppermute | solution.py:89
  96.5 37.7 %all-to-all-start.1 = ((bf16[8,192,512]{2,1,0:T(8,128)(2,1)}), bf16[8,192,512]{2,1,0:T(8,128)(2,1)S(1)}, u32[]{:S(2)}, u32[]{:S(2)}) async-start(bf16[8,192,512]{2,1,0:T(8,128)(2,1)} %get-tuple-element.54), calls=%async_computation.1 | async-start | bytes 3145728 | tf_op jit(solution)/shard_map/all_to_all | solution.py:93
  118.5 12.0 %collective-permute-start.6 = (bf16[384,512]{1,0:T(8,128)(2,1)S(1)}, bf16[384,512]{1,0:T(8,128)(2,1)S(1)}, u32[]{:S(2)}, u32[]{:S(2)}) collective-permute-start(bf16[384,512]{1,0:T(8,128)(2,1)S(1)} %get-tuple-element.57), channel_id=1, source_target_pairs={{0,1},{1,2},{2,3},{3,0},{4,5},{5,6},{6,7},{7,4},{8,9},{9,10},{10,1... | collective-permute-start | bytes 1179656 | tf_op jit(solution)/shard_map/ppermute | solution.py:89
  118.7 14.1 %collective-permute-start.10 = (bf16[384,512]{1,0:T(8,128)(2,1)S(1)}, bf16[384,512]{1,0:T(8,128)(2,1)S(1)}, u32[]{:S(2)}, u32[]{:S(2)}) collective-permute-start(bf16[384,512]{1,0:T(8,128)(2,1)S(1)} %get-tuple-element.59), channel_id=1, source_target_pairs={{0,3},{1,0},{2,1},{3,2},{4,7},{5,4},{6,5},{7,6},{8,11},{9,8},{10,9... | collective-permute-start | bytes 1179656 | tf_op jit(solution)/shard_map/ppermute | solution.py:89
  121.3 19.0 %collective-permute-start.9 = (bf16[384,512]{1,0:T(8,128)(2,1)}, bf16[384,512]{1,0:T(8,128)(2,1)S(1)}, u32[]{:S(2)}, u32[]{:S(2)}) collective-permute-start(bf16[384,512]{1,0:T(8,128)(2,1)} %slice.14), channel_id=1, source_target_pairs={{0,3},{1,0},{2,1},{3,2},{4,7},{5,4},{6,5},{7,6},{8,11},{9,8},{10,9... | collective-permute-start | bytes 1179656 | tf_op jit(solution)/shard_map/ppermute | solution.py:89
  121.7 18.6 %collective-permute-start.8 = (bf16[384,512]{1,0:T(8,128)(2,1)S(1)}, bf16[384,512]{1,0:T(8,128)(2,1)S(1)}, u32[]{:S(2)}, u32[]{:S(2)}) collective-permute-start(bf16[384,512]{1,0:T(8,128)(2,1)S(1)} %slice.13), channel_id=1, source_target_pairs={{0,1},{1,2},{2,3},{3,0},{4,5},{5,6},{6,7},{7,4},{8,9},{9,10},{10,1... | collective-permute-start | bytes 1179656 | tf_op jit(solution)/shard_map/ppermute | solution.py:89
  131.3 13.0 %collective-permute-start.7 = (bf16[384,512]{1,0:T(8,128)(2,1)}, bf16[384,512]{1,0:T(8,128)(2,1)S(1)}, u32[]{:S(2)}, u32[]{:S(2)}) collective-permute-start(bf16[384,512]{1,0:T(8,128)(2,1)} %add_convert_fusion.1), channel_id=1, source_target_pairs={{0,1},{1,2},{2,3},{3,0},{4,5},{5,6},{6,7},{7,4},{8,9},{9,10},{10,1... | collective-permute-start | bytes 1179656 | tf_op jit(solution)/shard_map/ppermute | solution.py:89
  133.6 12.1 %collective-permute-start.11 = (bf16[384,512]{1,0:T(8,128)(2,1)}, bf16[384,512]{1,0:T(8,128)(2,1)S(1)}, u32[]{:S(2)}, u32[]{:S(2)}) collective-permute-start(bf16[384,512]{1,0:T(8,128)(2,1)} %add_convert_fusion), channel_id=1, source_target_pairs={{0,3},{1,0},{2,1},{3,2},{4,7},{5,4},{6,5},{7,6},{8,11},{9,8},{10,9... | collective-permute-start | bytes 1179656 | tf_op jit(solution)/shard_map/ppermute | solution.py:89
  148.3 30.7 %all-to-all-start.2 = ((bf16[64,24,256]{2,1,0:T(8,128)(2,1)}), bf16[64,24,256]{2,1,0:T(8,128)(2,1)S(1)}, u32[]{:S(2)}, u32[]{:S(2)}) async-start(bf16[64,24,256]{2,1,0:T(8,128)(2,1)} %bitcast.26), calls=%async_computation.2 | async-start | bytes 1572864 | tf_op jit(solution)/shard_map/all_to_all | solution.py:93
  180.9 14.9 %collective-permute-start.17 = (bf16[192,512]{1,0:T(8,128)(2,1)S(1)}, bf16[192,512]{1,0:T(8,128)(2,1)S(1)}, u32[]{:S(2)}, u32[]{:S(2)}) collective-permute-start(bf16[192,512]{1,0:T(8,128)(2,1)S(1)} %get-tuple-element.69.p0), channel_id=1, source_target_pairs={{0,2},{1,3},{2,0},{3,1},{4,6},{5,7},{6,4},{7,5},{8,10},{9,11},{10,... | collective-permute-start | bytes 589832 | tf_op jit(solution)/shard_map/ppermute | solution.py:89
  181.7 14.1 %collective-permute-start.16 = (bf16[192,512]{1,0:T(8,128)(2,1)S(1)}, bf16[192,512]{1,0:T(8,128)(2,1)S(1)}, u32[]{:S(2)}, u32[]{:S(2)}) collective-permute-start(bf16[192,512]{1,0:T(8,128)(2,1)S(1)} %get-tuple-element.69.p0), channel_id=1, source_target_pairs={{0,3},{1,0},{2,1},{3,2},{4,7},{5,4},{6,5},{7,6},{8,11},{9,8},{10,9... | collective-permute-start | bytes 589832 | tf_op jit(solution)/shard_map/ppermute | solution.py:89
  182.1 13.7 %collective-permute-start.15 = (bf16[192,512]{1,0:T(8,128)(2,1)S(1)}, bf16[192,512]{1,0:T(8,128)(2,1)S(1)}, u32[]{:S(2)}, u32[]{:S(2)}) collective-permute-start(bf16[192,512]{1,0:T(8,128)(2,1)S(1)} %get-tuple-element.69.p0), channel_id=1, source_target_pairs={{0,1},{1,2},{2,3},{3,0},{4,5},{5,6},{6,7},{7,4},{8,9},{9,10},{10,1... | collective-permute-start | bytes 589832 | tf_op jit(solution)/shard_map/ppermute | solution.py:89
  199.8 18.9 %all-to-all-start.5 = ((f32[64,8,128]{2,1,0:T(8,128)}), f32[64,8,128]{2,1,0:T(8,128)S(1)}, u32[]{:S(2)}, u32[]{:S(2)}) async-start(f32[64,8,128]{2,1,0:T(8,128)} %bitcast.28), calls=%async_computation.5 | async-start | bytes 524288 | tf_op jit(solution)/shard_map/all_to_all | solution.py:93
  204.4 9.4 %collective-permute-start.14 = (bf16[8,96,128]{2,1,0:T(8,128)(2,1)S(1)}, bf16[8,96,128]{2,1,0:T(8,128)(2,1)S(1)}, u32[]{:S(2)}, u32[]{:S(2)}) collective-permute-start(bf16[8,96,128]{2,1,0:T(8,128)(2,1)S(1)} %all_to_all.54.p0), channel_id=1, source_target_pairs={{0,2},{1,3},{2,0},{3,1},{4,6},{5,7},{6,4},{7,5},{8,10},{9,11},{10,... | collective-permute-start | bytes 589832 | tf_op jit(solution)/shard_map/ppermute | solution.py:89
  206.1 10.9 %collective-permute-start.13 = (bf16[8,96,128]{2,1,0:T(8,128)(2,1)S(1)}, bf16[8,96,128]{2,1,0:T(8,128)(2,1)S(1)}, u32[]{:S(2)}, u32[]{:S(2)}) collective-permute-start(bf16[8,96,128]{2,1,0:T(8,128)(2,1)S(1)} %all_to_all.54.p0), channel_id=1, source_target_pairs={{0,3},{1,0},{2,1},{3,2},{4,7},{5,4},{6,5},{7,6},{8,11},{9,8},{10,9... | collective-permute-start | bytes 589832 | tf_op jit(solution)/shard_map/ppermute | solution.py:89
  206.5 10.5 %collective-permute-start.12 = (bf16[8,96,128]{2,1,0:T(8,128)(2,1)S(1)}, bf16[8,96,128]{2,1,0:T(8,128)(2,1)S(1)}, u32[]{:S(2)}, u32[]{:S(2)}) collective-permute-start(bf16[8,96,128]{2,1,0:T(8,128)(2,1)S(1)} %all_to_all.54.p0), channel_id=1, source_target_pairs={{0,1},{1,2},{2,3},{3,0},{4,5},{5,6},{6,7},{7,4},{8,9},{9,10},{10,1... | collective-permute-start | bytes 589832 | tf_op jit(solution)/shard_map/ppermute | solution.py:89
  218.7 19.1 %all-to-all-start.4 = ((bf16[8,32,512]{2,1,0:T(8,128)(2,1)}), bf16[8,32,512]{2,1,0:T(8,128)(2,1)S(1)}, u32[]{:S(2)}, u32[]{:S(2)}) async-start(bf16[8,32,512]{2,1,0:T(8,128)(2,1)} %bitcast.27), calls=%async_computation.4 | async-start | bytes 524288 | tf_op jit(solution)/shard_map/all_to_all | solution.py:93
  (6 other events, 91.7 us)

commit v4 on v3

--- a/solution.py
+++ b/solution.py
@@ -212,7 +212,8 @@
 def expert_far_kernel(me_ref, *refs):
     gate_ref, up_ref, down_ref = refs[2:5]
     near_refs = refs[5:8]
-    hidden_ref, d_up_ref, d_linear_ref, far_a, far_b, left_ref, right_ref, own_ref = refs[8:]
+    hidden_ref, d_up_ref, d_linear_ref = refs[8:11]
+    far_a, far_b, left_a, left_b, right_a, right_b, own_ref = refs[11:]
     for h in range(2):
         rows = slice(h * HALF, (h + 1) * HALF)
         terms = hidden_terms(me_ref, refs[:2], STEPS[3:], gate_ref, up_ref, down_ref, h)
@@ -232,11 +233,11 @@
         ).astype(BF16)
 
     top, low = (slice(0, HALF), slice(HALF, ROWS))
-    far_a[...] = part(top, 2)
-    far_b[...] = part(low, 2)
-    for rows in (top, low):
-        left_ref[rows, :] = part(rows, 3)
-        right_ref[rows, :] = part(rows, 1)
+    halves = ((top, far_a, left_a, right_a), (low, far_b, left_b, right_b))
+    for rows, far, left, right in halves:
+        far[...] = part(rows, 2)
+        left[...] = part(rows, 3)
+        right[...] = part(rows, 1)
         own_ref[rows, :] = part(rows, 0)
 
 
@@ -571,10 +572,10 @@
         smem=1,
     )
     merged_x = exchange(after(merged, pieces[3]), XC)
-    hidden, d_up, d_linear, far_a, far_b, left, right, own = local(
+    hidden, d_up, d_linear, far_a, far_b, left_top, left_low, right_top, right_low, own = local(
         expert_far_kernel,
         "expert_far",
-        (hid, hid, hid, *map(Near, (piece, piece, full, full)), full),
+        (hid, hid, hid, *map(Near, (piece,) * 6), full),
         3 * unit,
         me,
         *map(Near, pieces[6:]),
@@ -585,10 +586,10 @@
         smem=1,
     )
     over_a, over_b = (shift(far_a, "tp", 1), shift(far_b, "tp", -1))
-    right_b, left_a = (shift(right[HALF:], "tp", 1), shift(left[:HALF], "tp", -1))
+    right_b, left_a = (shift(right_low, "tp", 1), shift(left_top, "tp", -1))
     add = lambda u, v: (u.astype(F32) + v.astype(F32)).astype(BF16)
-    right_a = shift(add(right[:HALF], over_a), "tp", 1)
-    left_b = shift(add(left[HALF:], over_b), "tp", -1)
+    right_a = shift(add(right_top, over_a), "tp", 1)
+    left_b = shift(add(left_low, over_b), "tp", -1)
     returned = local(
         spread_kernel,
         "spread",

time: 240 us -> 240 us (level)
  transfers between devices with their start and end apart: 23 -> 23, of which waited for: 13 -> 14; matrix products, arithmetic and copies ran while one was open for 2% -> 2% of each run, Pallas kernels for 16% -> 15%
where the time goes in v4:
time: 240 us; the launch traced here: 239 us
  waiting for transfers between devices  113 us (47%)
  starting transfers between devices  56.6 us (24%)
  Pallas kernels  51 us (21%)
  blocking collectives  10.9 us (5%)
  local copies, waits for them, and re-layouts  3.57 us (1%)
  other arithmetic  2.96 us (1%)
    ppermute x18, waiting for transfers between devices, shift(): return lax.ppermute(value, axis, [(i, (i + by) % n) for i in range(n)])  62.8 us
    pallas_call x12, Pallas kernels, local(): pl.pallas_call(kernel, name=name, out_shape=result(outs) if single else t...  51 us
    all_to_all x5, waiting for transfers between devices, exchange(): return lax.all_to_all(value, axes, 0, 0, tiled=True)  50.1 us
    all_to_all x5, starting transfers between devices, exchange(): return lax.all_to_all(value, axes, 0, 0, tiled=True)  35.4 us
    ppermute x18, starting transfers between devices, shift(): return lax.ppermute(value, axis, [(i, (i + by) % n) for i in range(n)])  21.2 us
    all_to_all x1, blocking collectives, exchange(): return lax.all_to_all(value, axes, 0, 0, tiled=True)  10.9 us
  transfers between devices with their start and end apart: 23, of which 14 were waited for; matrix products, arithmetic and copies ran while one was open for 2% of the time, Pallas kernels for 15%

profile of v4, /device:TPU:24, one launch (start us, length us, event | category | flops | bytes accessed | tf_op | source)
XLA Modules:
  0.0 238.7 jit_solution(8901040227807826162)
XLA Ops:
  0.6 4.0 %route.1 = bf16[1536,512]{1,0:T(8,128)(2,1)} custom-call(s32[2,192]{1,0:T(2,128)} %bitcast.29, f32[2,192]{1,0:T(2,128)} %bitcast.32, bf16[192,512]{1,0:T(8,128)(2,1)} %mixed_ref.1, bf16[192,512]{1,0:T(8,128)(2,1)} %d_out_ref.3), custom_call_target="tpu_custom_call" | custom-call | flops 1300000000 | bytes 1969152 | tf_op jit(solution)/shard_map/route/pallas_call | solution.py:74
  4.6 12.1 %all-to-all-start = ((bf16[64,24,512]{2,1,0:T(8,128)(2,1)}), bf16[64,24,512]{2,1,0:T(8,128)(2,1)S(1)}, u32[]{:S(2)}, u32[]{:S(2)}) async-start(bf16[64,24,512]{2,1,0:T(8,128)(2,1)} %bitcast.19), calls=%async_computation | async-start | bytes 3145728 | tf_op jit(solution)/shard_map/all_to_all | solution.py:93
  20.8 5.6 %forward.1 = (bf16[8,192,512]{2,1,0:T(8,128)(2,1)}, f32[192,512]{1,0:T(8,128)}, f32[192,512]{1,0:T(8,128)}, f32[192,512]{1,0:T(8,128)}, f32[192,512]{1,0:T(8,128...) custom-call(bf16[192,512]{1,0:T(8,128)(2,1)} %conv_ref, bf16[192,512]{1,0:T(8,128)(2,1)} %gate_ref.1, f32[1,512]{1,0:T(1,128)} %start_ref.1, ...), custom_call_target="tpu_custom_call" | custom-call | flops 6000000000 | bytes 4592384 | tf_op jit(solution)/shard_map/forward/pallas_call | solution.py:74
  26.4 30.4 %all-to-all-done = bf16[64,24,512]{2,1,0:T(8,128)(2,1)S(1)} async-done(((bf16[64,24,512]{2,1,0:T(8,128)(2,1)}), bf16[64,24,512]{2,1,0:T(8,128)(2,1)S(1)}, u32[]{:S(2)}, u32[]{:S(2)}) %all-to-all-start) | async-done | bytes 1572896 | tf_op jit(solution)/shard_map/all_to_all | solution.py:93
  62.4 16.5 %collective-permute-done.refs_2_ = bf16[768,512]{1,0:T(8,128)(2,1)} collective-permute-done((bf16[768,512]{1,0:T(8,128)(2,1)S(1)}, bf16[768,512]{1,0:T(8,128)(2,1)}, u32[]{:S(2)}, u32[]{:S(2)}) %collective-permute-start) | collective-permute-done | bytes 786464 | tf_op jit(solution)/shard_map/ppermute | solution.py:89
  80.9 14.7 %collective-permute-done.1.refs_3_ = bf16[768,512]{1,0:T(8,128)(2,1)S(1)} collective-permute-done((bf16[768,512]{1,0:T(8,128)(2,1)S(1)}, bf16[768,512]{1,0:T(8,128)(2,1)S(1)}, u32[]{:S(2)}, u32[]{:S(2)}) %collective-permute-start.1) | collective-permute-done | bytes 786464 | tf_op jit(solution)/shard_map/ppermute | solution.py:89
  96.5 4.3 %all-to-all-start.1 = ((bf16[8,192,512]{2,1,0:T(8,128)(2,1)}), bf16[8,192,512]{2,1,0:T(8,128)(2,1)S(1)}, u32[]{:S(2)}, u32[]{:S(2)}) async-start(bf16[8,192,512]{2,1,0:T(8,128)(2,1)} %get-tuple-element.56), calls=%async_computation.1 | async-start | bytes 3145728 | tf_op jit(solution)/shard_map/all_to_all | solution.py:93
  101.9 5.6 %expert_near.1 = (f32[768,256]{1,0:T(8,128)}, f32[768,256]{1,0:T(8,128)}, f32[768,256]{1,0:T(8,128)}) custom-call(s32[1]{0:T(128)} %bitcast.me_ref, bf16[768,512]{1,0:T(8,128)(2,1)S(1)} %get-tuple-element.49.refs_0_, bf16[768,512]{1,0:T(8,128)(2,1)S(1)} %get-tuple-element.50.refs_1_, bf16[768,512]{1,0:T(8,128)(2,1)} %collective-permute-done.refs_2_, ...), custom_call_target="tpu_custom_call" | custom-call | flops 1610612736 | bytes 10223620 | tf_op jit(solution)/shard_map/expert_near/pallas_call | solution.py:74
  107.5 3.1 %collective-permute-done.4.refs_0_.refs_6_ = bf16[768,512]{1,0:T(8,128)(2,1)} collective-permute-done((bf16[768,512]{1,0:T(8,128)(2,1)}, bf16[768,512]{1,0:T(8,128)(2,1)}, u32[]{:S(2)}, u32[]{:S(2)}) %collective-permute-start.4) | collective-permute-done | bytes 786464 | tf_op jit(solution)/shard_map/ppermute | solution.py:89
  111.9 6.5 %expert_far.1 = (bf16[768,256]{1,0:T(8,128)(2,1)}, bf16[768,256]{1,0:T(8,128)(2,1)}, bf16[768,256]{1,0:T(8,128)(2,1)}, bf16[384,512]{1,0:T(8,128)(2,1)S(1)}, bf1...) custom-call(s32[1]{0:T(128)} %bitcast.me_ref, ...), custom_call_target="tpu_custom_call" | custom-call | flops 2415919104 | bytes 11403268 | tf_op jit(solution)/shard_map/expert_far/pallas_call | solution.py:74
  122.5 7.9 %collective-permute-done.6 = bf16[384,512]{1,0:T(8,128)(2,1)S(1)} collective-permute-done((bf16[384,512]{1,0:T(8,128)(2,1)S(1)}, bf16[384,512]{1,0:T(8,128)(2,1)S(1)}, u32[]{:S(2)}, u32[]{:S(2)}) %collective-permute-start.6) | collective-permute-done | bytes 393248 | tf_op jit(solution)/shard_map/ppermute | solution.py:89
  134.2 4.7 %collective-permute-done.8.lb_ref = bf16[384,512]{1,0:T(8,128)(2,1)S(1)} collective-permute-done((bf16[384,512]{1,0:T(8,128)(2,1)S(1)}, bf16[384,512]{1,0:T(8,128)(2,1)S(1)}, u32[]{:S(2)}, u32[]{:S(2)}) %collective-permute-start.8) | collective-permute-done | bytes 393248 | tf_op jit(solution)/shard_map/ppermute | solution.py:89
  140.3 4.0 %collective-permute-done.7.la_ref = bf16[384,512]{1,0:T(8,128)(2,1)S(1)} collective-permute-done((bf16[384,512]{1,0:T(8,128)(2,1)}, bf16[384,512]{1,0:T(8,128)(2,1)S(1)}, u32[]{:S(2)}, u32[]{:S(2)}) %collective-permute-start.7) | collective-permute-done | bytes 393248 | tf_op jit(solution)/shard_map/ppermute | solution.py:89
  148.5 7.5 %all-to-all-start.2 = ((bf16[64,24,256]{2,1,0:T(8,128)(2,1)}), bf16[64,24,256]{2,1,0:T(8,128)(2,1)S(1)}, u32[]{:S(2)}, u32[]{:S(2)}) async-start(bf16[64,24,256]{2,1,0:T(8,128)(2,1)} %bitcast.26), calls=%async_computation.2 | async-start | bytes 1572864 | tf_op jit(solution)/shard_map/all_to_all | solution.py:93
  156.0 12.9 %expert_grad.1 = (f32[1,2048,256]{2,1,0:T(8,128)}, f32[1,2048,256]{2,1,0:T(8,128)}, f32[1,256,2048]{2,1,0:T(8,128)}) custom-call(s32[1]{0:T(128)} %bitcast.me_ref, bf16[768,512]{1,0:T(8,128)(2,1)} %copy-done, bf16[768,512]{1,0:T(8,128)(2,1)} %copy-done.1, bf16[768,512]{1,0:T(8,128)(2,1)} %collective-permute-done.refs_2_, bf16[768,512]{1,0:T(8,128)(2,1)} %copy-done.2, ...), custom_call_target="tpu_custom_call" | custom-call | flops 2415919104 | bytes 13762564 | tf_op jit(solution)/shard_map/expert_grad/pallas_call | solution.py:74
  168.9 10.3 %all-to-all-done.2 = bf16[64,24,256]{2,1,0:T(8,128)(2,1)S(1)} async-done(((bf16[64,24,256]{2,1,0:T(8,128)(2,1)}), bf16[64,24,256]{2,1,0:T(8,128)(2,1)S(1)}, u32[]{:S(2)}, u32[]{:S(2)}) %all-to-all-start.2) | async-done | bytes 786464 | tf_op jit(solution)/shard_map/all_to_all | solution.py:93
  182.3 3.0 %collective-permute-start.15 = (bf16[192,512]{1,0:T(8,128)(2,1)S(1)}, bf16[192,512]{1,0:T(8,128)(2,1)S(1)}, u32[]{:S(2)}, u32[]{:S(2)}) collective-permute-start(bf16[192,512]{1,0:T(8,128)(2,1)S(1)} %get-tuple-element.73.p0), channel_id=1, source_target_pairs={{0,1},{1,2},{2,3},{3,0},{4,5},{5,6},{6,7},{7,4},{8,9},{9,10},{10,1... | collective-permute-start | bytes 589832 | tf_op jit(solution)/shard_map/ppermute | solution.py:89
  185.2 10.9 %all_to_all.54.p0 = bf16[8,96,128]{2,1,0:T(8,128)(2,1)S(1)} all-to-all(bf16[8,96,128]{2,1,0:T(8,128)(2,1)S(1)} %get-tuple-element.71), channel_id=1, replica_groups=mesh['z'=8,'x'=4,'c'=2,'tp'=4] {'x','c'}, dimensions={0} | all-to-all | bytes 393216 | tf_op jit(solution)/shard_map/all_to_all | solution.py:93
  196.1 4.0 %reverse.1 = (bf16[192,512]{1,0:T(8,128)(2,1)}, f32[192,512]{1,0:T(8,128)S(1)}, f32[192,512]{1,0:T(8,128)S(1)}, f32[512,128]{1,0:T(8,128)}) custom-call(s32[1]{0:T(128)} %bitcast.me_ref, bf16[192,512]{1,0:T(8,128)(2,1)S(1)} %get-tuple-element.73.p0, bf16[192,512]{1,0:T(8,128)(2,1)S(1)} %collective-permute-done.15.p1, ...), custom_call_target="tpu_custom_call" | custom-call | flops 4000000000 | bytes 5308420 | tf_op jit(solution)/shard_map/reverse/pallas_call | solution.py:74
  200.0 4.6 %all-to-all-start.5 = ((f32[64,8,128]{2,1,0:T(8,128)}), f32[64,8,128]{2,1,0:T(8,128)S(1)}, u32[]{:S(2)}, u32[]{:S(2)}) async-start(f32[64,8,128]{2,1,0:T(8,128)} %bitcast.28), calls=%async_computation.5 | async-start | bytes 524288 | tf_op jit(solution)/shard_map/all_to_all | solution.py:93
  209.5 4.5 %collective-permute-done.14.p3 = bf16[8,96,128]{2,1,0:T(8,128)(2,1)S(1)} collective-permute-done((bf16[8,96,128]{2,1,0:T(8,128)(2,1)S(1)}, bf16[8,96,128]{2,1,0:T(8,128)(2,1)S(1)}, u32[]{:S(2)}, u32[]{:S(2)}) %collective-permute-start.14) | collective-permute-done | bytes 196640 | tf_op jit(solution)/shard_map/ppermute | solution.py:89
  214.1 3.1 %collective-permute-done.13.p2 = bf16[8,96,128]{2,1,0:T(8,128)(2,1)S(1)} collective-permute-done((bf16[8,96,128]{2,1,0:T(8,128)(2,1)S(1)}, bf16[8,96,128]{2,1,0:T(8,128)(2,1)S(1)}, u32[]{:S(2)}, u32[]{:S(2)}) %collective-permute-start.13) | collective-permute-done | bytes 196640 | tf_op jit(solution)/shard_map/ppermute | solution.py:89
  219.0 7.0 %all-to-all-start.4 = ((bf16[8,32,512]{2,1,0:T(8,128)(2,1)}), bf16[8,32,512]{2,1,0:T(8,128)(2,1)S(1)}, u32[]{:S(2)}, u32[]{:S(2)}) async-start(bf16[8,32,512]{2,1,0:T(8,128)(2,1)} %bitcast.27), calls=%async_computation.4 | async-start | bytes 524288 | tf_op jit(solution)/shard_map/all_to_all | solution.py:93
  228.7 9.4 %all-to-all-done.4 = bf16[8,32,512]{2,1,0:T(8,128)(2,1)S(1)} async-done(((bf16[8,32,512]{2,1,0:T(8,128)(2,1)}), bf16[8,32,512]{2,1,0:T(8,128)(2,1)S(1)}, u32[]{:S(2)}, u32[]{:S(2)}) %all-to-all-start.4) | async-done | bytes 262176 | tf_op jit(solution)/shard_map/all_to_all | solution.py:93
  (55 shorter events, 41.4 us)
Async XLA Ops:
  4.6 52.2 %all-to-all-start = ((bf16[64,24,512]{2,1,0:T(8,128)(2,1)}), bf16[64,24,512]{2,1,0:T(8,128)(2,1)S(1)}, u32[]{:S(2)}, u32[]{:S(2)}) async-start(bf16[64,24,512]{2,1,0:T(8,128)(2,1)} %bitcast.19), calls=%async_computation | async-start | bytes 3145728 | tf_op jit(solution)/shard_map/all_to_all | solution.py:93
  58.2 49.2 %copy-start = (bf16[768,512]{1,0:T(8,128)(2,1)}, bf16[768,512]{1,0:T(8,128)(2,1)S(1)}, u32[]{:S(2)}) copy-start(bf16[768,512]{1,0:T(8,128)(2,1)S(1)} %get-tuple-element.49.refs_0_) | copy-start | bytes 2359300
  58.3 20.6 %collective-permute-start = (bf16[768,512]{1,0:T(8,128)(2,1)S(1)}, bf16[768,512]{1,0:T(8,128)(2,1)}, u32[]{:S(2)}, u32[]{:S(2)}) collective-permute-start(bf16[768,512]{1,0:T(8,128)(2,1)S(1)} %get-tuple-element.49.refs_0_), channel_id=1, source_target_pairs={{0,1},{1,2},{2,3},{3,0},{4,5},{5,6},{6,7},{7,4},{8,9},{9,10},{10,1... | collective-permute-start | bytes 2359304 | tf_op jit(solution)/shard_map/ppermute | solution.py:89
  58.6 21.7 %collective-permute-start.3 = (bf16[768,512]{1,0:T(8,128)(2,1)S(1)}, bf16[768,512]{1,0:T(8,128)(2,1)}, u32[]{:S(2)}, u32[]{:S(2)}) collective-permute-start(bf16[768,512]{1,0:T(8,128)(2,1)S(1)} %get-tuple-element.50.refs_1_), channel_id=1, source_target_pairs={{0,3},{1,0},{2,1},{3,2},{4,7},{5,4},{6,5},{7,6},{8,11},{9,8},{10,9... | collective-permute-start | bytes 2359304 | tf_op jit(solution)/shard_map/ppermute | solution.py:89
  60.4 35.2 %collective-permute-start.1 = (bf16[768,512]{1,0:T(8,128)(2,1)S(1)}, bf16[768,512]{1,0:T(8,128)(2,1)S(1)}, u32[]{:S(2)}, u32[]{:S(2)}) collective-permute-start(bf16[768,512]{1,0:T(8,128)(2,1)S(1)} %get-tuple-element.50.refs_1_), channel_id=1, source_target_pairs={{0,1},{1,2},{2,3},{3,0},{4,5},{5,6},{6,7},{7,4},{8,9},{9,10},{10,1... | collective-permute-start | bytes 2359304 | tf_op jit(solution)/shard_map/ppermute | solution.py:89
  61.8 39.0 %collective-permute-start.2 = (bf16[768,512]{1,0:T(8,128)(2,1)S(1)}, bf16[768,512]{1,0:T(8,128)(2,1)}, u32[]{:S(2)}, u32[]{:S(2)}) collective-permute-start(bf16[768,512]{1,0:T(8,128)(2,1)S(1)} %get-tuple-element.49.refs_0_), channel_id=1, source_target_pairs={{0,3},{1,0},{2,1},{3,2},{4,7},{5,4},{6,5},{7,6},{8,11},{9,8},{10,9... | collective-permute-start | bytes 2359304 | tf_op jit(solution)/shard_map/ppermute | solution.py:89
  78.9 31.7 %collective-permute-start.4 = (bf16[768,512]{1,0:T(8,128)(2,1)}, bf16[768,512]{1,0:T(8,128)(2,1)}, u32[]{:S(2)}, u32[]{:S(2)}) collective-permute-start(bf16[768,512]{1,0:T(8,128)(2,1)} %collective-permute-done.refs_2_), channel_id=1, source_target_pairs={{0,1},{1,2},{2,3},{3,0},{4,5},{5,6},{6,7},{7,4},{8,9},{9,10},{10,1... | collective-permute-start | bytes 2359304 | tf_op jit(solution)/shard_map/ppermute | solution.py:89
  80.3 31.6 %collective-permute-start.5 = (bf16[768,512]{1,0:T(8,128)(2,1)}, bf16[768,512]{1,0:T(8,128)(2,1)}, u32[]{:S(2)}, u32[]{:S(2)}) collective-permute-start(bf16[768,512]{1,0:T(8,128)(2,1)} %collective-permute-done.3.refs_5_), channel_id=1, source_target_pairs={{0,3},{1,0},{2,1},{3,2},{4,7},{5,4},{6,5},{7,6},{8,11},{9,8},{10,9... | collective-permute-start | bytes 2359304 | tf_op jit(solution)/shard_map/ppermute | solution.py:89
  96.5 37.7 %all-to-all-start.1 = ((bf16[8,192,512]{2,1,0:T(8,128)(2,1)}), bf16[8,192,512]{2,1,0:T(8,128)(2,1)S(1)}, u32[]{:S(2)}, u32[]{:S(2)}) async-start(bf16[8,192,512]{2,1,0:T(8,128)(2,1)} %get-tuple-element.56), calls=%async_computation.1 | async-start | bytes 3145728 | tf_op jit(solution)/shard_map/all_to_all | solution.py:93
  118.4 12.0 %collective-permute-start.6 = (bf16[384,512]{1,0:T(8,128)(2,1)S(1)}, bf16[384,512]{1,0:T(8,128)(2,1)S(1)}, u32[]{:S(2)}, u32[]{:S(2)}) collective-permute-start(bf16[384,512]{1,0:T(8,128)(2,1)S(1)} %get-tuple-element.59), channel_id=1, source_target_pairs={{0,1},{1,2},{2,3},{3,0},{4,5},{5,6},{6,7},{7,4},{8,9},{9,10},{10,1... | collective-permute-start | bytes 1179656 | tf_op jit(solution)/shard_map/ppermute | solution.py:89
  118.7 14.1 %collective-permute-start.10 = (bf16[384,512]{1,0:T(8,128)(2,1)S(1)}, bf16[384,512]{1,0:T(8,128)(2,1)S(1)}, u32[]{:S(2)}, u32[]{:S(2)}) collective-permute-start(bf16[384,512]{1,0:T(8,128)(2,1)S(1)} %get-tuple-element.63), channel_id=1, source_target_pairs={{0,3},{1,0},{2,1},{3,2},{4,7},{5,4},{6,5},{7,6},{8,11},{9,8},{10,9... | collective-permute-start | bytes 1179656 | tf_op jit(solution)/shard_map/ppermute | solution.py:89
  120.5 18.4 %collective-permute-start.8 = (bf16[384,512]{1,0:T(8,128)(2,1)S(1)}, bf16[384,512]{1,0:T(8,128)(2,1)S(1)}, u32[]{:S(2)}, u32[]{:S(2)}) collective-permute-start(bf16[384,512]{1,0:T(8,128)(2,1)S(1)} %get-tuple-element.60), channel_id=1, source_target_pairs={{0,1},{1,2},{2,3},{3,0},{4,5},{5,6},{6,7},{7,4},{8,9},{9,10},{10,1... | collective-permute-start | bytes 1179656 | tf_op jit(solution)/shard_map/ppermute | solution.py:89
  121.9 18.4 %collective-permute-start.9 = (bf16[384,512]{1,0:T(8,128)(2,1)S(1)}, bf16[384,512]{1,0:T(8,128)(2,1)S(1)}, u32[]{:S(2)}, u32[]{:S(2)}) collective-permute-start(bf16[384,512]{1,0:T(8,128)(2,1)S(1)} %get-tuple-element.61), channel_id=1, source_target_pairs={{0,3},{1,0},{2,1},{3,2},{4,7},{5,4},{6,5},{7,6},{8,11},{9,8},{10,9... | collective-permute-start | bytes 1179656 | tf_op jit(solution)/shard_map/ppermute | solution.py:89
  131.3 13.0 %collective-permute-start.7 = (bf16[384,512]{1,0:T(8,128)(2,1)}, bf16[384,512]{1,0:T(8,128)(2,1)S(1)}, u32[]{:S(2)}, u32[]{:S(2)}) collective-permute-start(bf16[384,512]{1,0:T(8,128)(2,1)} %add_convert_fusion.1), channel_id=1, source_target_pairs={{0,1},{1,2},{2,3},{3,0},{4,5},{5,6},{6,7},{7,4},{8,9},{9,10},{10,1... | collective-permute-start | bytes 1179656 | tf_op jit(solution)/shard_map/ppermute | solution.py:89
  133.6 12.2 %collective-permute-start.11 = (bf16[384,512]{1,0:T(8,128)(2,1)}, bf16[384,512]{1,0:T(8,128)(2,1)}, u32[]{:S(2)}, u32[]{:S(2)}) collective-permute-start(bf16[384,512]{1,0:T(8,128)(2,1)} %add_convert_fusion), channel_id=1, source_target_pairs={{0,3},{1,0},{2,1},{3,2},{4,7},{5,4},{6,5},{7,6},{8,11},{9,8},{10,9... | collective-permute-start | bytes 1179656 | tf_op jit(solution)/shard_map/ppermute | solution.py:89
  148.5 30.7 %all-to-all-start.2 = ((bf16[64,24,256]{2,1,0:T(8,128)(2,1)}), bf16[64,24,256]{2,1,0:T(8,128)(2,1)S(1)}, u32[]{:S(2)}, u32[]{:S(2)}) async-start(bf16[64,24,256]{2,1,0:T(8,128)(2,1)} %bitcast.26), calls=%async_computation.2 | async-start | bytes 1572864 | tf_op jit(solution)/shard_map/all_to_all | solution.py:93
  181.1 14.9 %collective-permute-start.17 = (bf16[192,512]{1,0:T(8,128)(2,1)S(1)}, bf16[192,512]{1,0:T(8,128)(2,1)S(1)}, u32[]{:S(2)}, u32[]{:S(2)}) collective-permute-start(bf16[192,512]{1,0:T(8,128)(2,1)S(1)} %get-tuple-element.73.p0), channel_id=1, source_target_pairs={{0,2},{1,3},{2,0},{3,1},{4,6},{5,7},{6,4},{7,5},{8,10},{9,11},{10,... | collective-permute-start | bytes 589832 | tf_op jit(solution)/shard_map/ppermute | solution.py:89
  182.0 14.1 %collective-permute-start.16 = (bf16[192,512]{1,0:T(8,128)(2,1)S(1)}, bf16[192,512]{1,0:T(8,128)(2,1)S(1)}, u32[]{:S(2)}, u32[]{:S(2)}) collective-permute-start(bf16[192,512]{1,0:T(8,128)(2,1)S(1)} %get-tuple-element.73.p0), channel_id=1, source_target_pairs={{0,3},{1,0},{2,1},{3,2},{4,7},{5,4},{6,5},{7,6},{8,11},{9,8},{10,9... | collective-permute-start | bytes 589832 | tf_op jit(solution)/shard_map/ppermute | solution.py:89
  182.3 13.8 %collective-permute-start.15 = (bf16[192,512]{1,0:T(8,128)(2,1)S(1)}, bf16[192,512]{1,0:T(8,128)(2,1)S(1)}, u32[]{:S(2)}, u32[]{:S(2)}) collective-permute-start(bf16[192,512]{1,0:T(8,128)(2,1)S(1)} %get-tuple-element.73.p0), channel_id=1, source_target_pairs={{0,1},{1,2},{2,3},{3,0},{4,5},{5,6},{6,7},{7,4},{8,9},{9,10},{10,1... | collective-permute-start | bytes 589832 | tf_op jit(solution)/shard_map/ppermute | solution.py:89
  200.0 18.9 %all-to-all-start.5 = ((f32[64,8,128]{2,1,0:T(8,128)}), f32[64,8,128]{2,1,0:T(8,128)S(1)}, u32[]{:S(2)}, u32[]{:S(2)}) async-start(f32[64,8,128]{2,1,0:T(8,128)} %bitcast.28), calls=%async_computation.5 | async-start | bytes 524288 | tf_op jit(solution)/shard_map/all_to_all | solution.py:93
  204.7 9.4 %collective-permute-start.14 = (bf16[8,96,128]{2,1,0:T(8,128)(2,1)S(1)}, bf16[8,96,128]{2,1,0:T(8,128)(2,1)S(1)}, u32[]{:S(2)}, u32[]{:S(2)}) collective-permute-start(bf16[8,96,128]{2,1,0:T(8,128)(2,1)S(1)} %all_to_all.54.p0), channel_id=1, source_target_pairs={{0,2},{1,3},{2,0},{3,1},{4,6},{5,7},{6,4},{7,5},{8,10},{9,11},{10,... | collective-permute-start | bytes 589832 | tf_op jit(solution)/shard_map/ppermute | solution.py:89
  206.3 10.9 %collective-permute-start.13 = (bf16[8,96,128]{2,1,0:T(8,128)(2,1)S(1)}, bf16[8,96,128]{2,1,0:T(8,128)(2,1)S(1)}, u32[]{:S(2)}, u32[]{:S(2)}) collective-permute-start(bf16[8,96,128]{2,1,0:T(8,128)(2,1)S(1)} %all_to_all.54.p0), channel_id=1, source_target_pairs={{0,3},{1,0},{2,1},{3,2},{4,7},{5,4},{6,5},{7,6},{8,11},{9,8},{10,9... | collective-permute-start | bytes 589832 | tf_op jit(solution)/shard_map/ppermute | solution.py:89
  206.7 10.5 %collective-permute-start.12 = (bf16[8,96,128]{2,1,0:T(8,128)(2,1)S(1)}, bf16[8,96,128]{2,1,0:T(8,128)(2,1)S(1)}, u32[]{:S(2)}, u32[]{:S(2)}) collective-permute-start(bf16[8,96,128]{2,1,0:T(8,128)(2,1)S(1)} %all_to_all.54.p0), channel_id=1, source_target_pairs={{0,1},{1,2},{2,3},{3,0},{4,5},{5,6},{6,7},{7,4},{8,9},{9,10},{10,1... | collective-permute-start | bytes 589832 | tf_op jit(solution)/shard_map/ppermute | solution.py:89
  219.0 19.1 %all-to-all-start.4 = ((bf16[8,32,512]{2,1,0:T(8,128)(2,1)}), bf16[8,32,512]{2,1,0:T(8,128)(2,1)S(1)}, u32[]{:S(2)}, u32[]{:S(2)}) async-start(bf16[8,32,512]{2,1,0:T(8,128)(2,1)} %bitcast.27), calls=%async_computation.4 | async-start | bytes 524288 | tf_op jit(solution)/shard_map/all_to_all | solution.py:93
  (6 other events, 91.7 us)
